TPU v7x, 512 devices: a whole 4x8x8 slice. The times are simulated.
512 devices in a mesh: sp: 64 (over z, y), fs: 4 (over x), tp: 2 (over core).
Axes of the slice: x: 4, y: 8, z: 8, core: 2. Of those that a mesh axis runs over, the one named last changes fastest.
Arguments:
- tokens: bfloat16 [65536, 2048], P('sp'), may hold values from -6 to 6
- norm_gain: float32 [2048], replicated, may hold values from 0.1 to 1.9
- w_query: bfloat16 [2048, 2048], P('sp', ('fs', 'tp')), may hold values from -3.6239223 to 3.6239223
- w_key: bfloat16 [2048, 512], P('sp', ('fs', 'tp')), may hold values from -0.088388348 to 0.088388348
- w_value: bfloat16 [2048, 512], P('sp', ('fs', 'tp')), may hold values from -0.8984375 to 0.8984375
- w_conv_in: bfloat16 [2048, 2048], P('sp', ('fs', 'tp')), may hold values from -0.125 to 0.125
- w_conv_gate: bfloat16 [2048, 2048], P('sp', ('fs', 'tp')), may hold values from -0.125 to 0.125
- conv_taps: bfloat16 [3, 2048], P(None, ('fs', 'tp')), may hold values from -3.5 to 3.5
- sink_logits: float32 [32], P(('fs', 'tp')), may hold values from 2 to 6
Outputs:
- mixed: bfloat16 [65536, 2048], P('sp', ('fs', 'tp'))
- log_sums: float32 [32, 65536], P(('fs', 'tp'), 'sp')
All inputs are finite; a program needn't handle non-finite values.
Results may differ from a plain program's by a relative error of at most 0.0077.
Values may be sent and summed in bfloat16 or wider, within the bound.
No kernel may reach another device: no remote copies, remote signals or barrier semaphores. Data moves between devices by JAX's collectives and lax.ppermute only.
A program may use at most 64 MiB of HBM per device.

v0:
```python
import jax
import jax.numpy as jnp
from jax import lax
from jax.experimental import pallas as pl
from jax.experimental.pallas import tpu as pltpu
from jax.sharding import Mesh, PartitionSpec as P


HEAD_DIM = 64
WINDOW = 128
EPS = 1e-06

SP = ("zh", "zl", "yh", "yl")
COLS = ("fs", "tp")
SIDE = 8
LANES = 128


def shift(value, dz, dy):
    pairs = []
    for z in range(SIDE):
        for y in range(SIDE):
            pairs.append((z * SIDE + y, (z + dz) % SIDE * SIDE + (y + dy) % SIDE))
    return lax.ppermute(value, SP, pairs)


def passed_along(value):
    n = SIDE * SIDE
    return lax.ppermute(value, SP, [(i, i + 1) for i in range(n - 1)])


def settings(mib):
    return pltpu.CompilerParams(vmem_limit_bytes=mib << 20)


def cost(us):
    return pl.CostEstimate(flops=int(us * 3.9e6), bytes_accessed=1 << 20, transcendentals=0)


def dot(a, b, dims=((1,), (0,))):
    return lax.dot_general(a, b, (dims, ((), ())), preferred_element_type=jnp.float32)


def norm_kernel(place, tok_ref, gain_ref, out_ref):
    widened = tok_ref[...].astype(jnp.float32)
    scale = lax.rsqrt(jnp.mean(widened * widened, axis=-1, keepdims=True) + EPS)
    normed = (widened * scale * gain_ref[...]).astype(jnp.bfloat16)
    span = 2 * LANES
    row = lax.broadcasted_iota(jnp.int32, (span, span), 0)
    col = lax.broadcasted_iota(jnp.int32, (span, span), 1)
    target = ((row >> 5) & 1) * LANES + (row >> 6) * 32 + (row & 31)
    swap = (target == col).astype(jnp.bfloat16)
    for zh in range(4):
        for zl in range(2):
            at = (zh * 2 + zl) * span
            sorted_cols = dot(normed[:, at : at + span], swap).astype(jnp.bfloat16)
            for yl in range(2):
                out_ref[(place[0] ^ zl) * 2 + (place[1] ^ yl), :, zh * LANES : (zh + 1) * LANES] = (
                    sorted_cols[:, yl * LANES : (yl + 1) * LANES]
                )


def norm_classes(place, rows, gain, block):
    n, width = rows.shape
    return pl.pallas_call(
        norm_kernel,
        grid_spec=pltpu.PrefetchScalarGridSpec(
            num_scalar_prefetch=1,
            grid=(n // block,),
            in_specs=[
                pl.BlockSpec((block, width), lambda i, p: (i, 0)),
                pl.BlockSpec((1, width), lambda i, p: (0, 0)),
            ],
            out_specs=pl.BlockSpec((4, block, width // 4), lambda i, p: (0, i, 0)),
        ),
        out_shape=jax.ShapeDtypeStruct((4, n, width // 4), jnp.bfloat16),
        compiler_params=settings(14),
        cost_estimate=cost(5 if n > 16 else 1),
        name="norm",
    )(place, rows, gain)


def attend_block(q, kv_prev, kv_cur, sinks, has_prev):
    lane = lax.broadcasted_iota(jnp.int32, (WINDOW, LANES), 1)
    left = lane < HEAD_DIM

    def split(kv):
        swapped = pltpu.roll(kv.astype(jnp.float32), HEAD_DIM, 1).astype(jnp.bfloat16)
        zero = jnp.zeros_like(kv)
        return jnp.where(left, kv, zero), jnp.where(left, zero, swapped)

    prev_lo, prev_hi = split(kv_prev)
    cur_lo, cur_hi = split(kv_cur)
    keys = jnp.concatenate([prev_lo, cur_lo, prev_hi, cur_hi], axis=0)
    key_idx = lax.broadcasted_iota(jnp.int32, (WINDOW, WINDOW), 0)
    query_idx = lax.broadcasted_iota(jnp.int32, (WINDOW, WINDOW), 1)
    from_prev = key_idx > query_idx
    weights, logs = [], []
    for pair in range(2):
        both = dot(keys, q[:, pair * LANES : (pair + 1) * LANES], ((1,), (1,)))
        for side in range(2):
            head = pair * 2 + side
            prev = both[side * 256 : side * 256 + WINDOW]
            cur = both[side * 256 + WINDOW : side * 256 + 2 * WINDOW]
            if has_prev is not None:
                prev = jnp.where(has_prev, prev, -jnp.inf)
            scores = jnp.where(from_prev, prev, cur) * HEAD_DIM ** (-0.5)
            top = jnp.maximum(jnp.max(scores, axis=0, keepdims=True), sinks[head])
            raised = jnp.exp(scores - top)
            total = jnp.sum(raised, axis=0, keepdims=True) + jnp.exp(sinks[head] - top)
            logs.append(top + jnp.log(total))
            share = raised / total
            zero = jnp.zeros_like(share)
            weights.append(
                jnp.concatenate(
                    [jnp.where(from_prev, share, zero), jnp.where(from_prev, zero, share)], axis=0
                ).astype(jnp.bfloat16)
            )
    values = jnp.concatenate([kv_prev, kv_cur], axis=0)
    outs = []
    for pair in range(2):
        got = dot(values, jnp.concatenate(weights[pair * 2 : pair * 2 + 2], axis=1), ((0,), (0,)))
        stacked = jnp.concatenate([got[HEAD_DIM:, :WINDOW], got[HEAD_DIM:, WINDOW:]], axis=0)
        outs.append(stacked.T)
    return jnp.concatenate(outs, axis=1), jnp.concatenate(logs, axis=0)


def tail_kernel(x_ref, w0, w1, w2, w3, out_ref):
    acc = dot(x_ref[0], w0[...])
    for c, w in ((1, w1), (2, w2), (3, w3)):
        acc = acc + dot(x_ref[c], w[...])
    out_ref[...] = acc.astype(jnp.bfloat16)


def tail_rows(x, parts):
    n, depth = x.shape[1], x.shape[2]
    last = n // WINDOW - 1
    return pl.pallas_call(
        tail_kernel,
        grid=(1,),
        in_specs=[pl.BlockSpec((4, WINDOW, depth), lambda i: (0, last, 0))]
        + [pl.BlockSpec((depth, LANES), lambda i: (0, 0))] * 4,
        out_specs=pl.BlockSpec((WINDOW, LANES), lambda i: (0, 0)),
        out_shape=jax.ShapeDtypeStruct((WINDOW, LANES), jnp.bfloat16),
        compiler_params=settings(6),
        cost_estimate=cost(1),
        name="tail",
    )(x, *parts)


def attn_kernel(sinks, x_ref, w0, w1, w2, w3, att_ref, log_ref, rows_ref):
    n = x_ref.shape[1]
    step = 256
    parts = (w0, w1, w2, w3)
    for at in range(0, n, step):
        acc = dot(x_ref[0, at : at + step, :], w0[...])
        for c in range(1, 4):
            acc = acc + dot(x_ref[c, at : at + step, :], parts[c][...])
        rows_ref[at : at + step, :] = acc.astype(jnp.bfloat16)
    heads = [sinks[h] for h in range(4)]
    att_ref[:WINDOW, :] = jnp.zeros((WINDOW, 2 * LANES), jnp.float32)
    log_ref[:, :WINDOW] = jnp.zeros((4, WINDOW), jnp.float32)

    for b in range(1, n // WINDOW):
        here, before = b * WINDOW, (b - 1) * WINDOW
        att, logs = attend_block(
            rows_ref[here : here + WINDOW, LANES:],
            rows_ref[before : before + WINDOW, :LANES],
            rows_ref[here : here + WINDOW, :LANES],
            heads,
            None,
        )
        att_ref[here : here + WINDOW, :] = att
        log_ref[:, here : here + WINDOW] = logs


VMEM = pl.BlockSpec(memory_space=pltpu.VMEM)
SMEM = pl.BlockSpec(memory_space=pltpu.SMEM)


def attention(sinks, x, parts):
    n = x.shape[1]
    cols = parts[0].shape[1]
    return pl.pallas_call(
        attn_kernel,
        in_specs=[SMEM] + [VMEM] * 5,
        out_specs=[VMEM] * 3,
        out_shape=[
            jax.ShapeDtypeStruct((n, 2 * LANES), jnp.float32),
            jax.ShapeDtypeStruct((4, n), jnp.float32),
            jax.ShapeDtypeStruct((n, cols), jnp.bfloat16),
        ],
        compiler_params=settings(20),
        cost_estimate=cost(8),
        name="attn",
    )(sinks, x, *parts)


def conv_kernel(
    sinks, has_prev, x_ref, w0, w1, w2, w3, prev_x, taps_ref, att_ref, log_ref, rows_ref, halo_ref,
    out_ref, log_out, pad_ref,
):
    n = x_ref.shape[1]
    width = 2 * LANES
    step = 256
    parts = (w0, w1, w2, w3)
    acc = dot(prev_x[0], w0[:, :width])
    for c in range(1, 4):
        acc = acc + dot(prev_x[c], parts[c][:, :width])
    pad_ref[:8, :] = acc[8:16].astype(jnp.bfloat16).astype(jnp.float32)
    att0, log0 = attend_block(
        rows_ref[:WINDOW, LANES:],
        halo_ref[...],
        rows_ref[:WINDOW, :LANES],
        [sinks[h] for h in range(4)],
        has_prev[0] > 0,
    )
    log_out[...] = log_ref[...]
    log_out[:, :WINDOW] = log0
    taps = taps_ref[...].astype(jnp.float32)
    for at in range(0, n, step):
        acc = dot(x_ref[0, at : at + step, :], w0[...])
        for c in range(1, 4):
            acc = acc + dot(x_ref[c, at : at + step, :], parts[c][...])
        rounded = acc.astype(jnp.bfloat16).astype(jnp.float32)
        pad_ref[8 + at : 8 + at + step, :] = rounded[:, :width]
        total = taps[0:1] * pad_ref[6 + at : 6 + at + step, :]
        total = total + taps[1:2] * pad_ref[7 + at : 7 + at + step, :]
        total = total + taps[2:3] * rounded[:, :width]
        gated = rounded[:, width:] * total
        if at == 0:
            first = jnp.concatenate([att0, att_ref[WINDOW:step, :]], axis=0)
        else:
            first = att_ref[at : at + step, :]
        out_ref[at : at + step, :] = (first + gated).astype(jnp.bfloat16)


def convolution(sinks, has_prev, x, parts, prev_x, taps, att, logs, rows, halo):
    n = x.shape[1]
    return pl.pallas_call(
        conv_kernel,
        in_specs=[SMEM] * 2 + [VMEM] * 11,
        out_specs=[VMEM] * 2,
        out_shape=[
            jax.ShapeDtypeStruct((n, 2 * LANES), jnp.bfloat16),
            jax.ShapeDtypeStruct((4, n), jnp.float32),
        ],
        scratch_shapes=[pltpu.VMEM((n + 8, 2 * LANES), jnp.float32)],
        compiler_params=settings(20),
        cost_estimate=cost(6),
        name="conv",
    )(sinks, has_prev, x, *parts, prev_x, taps, att, logs, rows, halo)


def body(
    tokens, norm_gain, w_query, w_key, w_value, w_conv_in, w_conv_gate, conv_taps, sink_logits
):
    return layer(
        tokens, norm_gain, (w_key, w_value, w_query), (w_conv_in, w_conv_gate), conv_taps, sink_logits
    )


def layer(tokens, norm_gain, attn_weights, conv_weights, conv_taps, sink_logits):
    n, width = tokens.shape
    mine = jnp.concatenate(attn_weights + conv_weights, axis=1)
    cut = sum(w.shape[1] for w in attn_weights)
    sent = jnp.broadcast_to(mine[None], (16,) + mine.shape)
    own = lax.all_to_all(sent, ("zh", "yh"), 0, 0)
    own = own.reshape(16 * mine.shape[0], mine.shape[1])
    prev_tokens = passed_along(tokens[n - 16 :])

    place = jnp.stack([lax.axis_index("zl"), lax.axis_index("yl")]).astype(jnp.int32)
    gain = norm_gain.reshape(1, width)
    x = norm_classes(place, tokens, gain, 256)
    prev_x = norm_classes(place, prev_tokens, gain, 16)

    def classes(block):
        parts = [block]
        for dz, dy in ((0, 1), (1, 0), (-1, -1)):
            parts.append(shift(block, dz, dy))
        return parts

    parts_a = classes(own[:, :cut])
    parts_b = classes(own[:, cut:])
    has_prev = (lax.axis_index(SP) > 0).astype(jnp.int32).reshape(1)
    last = tail_rows(x, parts_a)
    halo = passed_along(last)
    att, logs, rows = attention(sink_logits, x, parts_a)
    return tuple(
        convolution(
            sink_logits, has_prev, x, parts_b, prev_x, conv_taps, att, logs, rows, halo
        )
    )


def solution(mesh):
    fine = Mesh(
        mesh.devices.reshape(4, 2, 4, 2, mesh.shape["fs"], mesh.shape["tp"]), SP + COLS
    )
    weights = P(SP, COLS)
    return jax.shard_map(
        body,
        mesh=fine,
        in_specs=(P(SP, None), P()) + (weights,) * 5 + (P(None, COLS), P(COLS)),
        out_specs=(P(SP, COLS), P(COLS, SP)),
        check_vma=False,
    )
```

profile of v0, /device:TPU:6, one launch (start us, length us, event | category | flops | bytes accessed | tf_op | source)
XLA Modules:
  0.0 100.5 jit_solution(8847008086086059342)
XLA Ops:
  0.6 0.0 copy-start.3
  0.6 0.9 concatenate.3
  1.5 0.1 broadcast_in_dim.2
  1.6 44.8 %all_to_all.5 = bf16[16,32,896]{2,1,0:T(8,128)(2,1)S(1)} all-to-all(bf16[16,32,896]{2,1,0:T(8,128)(2,1)S(1)} %broadcast_in_dim.2), channel_id=1, replica_groups=mesh['zh'=4,'zl'=2,'yh'=4,'yl'=2,'fs'=4,'tp'=2] {'zh','yh'}, dimensions={0} | all-to-all | bytes 1835008 | tf_op jit(solution)/shard_map/all_to_all | solution.py:268
  46.4 1.9 %collective-permute-start.4 = (bf16[512,384]{1,0:T(8,128)(2,1)S(1)}, bf16[512,384]{1,0:T(8,128)(2,1)S(1)}, u32[]{:S(2)}, u32[]{:S(2)}) collective-permute-start(bf16[512,384]{1,0:T(8,128)(2,1)S(1)} %slice.13.w0), channel_id=1, source_target_pairs={{0,8},{8,16},{16,24},{24,32},{32,40},{40,48},{48,56},{56,0},{64,72... | collective-permute-start | bytes 1179656 | tf_op jit(solution)/shard_map/ppermute | solution.py:24
  48.3 3.3 %collective-permute-start.5 = (bf16[512,384]{1,0:T(8,128)(2,1)S(1)}, bf16[512,384]{1,0:T(8,128)(2,1)S(1)}, u32[]{:S(2)}, u32[]{:S(2)}) collective-permute-start(bf16[512,384]{1,0:T(8,128)(2,1)S(1)} %slice.13.w0), channel_id=1, source_target_pairs={{0,64},{8,72},{16,80},{24,88},{32,96},{40,104},{48,112},{56,120},{... | collective-permute-start | bytes 1179656 | tf_op jit(solution)/shard_map/ppermute | solution.py:24
  51.7 4.7 %collective-permute-start = (bf16[512,512]{1,0:T(8,128)(2,1)S(1)}, bf16[512,512]{1,0:T(8,128)(2,1)S(1)}, u32[]{:S(2)}, u32[]{:S(2)}) collective-permute-start(bf16[512,512]{1,0:T(8,128)(2,1)S(1)} %slice.12.w0), channel_id=1, source_target_pairs={{0,8},{8,16},{16,24},{24,32},{32,40},{40,48},{48,56},{56,0},{64,72... | collective-permute-start | bytes 1572872 | tf_op jit(solution)/shard_map/ppermute | solution.py:24
  56.5 1.9 %collective-permute-start.1 = (bf16[512,512]{1,0:T(8,128)(2,1)S(1)}, bf16[512,512]{1,0:T(8,128)(2,1)S(1)}, u32[]{:S(2)}, u32[]{:S(2)}) collective-permute-start(bf16[512,512]{1,0:T(8,128)(2,1)S(1)} %slice.12.w0), channel_id=1, source_target_pairs={{0,64},{8,72},{16,80},{24,88},{32,96},{40,104},{48,112},{56,120},{... | collective-permute-start | bytes 1572872 | tf_op jit(solution)/shard_map/ppermute | solution.py:24
  58.4 5.0 %collective-permute-start.2 = (bf16[512,512]{1,0:T(8,128)(2,1)S(1)}, bf16[512,512]{1,0:T(8,128)(2,1)}, u32[]{:S(2)}, u32[]{:S(2)}) collective-permute-start(bf16[512,512]{1,0:T(8,128)(2,1)S(1)} %slice.12.w0), channel_id=1, source_target_pairs={{0,504},{8,448},{16,456},{24,464},{32,472},{40,480},{48,488},{56,4... | collective-permute-start | bytes 1572872 | tf_op jit(solution)/shard_map/ppermute | solution.py:24
  63.4 0.0 collective-permute-done.4.w1
  63.4 4.0 %collective-permute-start.6 = (bf16[512,384]{1,0:T(8,128)(2,1)S(1)}, bf16[512,384]{1,0:T(8,128)(2,1)S(1)}, u32[]{:S(2)}, u32[]{:S(2)}) collective-permute-start(bf16[512,384]{1,0:T(8,128)(2,1)S(1)} %slice.13.w0), channel_id=1, source_target_pairs={{0,504},{8,448},{16,456},{24,464},{32,472},{40,480},{48,488},{56,4... | collective-permute-start | bytes 1179656 | tf_op jit(solution)/shard_map/ppermute | solution.py:24
  67.4 0.8 slice.10
  68.2 0.0 collective-permute-done.5.w2
  68.2 1.9 %collective-permute-start.3 = (bf16[16,2048]{1,0:T(8,128)(2,1)S(1)}, bf16[16,2048]{1,0:T(8,128)(2,1)S(1)}, u32[]{:S(2)}, u32[]{:S(2)}) collective-permute-start(bf16[16,2048]{1,0:T(8,128)(2,1)S(1)} %slice.10), channel_id=1, source_target_pairs={{0,8},{8,16},{16,24},{24,32},{32,40},{40,48},{48,56},{56,64},{64,7... | collective-permute-start | bytes 196616 | tf_op jit(solution)/shard_map/ppermute | solution.py:29
  70.1 0.1 pad_add_fusion.place
  70.2 0.0 copy-done.3
  70.2 0.0 copy-start.2
  70.2 2.2 %copy-done.2 = bf16[1024,2048]{1,0:T(8,128)(2,1)S(1)} copy-done((bf16[1024,2048]{1,0:T(8,128)(2,1)S(1)}, bf16[1024,2048]{1,0:T(8,128)(2,1)}, u32[]{:S(2)}) %copy-start.2) | copy-done | bytes 4194328
  72.4 4.1 %norm.2.x_ref = bf16[4,1024,512]{2,1,0:T(8,128)(2,1)S(1)} custom-call(s32[2]{0:T(128)S(1)} %pad_add_fusion.place, bf16[1024,2048]{1,0:T(8,128)(2,1)S(1)} %copy-done.2, f32[1,2048]{1,0:T(1,128)S(1)} %bitcast.5), custom_call_target="tpu_custom_call" | custom-call | flops 19500000 | bytes 1048576 | tf_op jit(solution)/shard_map/norm/pallas_call | solution.py:65
  76.5 0.0 copy-start.5
  76.5 5.2 %collective-permute-done.6.w3 = bf16[512,384]{1,0:T(8,128)(2,1)S(1)} collective-permute-done((bf16[512,384]{1,0:T(8,128)(2,1)S(1)}, bf16[512,384]{1,0:T(8,128)(2,1)S(1)}, u32[]{:S(2)}, u32[]{:S(2)}) %collective-permute-start.6) | collective-permute-done | bytes 393248 | tf_op jit(solution)/shard_map/ppermute | solution.py:24
  81.7 0.3 tail.1
  82.0 0.0 copy-start
  82.1 1.9 %copy-done = bf16[4,1024,512]{2,1,0:T(8,128)(2,1)} copy-done((bf16[4,1024,512]{2,1,0:T(8,128)(2,1)}, bf16[4,1024,512]{2,1,0:T(8,128)(2,1)S(1)}, u32[]{:S(2)}) %copy-start) | copy-done | bytes 4194328
  84.0 0.0 copy-start.4
  84.0 3.3 %collective-permute-start.7 = (bf16[128,128]{1,0:T(8,128)(2,1)S(1)}, bf16[128,128]{1,0:T(8,128)(2,1)S(1)}, u32[]{:S(2)}, u32[]{:S(2)}) collective-permute-start(bf16[128,128]{1,0:T(8,128)(2,1)S(1)} %tail.1), channel_id=1, source_target_pairs={{0,8},{8,16},{16,24},{24,32},{32,40},{40,48},{48,56},{56,64},{64,7... | collective-permute-start | bytes 98312 | tf_op jit(solution)/shard_map/ppermute | solution.py:29
  87.4 0.0 collective-permute-done.3.tok_ref
  87.4 0.9 norm.3.prev_x
  88.2 0.0 copy-done.5
  88.2 0.0 copy-start.1
  88.3 2.2 %copy-done.1 = bf16[4,1024,512]{2,1,0:T(8,128)(2,1)S(1)} copy-done((bf16[4,1024,512]{2,1,0:T(8,128)(2,1)S(1)}, bf16[4,1024,512]{2,1,0:T(8,128)(2,1)}, u32[]{:S(2)}) %copy-start.1) | copy-done | bytes 4194328
  90.4 5.3 %attn.1 = (f32[1024,256]{1,0:T(8,128)S(1)}, f32[4,1024]{1,0:T(4,128)S(1)}, bf16[1024,384]{1,0:T(8,128)(2,1)S(1)}) custom-call(f32[4]{0:T(128)S(1)} %copy-done.5, bf16[4,1024,512]{2,1,0:T(8,128)(2,1)S(1)} %copy-done.1, bf16[512,384]{1,0:T(8,128)(2,1)S(1)} %slice.13.w0, bf16[512,384]{1,0:T(8,128)(2,1)S(1)} %collective-permute-done.4.w1, ...), custom_call_target="tpu_custom_call" | custom-call | flops 31200000 | bytes 1048576 | tf_op jit(solution)/shard_map/attn/pallas_call | solution.py:184
  95.7 0.0 collective-permute-done.7.halo_ref
  95.7 0.0 collective-permute-done.w1
  95.7 0.0 collective-permute-done.1.w2
  95.7 0.0 collective-permute-done.2.w3
  95.7 0.0 copy-done.4
  95.8 4.7 %conv.1 = (bf16[1024,256]{1,0:T(8,128)(2,1)}, f32[4,1024]{1,0:T(4,128)}) custom-call(f32[4]{0:T(128)S(1)} %copy-done.5, s32[1]{0:T(128)} %bitcast.has_prev, bf16[4,1024,512]{2,1,0:T(8,128)(2,1)S(1)} %copy-done.1, bf16[512,512]{1,0:T(8,128)(2,1)S(1)} %slice.12.w0, bf16[512,512]{1,0:T(8,128)(2,1)S(1)} %collective-permute-done.w1, ...), custom_call_target="tpu_custom_call" | custom-call | flops 23400000 | bytes 1048576 | tf_op jit(solution)/shard_map/conv/pallas_call | solution.py:240
  (2 shorter events, 0.1 us)
Async XLA Ops:
  0.6 69.6 %copy-start.3 = (f32[2048]{0:T(1024)S(1)}, f32[2048]{0:T(1024)}, u32[]{:S(2)}) copy-start(f32[2048]{0:T(1024)} %param.10) | copy-start | bytes 24580
  46.4 17.0 %collective-permute-start.4 = (bf16[512,384]{1,0:T(8,128)(2,1)S(1)}, bf16[512,384]{1,0:T(8,128)(2,1)S(1)}, u32[]{:S(2)}, u32[]{:S(2)}) collective-permute-start(bf16[512,384]{1,0:T(8,128)(2,1)S(1)} %slice.13.w0), channel_id=1, source_target_pairs={{0,8},{8,16},{16,24},{24,32},{32,40},{40,48},{48,56},{56,0},{64,72... | collective-permute-start | bytes 1179656 | tf_op jit(solution)/shard_map/ppermute | solution.py:24
  48.3 19.9 %collective-permute-start.5 = (bf16[512,384]{1,0:T(8,128)(2,1)S(1)}, bf16[512,384]{1,0:T(8,128)(2,1)S(1)}, u32[]{:S(2)}, u32[]{:S(2)}) collective-permute-start(bf16[512,384]{1,0:T(8,128)(2,1)S(1)} %slice.13.w0), channel_id=1, source_target_pairs={{0,64},{8,72},{16,80},{24,88},{32,96},{40,104},{48,112},{56,120},{... | collective-permute-start | bytes 1179656 | tf_op jit(solution)/shard_map/ppermute | solution.py:24
  51.7 44.0 %collective-permute-start = (bf16[512,512]{1,0:T(8,128)(2,1)S(1)}, bf16[512,512]{1,0:T(8,128)(2,1)S(1)}, u32[]{:S(2)}, u32[]{:S(2)}) collective-permute-start(bf16[512,512]{1,0:T(8,128)(2,1)S(1)} %slice.12.w0), channel_id=1, source_target_pairs={{0,8},{8,16},{16,24},{24,32},{32,40},{40,48},{48,56},{56,0},{64,72... | collective-permute-start | bytes 1572872 | tf_op jit(solution)/shard_map/ppermute | solution.py:24
  56.5 39.3 %collective-permute-start.1 = (bf16[512,512]{1,0:T(8,128)(2,1)S(1)}, bf16[512,512]{1,0:T(8,128)(2,1)S(1)}, u32[]{:S(2)}, u32[]{:S(2)}) collective-permute-start(bf16[512,512]{1,0:T(8,128)(2,1)S(1)} %slice.12.w0), channel_id=1, source_target_pairs={{0,64},{8,72},{16,80},{24,88},{32,96},{40,104},{48,112},{56,120},{... | collective-permute-start | bytes 1572872 | tf_op jit(solution)/shard_map/ppermute | solution.py:24
  58.4 37.4 %collective-permute-start.2 = (bf16[512,512]{1,0:T(8,128)(2,1)S(1)}, bf16[512,512]{1,0:T(8,128)(2,1)}, u32[]{:S(2)}, u32[]{:S(2)}) collective-permute-start(bf16[512,512]{1,0:T(8,128)(2,1)S(1)} %slice.12.w0), channel_id=1, source_target_pairs={{0,504},{8,448},{16,456},{24,464},{32,472},{40,480},{48,488},{56,4... | collective-permute-start | bytes 1572872 | tf_op jit(solution)/shard_map/ppermute | solution.py:24
  63.4 18.3 %collective-permute-start.6 = (bf16[512,384]{1,0:T(8,128)(2,1)S(1)}, bf16[512,384]{1,0:T(8,128)(2,1)S(1)}, u32[]{:S(2)}, u32[]{:S(2)}) collective-permute-start(bf16[512,384]{1,0:T(8,128)(2,1)S(1)} %slice.13.w0), channel_id=1, source_target_pairs={{0,504},{8,448},{16,456},{24,464},{32,472},{40,480},{48,488},{56,4... | collective-permute-start | bytes 1179656 | tf_op jit(solution)/shard_map/ppermute | solution.py:24
  68.2 19.2 %collective-permute-start.3 = (bf16[16,2048]{1,0:T(8,128)(2,1)S(1)}, bf16[16,2048]{1,0:T(8,128)(2,1)S(1)}, u32[]{:S(2)}, u32[]{:S(2)}) collective-permute-start(bf16[16,2048]{1,0:T(8,128)(2,1)S(1)} %slice.10), channel_id=1, source_target_pairs={{0,8},{8,16},{16,24},{24,32},{32,40},{40,48},{48,56},{56,64},{64,7... | collective-permute-start | bytes 196616 | tf_op jit(solution)/shard_map/ppermute | solution.py:29
  70.2 2.2 %copy-start.2 = (bf16[1024,2048]{1,0:T(8,128)(2,1)S(1)}, bf16[1024,2048]{1,0:T(8,128)(2,1)}, u32[]{:S(2)}) copy-start(bf16[1024,2048]{1,0:T(8,128)(2,1)} %tok_ref.1) | copy-start | bytes 12582916
  76.5 11.7 %copy-start.5 = (f32[4]{0:T(128)S(1)}, f32[4]{0:T(128)}, u32[]{:S(2)}) copy-start(f32[4]{0:T(128)} %sinks.3) | copy-start | bytes 52
  82.0 1.9 %copy-start = (bf16[4,1024,512]{2,1,0:T(8,128)(2,1)}, bf16[4,1024,512]{2,1,0:T(8,128)(2,1)S(1)}, u32[]{:S(2)}) copy-start(bf16[4,1024,512]{2,1,0:T(8,128)(2,1)S(1)} %norm.2.x_ref) | copy-start | bytes 12582916
  84.0 11.8 %copy-start.4 = (bf16[3,256]{1,0:T(4,128)(2,1)S(1)}, bf16[3,256]{1,0:T(4,128)(2,1)}, u32[]{:S(2)}) copy-start(bf16[3,256]{1,0:T(4,128)(2,1)} %taps_ref.1) | copy-start | bytes 4612
  84.0 11.7 %collective-permute-start.7 = (bf16[128,128]{1,0:T(8,128)(2,1)S(1)}, bf16[128,128]{1,0:T(8,128)(2,1)S(1)}, u32[]{:S(2)}, u32[]{:S(2)}) collective-permute-start(bf16[128,128]{1,0:T(8,128)(2,1)S(1)} %tail.1), channel_id=1, source_target_pairs={{0,8},{8,16},{16,24},{24,32},{32,40},{40,48},{48,56},{56,64},{64,7... | collective-permute-start | bytes 98312 | tf_op jit(solution)/shard_map/ppermute | solution.py:29
  88.2 2.2 %copy-start.1 = (bf16[4,1024,512]{2,1,0:T(8,128)(2,1)S(1)}, bf16[4,1024,512]{2,1,0:T(8,128)(2,1)}, u32[]{:S(2)}) copy-start(bf16[4,1024,512]{2,1,0:T(8,128)(2,1)} %copy-done) | copy-start | bytes 12582916
where the time goes:
time: 101 us; the launch traced here: 100 us
  blocking collectives  44.8 us (44%)
  starting transfers between devices  26.1 us (26%)
  Pallas kernels  15.3 us (15%)
  local copies, waits for them, and re-layouts  8.21 us (8%)
  waiting for transfers between devices  5.19 us (5%)
    all_to_all x1, blocking collectives, layer(): own = lax.all_to_all(sent, ('zh', 'yh'), 0, 0)  44.8 us
    ppermute x6, starting transfers between devices, shift(): return lax.ppermute(value, SP, pairs)  20.8 us
    unnamed x12, local copies, waits for them, and re-layouts  6.34 us
    pallas_call x1, Pallas kernels, attention(): pl.pallas_call(attn_kernel, in_specs=[SMEM] + [VMEM] * 5, out_specs=[VMEM...  5.26 us
    ppermute x2, starting transfers between devices, passed_along(): return lax.ppermute(value, SP, [(i, i + 1) for i in range(n - 1)])  5.26 us
    ppermute x6, waiting for transfers between devices, shift(): return lax.ppermute(value, SP, pairs)  5.19 us
    pallas_call x2, Pallas kernels, norm_classes(): pl.pallas_call(norm_kernel, grid_spec=pltpu.PrefetchScalarGridSpec(num_sc...  4.97 us
    pallas_call x1, Pallas kernels, convolution(): pl.pallas_call(conv_kernel, in_specs=[SMEM] * 2 + [VMEM] * 11, out_specs=...  4.73 us
  transfers between devices with their start and end apart: 8, of which 1 were waited for; matrix products, arithmetic and copies ran while one was open for 1% of the time, Pallas kernels for 11%

commit v1 on v0

--- a/solution.py
+++ b/solution.py
@@ -1,3 +1,5 @@
+import functools
+
 import jax
 import jax.numpy as jnp
 from jax import lax
@@ -14,6 +16,9 @@
 COLS = ("fs", "tp")
 SIDE = 8
 LANES = 128
+VMEM = pl.BlockSpec(memory_space=pltpu.VMEM)
+SMEM = pl.BlockSpec(memory_space=pltpu.SMEM)
+HBM = pl.BlockSpec(memory_space=pltpu.HBM)
 
 
 def shift(value, dz, dy):
@@ -41,39 +46,43 @@
     return lax.dot_general(a, b, (dims, ((), ())), preferred_element_type=jnp.float32)
 
 
-def norm_kernel(place, tok_ref, gain_ref, out_ref):
-    widened = tok_ref[...].astype(jnp.float32)
-    scale = lax.rsqrt(jnp.mean(widened * widened, axis=-1, keepdims=True) + EPS)
-    normed = (widened * scale * gain_ref[...]).astype(jnp.bfloat16)
+def norm_kernel(place, tok_hbm, gain_ref, out_hbm, *, block):
+    n, width = tok_hbm.shape
     span = 2 * LANES
     row = lax.broadcasted_iota(jnp.int32, (span, span), 0)
     col = lax.broadcasted_iota(jnp.int32, (span, span), 1)
     target = ((row >> 5) & 1) * LANES + (row >> 6) * 32 + (row & 31)
     swap = (target == col).astype(jnp.bfloat16)
-    for zh in range(4):
-        for zl in range(2):
-            at = (zh * 2 + zl) * span
-            sorted_cols = dot(normed[:, at : at + span], swap).astype(jnp.bfloat16)
-            for yl in range(2):
-                out_ref[(place[0] ^ zl) * 2 + (place[1] ^ yl), :, zh * LANES : (zh + 1) * LANES] = (
-                    sorted_cols[:, yl * LANES : (yl + 1) * LANES]
-                )
+
+    def step(tok_ref, out_ref):
+        widened = tok_ref[...].astype(jnp.float32)
+        scale = lax.rsqrt(jnp.mean(widened * widened, axis=-1, keepdims=True) + EPS)
+        normed = (widened * scale * gain_ref[...]).astype(jnp.bfloat16)
+        for zh in range(4):
+            for zl in range(2):
+                at = (zh * 2 + zl) * span
+                sorted_cols = dot(normed[:, at : at + span], swap).astype(jnp.bfloat16)
+                for yl in range(2):
+                    into = (place[0] ^ zl) * 2 + (place[1] ^ yl)
+                    out_ref[into, :, zh * LANES : (zh + 1) * LANES] = sorted_cols[
+                        :, yl * LANES : (yl + 1) * LANES
+                    ]
+
+    pltpu.emit_pipeline(
+        step,
+        grid=(n // block,),
+        in_specs=[pl.BlockSpec((block, width), lambda i: (i, 0))],
+        out_specs=[pl.BlockSpec((4, block, width // 4), lambda i: (0, i, 0))],
+    )(tok_hbm, out_hbm)
 
 
 def norm_classes(place, rows, gain, block):
     n, width = rows.shape
     return pl.pallas_call(
-        norm_kernel,
-        grid_spec=pltpu.PrefetchScalarGridSpec(
-            num_scalar_prefetch=1,
-            grid=(n // block,),
-            in_specs=[
-                pl.BlockSpec((block, width), lambda i, p: (i, 0)),
-                pl.BlockSpec((1, width), lambda i, p: (0, 0)),
-            ],
-            out_specs=pl.BlockSpec((4, block, width // 4), lambda i, p: (0, i, 0)),
-        ),
-        out_shape=jax.ShapeDtypeStruct((4, n, width // 4), jnp.bfloat16),
+        functools.partial(norm_kernel, block=block),
+        in_specs=[SMEM, HBM, VMEM],
+        out_specs=HBM,
+        out_shape=pltpu.HBM((4, n, width // 4), jnp.bfloat16),
         compiler_params=settings(14),
         cost_estimate=cost(5 if n > 16 else 1),
         name="norm",
@@ -125,34 +134,47 @@
     return jnp.concatenate(outs, axis=1), jnp.concatenate(logs, axis=0)
 
 
-def tail_kernel(x_ref, w0, w1, w2, w3, out_ref):
-    acc = dot(x_ref[0], w0[...])
+def tail_kernel(x_hbm, w0, w1, w2, w3, out_ref, x_ref, sem):
+    n = x_hbm.shape[1]
+    copy = pltpu.make_async_copy(x_hbm.at[:, n - WINDOW : n, :], x_ref, sem)
+    copy.start()
+    copy.wait()
+    acc = dot(x_ref[0], w0[:, :LANES])
     for c, w in ((1, w1), (2, w2), (3, w3)):
-        acc = acc + dot(x_ref[c], w[...])
+        acc = acc + dot(x_ref[c], w[:, :LANES])
     out_ref[...] = acc.astype(jnp.bfloat16)
 
 
 def tail_rows(x, parts):
-    n, depth = x.shape[1], x.shape[2]
-    last = n // WINDOW - 1
     return pl.pallas_call(
         tail_kernel,
-        grid=(1,),
-        in_specs=[pl.BlockSpec((4, WINDOW, depth), lambda i: (0, last, 0))]
-        + [pl.BlockSpec((depth, LANES), lambda i: (0, 0))] * 4,
-        out_specs=pl.BlockSpec((WINDOW, LANES), lambda i: (0, 0)),
+        in_specs=[HBM] + [VMEM] * 4,
+        out_specs=VMEM,
         out_shape=jax.ShapeDtypeStruct((WINDOW, LANES), jnp.bfloat16),
+        scratch_shapes=[
+            pltpu.VMEM((4, WINDOW, x.shape[2]), jnp.bfloat16),
+            pltpu.SemaphoreType.DMA(()),
+        ],
         compiler_params=settings(6),
         cost_estimate=cost(1),
         name="tail",
     )(x, *parts)
 
 
-def attn_kernel(sinks, x_ref, w0, w1, w2, w3, att_ref, log_ref, rows_ref):
+def attn_kernel(sinks, x_hbm, w0, w1, w2, w3, att_ref, log_ref, rows_ref, x_ref, sems):
     n = x_ref.shape[1]
     step = 256
     parts = (w0, w1, w2, w3)
-    for at in range(0, n, step):
+    copies = []
+    for k, at in enumerate(range(0, n, step)):
+        copies.append(
+            pltpu.make_async_copy(
+                x_hbm.at[:, at : at + step, :], x_ref.at[:, at : at + step, :], sems.at[k]
+            )
+        )
+        copies[-1].start()
+    for k, at in enumerate(range(0, n, step)):
+        copies[k].wait()
         acc = dot(x_ref[0, at : at + step, :], w0[...])
         for c in range(1, 4):
             acc = acc + dot(x_ref[c, at : at + step, :], parts[c][...])
@@ -174,22 +196,20 @@
         log_ref[:, here : here + WINDOW] = logs
 
 
-VMEM = pl.BlockSpec(memory_space=pltpu.VMEM)
-SMEM = pl.BlockSpec(memory_space=pltpu.SMEM)
-
-
 def attention(sinks, x, parts):
     n = x.shape[1]
     cols = parts[0].shape[1]
     return pl.pallas_call(
         attn_kernel,
-        in_specs=[SMEM] + [VMEM] * 5,
-        out_specs=[VMEM] * 3,
+        in_specs=[SMEM, HBM] + [VMEM] * 4,
+        out_specs=[VMEM] * 4,
         out_shape=[
             jax.ShapeDtypeStruct((n, 2 * LANES), jnp.float32),
             jax.ShapeDtypeStruct((4, n), jnp.float32),
             jax.ShapeDtypeStruct((n, cols), jnp.bfloat16),
+            jax.ShapeDtypeStruct(x.shape, x.dtype),
         ],
+        scratch_shapes=[pltpu.SemaphoreType.DMA((n // 256,))],
         compiler_params=settings(20),
         cost_estimate=cost(8),
         name="attn",
@@ -197,7 +217,7 @@
 
 
 def conv_kernel(
-    sinks, has_prev, x_ref, w0, w1, w2, w3, prev_x, taps_ref, att_ref, log_ref, rows_ref, halo_ref,
+    sinks, place, x_ref, w0, w1, w2, w3, prev_x, taps_ref, att_ref, log_ref, rows_ref, halo_ref,
     out_ref, log_out, pad_ref,
 ):
     n = x_ref.shape[1]
@@ -213,7 +233,7 @@
         halo_ref[...],
         rows_ref[:WINDOW, :LANES],
         [sinks[h] for h in range(4)],
-        has_prev[0] > 0,
+        place[2] > 0,
     )
     log_out[...] = log_ref[...]
     log_out[:, :WINDOW] = log0
@@ -235,7 +255,7 @@
         out_ref[at : at + step, :] = (first + gated).astype(jnp.bfloat16)
 
 
-def convolution(sinks, has_prev, x, parts, prev_x, taps, att, logs, rows, halo):
+def convolution(sinks, place, x, parts, prev_x, taps, att, logs, rows, halo):
     n = x.shape[1]
     return pl.pallas_call(
         conv_kernel,
@@ -249,7 +269,7 @@
         compiler_params=settings(20),
         cost_estimate=cost(6),
         name="conv",
-    )(sinks, has_prev, x, *parts, prev_x, taps, att, logs, rows, halo)
+    )(sinks, place, x, *parts, prev_x, taps, att, logs, rows, halo)
 
 
 def body(
@@ -262,17 +282,16 @@
 
 def layer(tokens, norm_gain, attn_weights, conv_weights, conv_taps, sink_logits):
     n, width = tokens.shape
-    mine = jnp.concatenate(attn_weights + conv_weights, axis=1)
-    cut = sum(w.shape[1] for w in attn_weights)
-    sent = jnp.broadcast_to(mine[None], (16,) + mine.shape)
-    own = lax.all_to_all(sent, ("zh", "yh"), 0, 0)
-    own = own.reshape(16 * mine.shape[0], mine.shape[1])
-    prev_tokens = passed_along(tokens[n - 16 :])
-
-    place = jnp.stack([lax.axis_index("zl"), lax.axis_index("yl")]).astype(jnp.int32)
     gain = norm_gain.reshape(1, width)
-    x = norm_classes(place, tokens, gain, 256)
-    prev_x = norm_classes(place, prev_tokens, gain, 16)
+    place = jnp.stack(
+        [lax.axis_index("zl"), lax.axis_index("yl"), jnp.minimum(lax.axis_index(SP), 1)]
+    ).astype(jnp.int32)
+
+    def gathered(weights):
+        mine = jnp.concatenate(weights, axis=1)
+        sent = jnp.broadcast_to(mine[None], (16,) + mine.shape)
+        own = lax.all_to_all(sent, ("zh", "yh"), 0, 0)
+        return own.reshape(16 * mine.shape[0], mine.shape[1])
 
     def classes(block):
         parts = [block]
@@ -280,16 +299,19 @@
             parts.append(shift(block, dz, dy))
         return parts
 
-    parts_a = classes(own[:, :cut])
-    parts_b = classes(own[:, cut:])
-    has_prev = (lax.axis_index(SP) > 0).astype(jnp.int32).reshape(1)
+    own_a = gathered(attn_weights)
+    own_b = gathered(conv_weights)
+    prev_tokens = passed_along(tokens[n - 16 :])
+    x = norm_classes(place, pltpu.with_memory_space_constraint(tokens, pltpu.HBM), gain, 256)
+    x = pltpu.with_memory_space_constraint(x, pltpu.HBM)
+    prev_x = norm_classes(place, prev_tokens, gain, 16)
+    parts_a = classes(own_a)
+    parts_b = classes(own_b)
     last = tail_rows(x, parts_a)
     halo = passed_along(last)
-    att, logs, rows = attention(sink_logits, x, parts_a)
+    att, logs, rows, x_near = attention(sink_logits, x, parts_a)
     return tuple(
-        convolution(
-            sink_logits, has_prev, x, parts_b, prev_x, conv_taps, att, logs, rows, halo
-        )
+        convolution(sink_logits, place, x_near, parts_b, prev_x, conv_taps, att, logs, rows, halo)
     )
 
 

time: 101 us -> 110 us (1.089)
  the two profiles are of different devices: /device:TPU:6 before, /device:TPU:20 now
where the time goes in v1:
time: 110 us; the launch traced here: 109 us
  starting transfers between devices  48.2 us (44%)
  waiting for transfers between devices  33.8 us (31%)
  Pallas kernels  21.3 us (19%)
  local copies, waits for them, and re-layouts  3.19 us (3%)
  other arithmetic  1.63 us (1%)
    all_to_all x2, waiting for transfers between devices, gathered(): own = lax.all_to_all(sent, ('zh', 'yh'), 0, 0)  28.5 us
    all_to_all x2, starting transfers between devices, gathered(): own = lax.all_to_all(sent, ('zh', 'yh'), 0, 0)  22 us
    ppermute x6, starting transfers between devices, shift(): return lax.ppermute(value, SP, pairs)  18.3 us
    pallas_call x2, Pallas kernels, norm_classes(): pl.pallas_call(functools.partial(norm_kernel, block=block), in_specs=[SME...  8.08 us
    ppermute x2, starting transfers between devices, passed_along(): return lax.ppermute(value, SP, [(i, i + 1) for i in range(n - 1)])  7.85 us
    pallas_call x1, Pallas kernels, attention(): pl.pallas_call(attn_kernel, in_specs=[SMEM, HBM] + [VMEM] * 4, out_specs=...  7.07 us
    ppermute x6, waiting for transfers between devices, shift(): return lax.ppermute(value, SP, pairs)  5.3 us
    pallas_call x1, Pallas kernels, convolution(): pl.pallas_call(conv_kernel, in_specs=[SMEM] * 2 + [VMEM] * 11, out_specs=...  4.86 us
  transfers between devices with their start and end apart: 10, of which 3 were waited for; matrix products, arithmetic and copies ran while one was open for 2% of the time, Pallas kernels for 15%

profile of v1, /device:TPU:20, one launch (start us, length us, event | category | flops | bytes accessed | tf_op | source)
XLA Modules:
  0.0 109.0 jit_solution(8933306203776149151)
XLA Ops:
  0.6 0.8 pad_maximum_fusion.1
  1.4 0.8 broadcast_in_dim.4
  2.2 15.9 %all-to-all-start = ((bf16[16,32,384]{2,1,0:T(8,128)(2,1)}), bf16[16,32,384]{2,1,0:T(8,128)(2,1)S(1)}, u32[]{:S(2)}, u32[]{:S(2)}) async-start(bf16[16,32,384]{2,1,0:T(8,128)(2,1)} %broadcast_in_dim.4), calls=%async_computation | async-start | bytes 786432 | tf_op jit(solution)/shard_map/all_to_all | solution.py:293
  18.1 0.7 pad_maximum_fusion
  18.9 15.6 %all-to-all-done = bf16[16,32,384]{2,1,0:T(8,128)(2,1)S(1)} async-done(((bf16[16,32,384]{2,1,0:T(8,128)(2,1)}), bf16[16,32,384]{2,1,0:T(8,128)(2,1)S(1)}, u32[]{:S(2)}, u32[]{:S(2)}) %all-to-all-start) | async-done | bytes 393248 | tf_op jit(solution)/shard_map/all_to_all | solution.py:293
  34.5 0.8 broadcast_in_dim.5
  35.3 6.1 %all-to-all-start.1 = ((bf16[16,32,512]{2,1,0:T(8,128)(2,1)}), bf16[16,32,512]{2,1,0:T(8,128)(2,1)S(1)}, u32[]{:S(2)}, u32[]{:S(2)}) async-start(bf16[16,32,512]{2,1,0:T(8,128)(2,1)} %broadcast_in_dim.5), calls=%async_computation.1 | async-start | bytes 1048576 | tf_op jit(solution)/shard_map/all_to_all | solution.py:293
  41.5 1.9 %collective-permute-start = (bf16[512,384]{1,0:T(8,128)(2,1)S(1)}, bf16[512,384]{1,0:T(8,128)(2,1)S(1)}, u32[]{:S(2)}, u32[]{:S(2)}) collective-permute-start(bf16[512,384]{1,0:T(8,128)(2,1)S(1)} %bitcast.6), channel_id=1, source_target_pairs={{0,8},{8,16},{16,24},{24,32},{32,40},{40,48},{48,56},{56,0},{64,72... | collective-permute-start | bytes 1179656 | tf_op jit(solution)/shard_map/ppermute | solution.py:29
  43.4 3.1 %collective-permute-start.1 = (bf16[512,384]{1,0:T(8,128)(2,1)S(1)}, bf16[512,384]{1,0:T(8,128)(2,1)S(1)}, u32[]{:S(2)}, u32[]{:S(2)}) collective-permute-start(bf16[512,384]{1,0:T(8,128)(2,1)S(1)} %bitcast.7), channel_id=1, source_target_pairs={{0,64},{8,72},{16,80},{24,88},{32,96},{40,104},{48,112},{56,120},{... | collective-permute-start | bytes 1179656 | tf_op jit(solution)/shard_map/ppermute | solution.py:29
  46.5 12.9 %all-to-all-done.1 = bf16[16,32,512]{2,1,0:T(8,128)(2,1)S(1)} async-done(((bf16[16,32,512]{2,1,0:T(8,128)(2,1)}), bf16[16,32,512]{2,1,0:T(8,128)(2,1)S(1)}, u32[]{:S(2)}, u32[]{:S(2)}) %all-to-all-start.1) | async-done | bytes 524320 | tf_op jit(solution)/shard_map/all_to_all | solution.py:293
  59.4 1.9 %collective-permute-start.3 = (bf16[512,512]{1,0:T(8,128)(2,1)S(1)}, bf16[512,512]{1,0:T(8,128)(2,1)S(1)}, u32[]{:S(2)}, u32[]{:S(2)}) collective-permute-start(bf16[512,512]{1,0:T(8,128)(2,1)S(1)} %bitcast.11), channel_id=1, source_target_pairs={{0,8},{8,16},{16,24},{24,32},{32,40},{40,48},{48,56},{56,0},{64,72... | collective-permute-start | bytes 1572872 | tf_op jit(solution)/shard_map/ppermute | solution.py:29
  61.3 3.6 %collective-permute-start.4 = (bf16[512,512]{1,0:T(8,128)(2,1)S(1)}, bf16[512,512]{1,0:T(8,128)(2,1)S(1)}, u32[]{:S(2)}, u32[]{:S(2)}) collective-permute-start(bf16[512,512]{1,0:T(8,128)(2,1)S(1)} %bitcast.12), channel_id=1, source_target_pairs={{0,64},{8,72},{16,80},{24,88},{32,96},{40,104},{48,112},{56,120},{... | collective-permute-start | bytes 1572872 | tf_op jit(solution)/shard_map/ppermute | solution.py:29
  64.9 5.0 %collective-permute-start.5 = (bf16[512,512]{1,0:T(8,128)(2,1)S(1)}, bf16[512,512]{1,0:T(8,128)(2,1)}, u32[]{:S(2)}, u32[]{:S(2)}) collective-permute-start(bf16[512,512]{1,0:T(8,128)(2,1)S(1)} %bitcast.13), channel_id=1, source_target_pairs={{0,504},{8,448},{16,456},{24,464},{32,472},{40,480},{48,488},{56,4... | collective-permute-start | bytes 1572872 | tf_op jit(solution)/shard_map/ppermute | solution.py:29
  69.8 0.0 collective-permute-done.w1
  69.9 2.9 %collective-permute-start.2 = (bf16[512,384]{1,0:T(8,128)(2,1)S(1)}, bf16[512,384]{1,0:T(8,128)(2,1)S(1)}, u32[]{:S(2)}, u32[]{:S(2)}) collective-permute-start(bf16[512,384]{1,0:T(8,128)(2,1)S(1)} %bitcast.8), channel_id=1, source_target_pairs={{0,504},{8,448},{16,456},{24,464},{32,472},{40,480},{48,488},{56,4... | collective-permute-start | bytes 1179656 | tf_op jit(solution)/shard_map/ppermute | solution.py:29
  72.8 0.8 slice.3
  73.6 0.0 collective-permute-done.1.w2
  73.6 2.9 %collective-permute-start.6 = (bf16[16,2048]{1,0:T(8,128)(2,1)S(1)}, bf16[16,2048]{1,0:T(8,128)(2,1)S(1)}, u32[]{:S(2)}, u32[]{:S(2)}) collective-permute-start(bf16[16,2048]{1,0:T(8,128)(2,1)S(1)} %slice.3), channel_id=1, source_target_pairs={{0,8},{8,16},{16,24},{24,32},{32,40},{40,48},{48,56},{56,64},{64,7... | collective-permute-start | bytes 196616 | tf_op jit(solution)/shard_map/ppermute | solution.py:34
  76.5 0.1 pad_add_fusion.place
  76.5 0.0 copy-start.1
  76.5 0.7 copy-done.1
  77.2 6.5 %norm.2.x_hbm = bf16[4,1024,512]{2,1,0:T(8,128)(2,1)} custom-call(s32[3]{0:T(128)S(1)} %pad_add_fusion.place, bf16[1024,2048]{1,0:T(8,128)(2,1)} %tok_hbm.1, f32[1,2048]{1,0:T(1,128)S(1)} %bitcast.15), custom_call_target="tpu_custom_call" | custom-call | flops 19500000 | bytes 1048576 | tf_op jit(solution)/shard_map/norm/pallas_call | solution.py:81
  83.8 0.0 copy-start.3
  83.8 5.3 %collective-permute-done.2.w3 = bf16[512,384]{1,0:T(8,128)(2,1)S(1)} collective-permute-done((bf16[512,384]{1,0:T(8,128)(2,1)S(1)}, bf16[512,384]{1,0:T(8,128)(2,1)S(1)}, u32[]{:S(2)}, u32[]{:S(2)}) %collective-permute-start.2) | collective-permute-done | bytes 393248 | tf_op jit(solution)/shard_map/ppermute | solution.py:29
  89.0 1.3 %tail.1 = bf16[128,128]{1,0:T(8,128)(2,1)S(1)} custom-call(bf16[4,1024,512]{2,1,0:T(8,128)(2,1)} %norm.2.x_hbm, bf16[512,384]{1,0:T(8,128)(2,1)S(1)} %bitcast.9, bf16[512,384]{1,0:T(8,128)(2,1)S(1)} %collective-permute-done.w1, bf16[512,384]{1,0:T(8,128)(2,1)S(1)} %collective-permute-done.1.w2, bf16[512,384]{1,0:T(8,128)(2,1)S(1)} %collective-permute-done.2.w3), custom_call_target="tpu_custom_call" | custom-call | flops 3900000 | bytes 1048576 | tf_op jit(solution)/shard_map/tail/pallas_call | solution.py:149
  90.4 0.0 copy-start.2
  90.4 5.0 %collective-permute-start.7 = (bf16[128,128]{1,0:T(8,128)(2,1)S(1)}, bf16[128,128]{1,0:T(8,128)(2,1)S(1)}, u32[]{:S(2)}, u32[]{:S(2)}) collective-permute-start(bf16[128,128]{1,0:T(8,128)(2,1)S(1)} %tail.1), channel_id=1, source_target_pairs={{0,8},{8,16},{16,24},{24,32},{32,40},{40,48},{48,56},{56,64},{64,7... | collective-permute-start | bytes 98312 | tf_op jit(solution)/shard_map/ppermute | solution.py:34
  95.4 0.0 collective-permute-done.6.tok_hbm
  95.4 1.6 %norm.3.prev_x = bf16[4,16,512]{2,1,0:T(8,128)(2,1)} custom-call(s32[3]{0:T(128)S(1)} %pad_add_fusion.place, bf16[16,2048]{1,0:T(8,128)(2,1)S(1)} %collective-permute-done.6.tok_hbm, f32[1,2048]{1,0:T(1,128)S(1)} %bitcast.16), custom_call_target="tpu_custom_call" | custom-call | flops 3900000 | bytes 1048576 | tf_op jit(solution)/shard_map/norm/pallas_call | solution.py:81
  97.0 0.0 copy-done.3
  97.0 0.0 copy-start
  97.0 7.1 %attn.1 = (f32[1024,256]{1,0:T(8,128)S(1)}, f32[4,1024]{1,0:T(4,128)S(1)}, bf16[1024,384]{1,0:T(8,128)(2,1)S(1)}, bf16[4,1024,512]{2,1,0:T(8,128)(2,1)S(1)}) custom-call(f32[4]{0:T(128)S(1)} %copy-done.3, bf16[4,1024,512]{2,1,0:T(8,128)(2,1)} %norm.2.x_hbm, bf16[512,384]{1,0:T(8,128)(2,1)S(1)} %bitcast.10, bf16[512,384]{1,0:T(8,128)(2,1)S(1)} %collective-permute-done.w1, ...), custom_call_target="tpu_custom_call" | custom-call | flops 31200000 | bytes 1048576 | tf_op jit(solution)/shard_map/attn/pallas_call | solution.py:202
  104.1 0.0 collective-permute-done.7.halo_ref
  104.1 0.0 collective-permute-done.3.w1
  104.1 0.0 collective-permute-done.4.w2
  104.1 0.0 collective-permute-done.5.w3
  104.1 0.0 copy-done.2
  104.1 0.0 copy-done
  104.1 4.9 %conv.1 = (bf16[1024,256]{1,0:T(8,128)(2,1)}, f32[4,1024]{1,0:T(4,128)}) custom-call(f32[4]{0:T(128)S(1)} %copy-done.3, s32[3]{0:T(128)S(1)} %pad_add_fusion.place, bf16[4,1024,512]{2,1,0:T(8,128)(2,1)S(1)} %get-tuple-element.6.x_ref, bf16[512,512]{1,0:T(8,128)(2,1)S(1)} %bitcast.14, bf16[512,512]{1,0:T(8,128)(2,1)S(1)} %collective-permute-done.3.w1, ...), custom_call_target="tpu_custom_call" | custom-call | flops 23400000 | bytes 1048576 | tf_op jit(solution)/shard_map/conv/pallas_call | solution.py:260
Async XLA Ops:
  2.2 32.3 %all-to-all-start = ((bf16[16,32,384]{2,1,0:T(8,128)(2,1)}), bf16[16,32,384]{2,1,0:T(8,128)(2,1)S(1)}, u32[]{:S(2)}, u32[]{:S(2)}) async-start(bf16[16,32,384]{2,1,0:T(8,128)(2,1)} %broadcast_in_dim.4), calls=%async_computation | async-start | bytes 786432 | tf_op jit(solution)/shard_map/all_to_all | solution.py:293
  35.3 24.1 %all-to-all-start.1 = ((bf16[16,32,512]{2,1,0:T(8,128)(2,1)}), bf16[16,32,512]{2,1,0:T(8,128)(2,1)S(1)}, u32[]{:S(2)}, u32[]{:S(2)}) async-start(bf16[16,32,512]{2,1,0:T(8,128)(2,1)} %broadcast_in_dim.5), calls=%async_computation.1 | async-start | bytes 1048576 | tf_op jit(solution)/shard_map/all_to_all | solution.py:293
  41.5 28.4 %collective-permute-start = (bf16[512,384]{1,0:T(8,128)(2,1)S(1)}, bf16[512,384]{1,0:T(8,128)(2,1)S(1)}, u32[]{:S(2)}, u32[]{:S(2)}) collective-permute-start(bf16[512,384]{1,0:T(8,128)(2,1)S(1)} %bitcast.6), channel_id=1, source_target_pairs={{0,8},{8,16},{16,24},{24,32},{32,40},{40,48},{48,56},{56,0},{64,72... | collective-permute-start | bytes 1179656 | tf_op jit(solution)/shard_map/ppermute | solution.py:29
  43.4 30.2 %collective-permute-start.1 = (bf16[512,384]{1,0:T(8,128)(2,1)S(1)}, bf16[512,384]{1,0:T(8,128)(2,1)S(1)}, u32[]{:S(2)}, u32[]{:S(2)}) collective-permute-start(bf16[512,384]{1,0:T(8,128)(2,1)S(1)} %bitcast.7), channel_id=1, source_target_pairs={{0,64},{8,72},{16,80},{24,88},{32,96},{40,104},{48,112},{56,120},{... | collective-permute-start | bytes 1179656 | tf_op jit(solution)/shard_map/ppermute | solution.py:29
  59.4 44.7 %collective-permute-start.3 = (bf16[512,512]{1,0:T(8,128)(2,1)S(1)}, bf16[512,512]{1,0:T(8,128)(2,1)S(1)}, u32[]{:S(2)}, u32[]{:S(2)}) collective-permute-start(bf16[512,512]{1,0:T(8,128)(2,1)S(1)} %bitcast.11), channel_id=1, source_target_pairs={{0,8},{8,16},{16,24},{24,32},{32,40},{40,48},{48,56},{56,0},{64,72... | collective-permute-start | bytes 1572872 | tf_op jit(solution)/shard_map/ppermute | solution.py:29
  61.3 42.8 %collective-permute-start.4 = (bf16[512,512]{1,0:T(8,128)(2,1)S(1)}, bf16[512,512]{1,0:T(8,128)(2,1)S(1)}, u32[]{:S(2)}, u32[]{:S(2)}) collective-permute-start(bf16[512,512]{1,0:T(8,128)(2,1)S(1)} %bitcast.12), channel_id=1, source_target_pairs={{0,64},{8,72},{16,80},{24,88},{32,96},{40,104},{48,112},{56,120},{... | collective-permute-start | bytes 1572872 | tf_op jit(solution)/shard_map/ppermute | solution.py:29
  64.9 39.2 %collective-permute-start.5 = (bf16[512,512]{1,0:T(8,128)(2,1)S(1)}, bf16[512,512]{1,0:T(8,128)(2,1)}, u32[]{:S(2)}, u32[]{:S(2)}) collective-permute-start(bf16[512,512]{1,0:T(8,128)(2,1)S(1)} %bitcast.13), channel_id=1, source_target_pairs={{0,504},{8,448},{16,456},{24,464},{32,472},{40,480},{48,488},{56,4... | collective-permute-start | bytes 1572872 | tf_op jit(solution)/shard_map/ppermute | solution.py:29
  69.9 19.2 %collective-permute-start.2 = (bf16[512,384]{1,0:T(8,128)(2,1)S(1)}, bf16[512,384]{1,0:T(8,128)(2,1)S(1)}, u32[]{:S(2)}, u32[]{:S(2)}) collective-permute-start(bf16[512,384]{1,0:T(8,128)(2,1)S(1)} %bitcast.8), channel_id=1, source_target_pairs={{0,504},{8,448},{16,456},{24,464},{32,472},{40,480},{48,488},{56,4... | collective-permute-start | bytes 1179656 | tf_op jit(solution)/shard_map/ppermute | solution.py:29
  73.6 21.8 %collective-permute-start.6 = (bf16[16,2048]{1,0:T(8,128)(2,1)S(1)}, bf16[16,2048]{1,0:T(8,128)(2,1)S(1)}, u32[]{:S(2)}, u32[]{:S(2)}) collective-permute-start(bf16[16,2048]{1,0:T(8,128)(2,1)S(1)} %slice.3), channel_id=1, source_target_pairs={{0,8},{8,16},{16,24},{24,32},{32,40},{40,48},{48,56},{56,64},{64,7... | collective-permute-start | bytes 196616 | tf_op jit(solution)/shard_map/ppermute | solution.py:34
  76.5 0.7 copy-start.1
  83.8 13.2 %copy-start.3 = (f32[4]{0:T(128)S(1)}, f32[4]{0:T(128)}, u32[]{:S(2)}) copy-start(f32[4]{0:T(128)} %sinks.3) | copy-start | bytes 52
  90.4 13.7 %copy-start.2 = (bf16[3,256]{1,0:T(4,128)(2,1)S(1)}, bf16[3,256]{1,0:T(4,128)(2,1)}, u32[]{:S(2)}) copy-start(bf16[3,256]{1,0:T(4,128)(2,1)} %taps_ref.1) | copy-start | bytes 4612
  90.4 13.7 %collective-permute-start.7 = (bf16[128,128]{1,0:T(8,128)(2,1)S(1)}, bf16[128,128]{1,0:T(8,128)(2,1)S(1)}, u32[]{:S(2)}, u32[]{:S(2)}) collective-permute-start(bf16[128,128]{1,0:T(8,128)(2,1)S(1)} %tail.1), channel_id=1, source_target_pairs={{0,8},{8,16},{16,24},{24,32},{32,40},{40,48},{48,56},{56,64},{64,7... | collective-permute-start | bytes 98312 | tf_op jit(solution)/shard_map/ppermute | solution.py:34
  97.0 7.1 %copy-start = (bf16[4,16,512]{2,1,0:T(8,128)(2,1)S(1)}, bf16[4,16,512]{2,1,0:T(8,128)(2,1)}, u32[]{:S(2)}) copy-start(bf16[4,16,512]{2,1,0:T(8,128)(2,1)} %norm.3.prev_x) | copy-start | bytes 196612

commit v2 on v0

--- a/solution.py
+++ b/solution.py
@@ -14,6 +14,10 @@
 COLS = ("fs", "tp")
 SIDE = 8
 LANES = 128
+RIM = 16
+VMEM = pl.BlockSpec(memory_space=pltpu.VMEM)
+SMEM = pl.BlockSpec(memory_space=pltpu.SMEM)
+HBM = pl.BlockSpec(memory_space=pltpu.HBM)
 
 
 def shift(value, dz, dy):
@@ -41,23 +45,32 @@
     return lax.dot_general(a, b, (dims, ((), ())), preferred_element_type=jnp.float32)
 
 
-def norm_kernel(place, tok_ref, gain_ref, out_ref):
-    widened = tok_ref[...].astype(jnp.float32)
-    scale = lax.rsqrt(jnp.mean(widened * widened, axis=-1, keepdims=True) + EPS)
-    normed = (widened * scale * gain_ref[...]).astype(jnp.bfloat16)
+def column_sort():
     span = 2 * LANES
     row = lax.broadcasted_iota(jnp.int32, (span, span), 0)
     col = lax.broadcasted_iota(jnp.int32, (span, span), 1)
     target = ((row >> 5) & 1) * LANES + (row >> 6) * 32 + (row & 31)
-    swap = (target == col).astype(jnp.bfloat16)
+    return (target == col).astype(jnp.bfloat16)
+
+
+def norm_into(place, rows, gain, swap, out_ref):
+    widened = rows.astype(jnp.float32)
+    scale = lax.rsqrt(jnp.mean(widened * widened, axis=-1, keepdims=True) + EPS)
+    normed = (widened * scale * gain).astype(jnp.bfloat16)
+    span = 2 * LANES
     for zh in range(4):
         for zl in range(2):
             at = (zh * 2 + zl) * span
             sorted_cols = dot(normed[:, at : at + span], swap).astype(jnp.bfloat16)
             for yl in range(2):
-                out_ref[(place[0] ^ zl) * 2 + (place[1] ^ yl), :, zh * LANES : (zh + 1) * LANES] = (
-                    sorted_cols[:, yl * LANES : (yl + 1) * LANES]
-                )
+                into = (place[0] ^ zl) * 2 + (place[1] ^ yl)
+                out_ref[into, :, zh * LANES : (zh + 1) * LANES] = sorted_cols[
+                    :, yl * LANES : (yl + 1) * LANES
+                ]
+
+
+def norm_kernel(place, tok_ref, gain_ref, out_ref):
+    norm_into(place, tok_ref[...], gain_ref[...], column_sort(), out_ref)
 
 
 def norm_classes(place, rows, gain, block):
@@ -75,7 +88,7 @@
         ),
         out_shape=jax.ShapeDtypeStruct((4, n, width // 4), jnp.bfloat16),
         compiler_params=settings(14),
-        cost_estimate=cost(5 if n > 16 else 1),
+        cost_estimate=cost(5),
         name="norm",
     )(place, rows, gain)
 
@@ -125,27 +138,33 @@
     return jnp.concatenate(outs, axis=1), jnp.concatenate(logs, axis=0)
 
 
-def tail_kernel(x_ref, w0, w1, w2, w3, out_ref):
+def tail_kernel(x_ref, w0, w1, w2, w3, rim_ref, out_ref):
     acc = dot(x_ref[0], w0[...])
     for c, w in ((1, w1), (2, w2), (3, w3)):
         acc = acc + dot(x_ref[c], w[...])
-    out_ref[...] = acc.astype(jnp.bfloat16)
-
-
-def tail_rows(x, parts):
+    out_ref[:WINDOW, :] = acc.astype(jnp.bfloat16)
+    for k in range(rim_ref.shape[1] // LANES):
+        out_ref[WINDOW + k * RIM : WINDOW + (k + 1) * RIM, :] = rim_ref[
+            :, k * LANES : (k + 1) * LANES
+        ]
+
+
+def tail_rows(x, parts, rim):
     n, depth = x.shape[1], x.shape[2]
     last = n // WINDOW - 1
+    rows = WINDOW + rim.shape[1] // LANES * RIM
     return pl.pallas_call(
         tail_kernel,
         grid=(1,),
         in_specs=[pl.BlockSpec((4, WINDOW, depth), lambda i: (0, last, 0))]
-        + [pl.BlockSpec((depth, LANES), lambda i: (0, 0))] * 4,
-        out_specs=pl.BlockSpec((WINDOW, LANES), lambda i: (0, 0)),
-        out_shape=jax.ShapeDtypeStruct((WINDOW, LANES), jnp.bfloat16),
+        + [pl.BlockSpec((depth, LANES), lambda i: (0, 0))] * 4
+        + [pl.BlockSpec(rim.shape, lambda i: (0, 0))],
+        out_specs=pl.BlockSpec((rows, LANES), lambda i: (0, 0)),
+        out_shape=jax.ShapeDtypeStruct((rows, LANES), jnp.bfloat16),
         compiler_params=settings(6),
         cost_estimate=cost(1),
         name="tail",
-    )(x, *parts)
+    )(x, *parts, rim)
 
 
 def attn_kernel(sinks, x_ref, w0, w1, w2, w3, att_ref, log_ref, rows_ref):
@@ -172,10 +191,6 @@
         )
         att_ref[here : here + WINDOW, :] = att
         log_ref[:, here : here + WINDOW] = logs
-
-
-VMEM = pl.BlockSpec(memory_space=pltpu.VMEM)
-SMEM = pl.BlockSpec(memory_space=pltpu.SMEM)
 
 
 def attention(sinks, x, parts):
@@ -197,23 +212,28 @@
 
 
 def conv_kernel(
-    sinks, has_prev, x_ref, w0, w1, w2, w3, prev_x, taps_ref, att_ref, log_ref, rows_ref, halo_ref,
-    out_ref, log_out, pad_ref,
+    sinks, place, x_ref, w0, w1, w2, w3, gain_ref, taps_ref, att_ref, log_ref, rows_ref, halo_ref,
+    out_ref, log_out, pad_ref, prev_x,
 ):
     n = x_ref.shape[1]
     width = 2 * LANES
     step = 256
     parts = (w0, w1, w2, w3)
+    rim = [
+        halo_ref[WINDOW + k * RIM : WINDOW + (k + 1) * RIM, :]
+        for k in range(gain_ref.shape[1] // LANES)
+    ]
+    norm_into(place, jnp.concatenate(rim, axis=1), gain_ref[...], column_sort(), prev_x)
     acc = dot(prev_x[0], w0[:, :width])
     for c in range(1, 4):
         acc = acc + dot(prev_x[c], parts[c][:, :width])
     pad_ref[:8, :] = acc[8:16].astype(jnp.bfloat16).astype(jnp.float32)
     att0, log0 = attend_block(
         rows_ref[:WINDOW, LANES:],
-        halo_ref[...],
+        halo_ref[:WINDOW, :],
         rows_ref[:WINDOW, :LANES],
         [sinks[h] for h in range(4)],
-        has_prev[0] > 0,
+        place[2] > 0,
     )
     log_out[...] = log_ref[...]
     log_out[:, :WINDOW] = log0
@@ -235,7 +255,7 @@
         out_ref[at : at + step, :] = (first + gated).astype(jnp.bfloat16)
 
 
-def convolution(sinks, has_prev, x, parts, prev_x, taps, att, logs, rows, halo):
+def convolution(sinks, place, x, parts, gain, taps, att, logs, rows, halo):
     n = x.shape[1]
     return pl.pallas_call(
         conv_kernel,
@@ -245,11 +265,14 @@
             jax.ShapeDtypeStruct((n, 2 * LANES), jnp.bfloat16),
             jax.ShapeDtypeStruct((4, n), jnp.float32),
         ],
-        scratch_shapes=[pltpu.VMEM((n + 8, 2 * LANES), jnp.float32)],
+        scratch_shapes=[
+            pltpu.VMEM((n + 8, 2 * LANES), jnp.float32),
+            pltpu.VMEM((4, RIM, x.shape[2]), jnp.bfloat16),
+        ],
         compiler_params=settings(20),
         cost_estimate=cost(6),
         name="conv",
-    )(sinks, has_prev, x, *parts, prev_x, taps, att, logs, rows, halo)
+    )(sinks, place, x, *parts, gain, taps, att, logs, rows, halo)
 
 
 def body(
@@ -262,33 +285,32 @@
 
 def layer(tokens, norm_gain, attn_weights, conv_weights, conv_taps, sink_logits):
     n, width = tokens.shape
+    gain = norm_gain.reshape(1, width)
+    place = jnp.stack(
+        [lax.axis_index("zl"), lax.axis_index("yl"), jnp.minimum(lax.axis_index(SP), 1)]
+    ).astype(jnp.int32)
+
     mine = jnp.concatenate(attn_weights + conv_weights, axis=1)
     cut = sum(w.shape[1] for w in attn_weights)
     sent = jnp.broadcast_to(mine[None], (16,) + mine.shape)
     own = lax.all_to_all(sent, ("zh", "yh"), 0, 0)
     own = own.reshape(16 * mine.shape[0], mine.shape[1])
-    prev_tokens = passed_along(tokens[n - 16 :])
-
-    place = jnp.stack([lax.axis_index("zl"), lax.axis_index("yl")]).astype(jnp.int32)
-    gain = norm_gain.reshape(1, width)
-    x = norm_classes(place, tokens, gain, 256)
-    prev_x = norm_classes(place, prev_tokens, gain, 16)
 
     def classes(block):
-        parts = [block]
-        for dz, dy in ((0, 1), (1, 0), (-1, -1)):
-            parts.append(shift(block, dz, dy))
-        return parts
+        corner = shift(block, -1, -1)
+        along_y = shift(block, 0, 1)
+        along_z = shift(block, 1, 0)
+        return [block, along_y, along_z, corner]
 
     parts_a = classes(own[:, :cut])
     parts_b = classes(own[:, cut:])
-    has_prev = (lax.axis_index(SP) > 0).astype(jnp.int32).reshape(1)
-    last = tail_rows(x, parts_a)
+    x = norm_classes(place, pltpu.with_memory_space_constraint(tokens, pltpu.HBM), gain, 256)
+    last = tail_rows(x, parts_a, tokens[n - RIM :])
     halo = passed_along(last)
     att, logs, rows = attention(sink_logits, x, parts_a)
     return tuple(
         convolution(
-            sink_logits, has_prev, x, parts_b, prev_x, conv_taps, att, logs, rows, halo
+            sink_logits, place, x, parts_b, gain, conv_taps, att, logs, rows, halo
         )
     )
 

time: 101 us -> 94 us (0.931)
  the two profiles are of different devices: /device:TPU:6 before, /device:TPU:30 now
where the time goes in v2:
time: 94 us; the launch traced here: 93.5 us
  blocking collectives  41 us (44%)
  starting transfers between devices  25.9 us (28%)
  Pallas kernels  16.4 us (17%)
  waiting for transfers between devices  7.47 us (8%)
  local copies, waits for them, and re-layouts  1.89 us (2%)
    all_to_all x1, blocking collectives, layer(): own = lax.all_to_all(sent, ('zh', 'yh'), 0, 0)  41 us
    ppermute x6, starting transfers between devices, shift(): return lax.ppermute(value, SP, pairs)  22.3 us
    ppermute x6, waiting for transfers between devices, shift(): return lax.ppermute(value, SP, pairs)  7.47 us
    pallas_call x1, Pallas kernels, norm_classes(): pl.pallas_call(norm_kernel, grid_spec=pltpu.PrefetchScalarGridSpec(num_sc...  5.69 us
    pallas_call x1, Pallas kernels, attention(): pl.pallas_call(attn_kernel, in_specs=[SMEM] + [VMEM] * 5, out_specs=[VMEM...  5.33 us
    pallas_call x1, Pallas kernels, convolution(): pl.pallas_call(conv_kernel, in_specs=[SMEM] * 2 + [VMEM] * 11, out_specs=...  4.99 us
    ppermute x1, starting transfers between devices, passed_along(): return lax.ppermute(value, SP, [(i, i + 1) for i in range(n - 1)])  3.59 us
  transfers between devices with their start and end apart: 7, of which 2 were waited for; matrix products, arithmetic and copies ran while one was open for 1% of the time, Pallas kernels for 12%

profile of v2, /device:TPU:30, one launch (start us, length us, event | category | flops | bytes accessed | tf_op | source)
XLA Modules:
  0.0 93.5 jit_solution(16765590814302175749)
XLA Ops:
  0.6 0.0 copy-start
  0.6 0.9 concatenate.3
  1.5 0.1 broadcast_in_dim.2
  1.6 41.0 %all_to_all.5 = bf16[16,32,896]{2,1,0:T(8,128)(2,1)S(1)} all-to-all(bf16[16,32,896]{2,1,0:T(8,128)(2,1)S(1)} %broadcast_in_dim.2), channel_id=1, replica_groups=mesh['zh'=4,'zl'=2,'yh'=4,'yl'=2,'fs'=4,'tp'=2] {'zh','yh'}, dimensions={0} | all-to-all | bytes 1835008 | tf_op jit(solution)/shard_map/all_to_all | solution.py:296
  42.6 5.8 %collective-permute-start.3 = (bf16[512,384]{1,0:T(8,128)(2,1)S(1)}, bf16[512,384]{1,0:T(8,128)(2,1)S(1)}, u32[]{:S(2)}, u32[]{:S(2)}) collective-permute-start(bf16[512,384]{1,0:T(8,128)(2,1)S(1)} %slice.13.w0), channel_id=1, source_target_pairs={{0,8},{8,16},{16,24},{24,32},{32,40},{40,48},{48,56},{56,0},{64,72... | collective-permute-start | bytes 1179656 | tf_op jit(solution)/shard_map/ppermute | solution.py:28
  48.5 1.9 %collective-permute-start = (bf16[512,512]{1,0:T(8,128)(2,1)S(1)}, bf16[512,512]{1,0:T(8,128)(2,1)S(1)}, u32[]{:S(2)}, u32[]{:S(2)}) collective-permute-start(bf16[512,512]{1,0:T(8,128)(2,1)S(1)} %slice.12.w0), channel_id=1, source_target_pairs={{0,8},{8,16},{16,24},{24,32},{32,40},{40,48},{48,56},{56,0},{64,72... | collective-permute-start | bytes 1572872 | tf_op jit(solution)/shard_map/ppermute | solution.py:28
  50.4 3.7 %collective-permute-start.1 = (bf16[512,512]{1,0:T(8,128)(2,1)S(1)}, bf16[512,512]{1,0:T(8,128)(2,1)S(1)}, u32[]{:S(2)}, u32[]{:S(2)}) collective-permute-start(bf16[512,512]{1,0:T(8,128)(2,1)S(1)} %slice.12.w0), channel_id=1, source_target_pairs={{0,64},{8,72},{16,80},{24,88},{32,96},{40,104},{48,112},{56,120},{... | collective-permute-start | bytes 1572872 | tf_op jit(solution)/shard_map/ppermute | solution.py:28
  54.1 4.8 %collective-permute-start.2 = (bf16[512,512]{1,0:T(8,128)(2,1)S(1)}, bf16[512,512]{1,0:T(8,128)(2,1)}, u32[]{:S(2)}, u32[]{:S(2)}) collective-permute-start(bf16[512,512]{1,0:T(8,128)(2,1)S(1)} %slice.12.w0), channel_id=1, source_target_pairs={{0,504},{8,448},{16,456},{24,464},{32,472},{40,480},{48,488},{56,4... | collective-permute-start | bytes 1572872 | tf_op jit(solution)/shard_map/ppermute | solution.py:28
  58.9 2.5 %collective-permute-start.4 = (bf16[512,384]{1,0:T(8,128)(2,1)S(1)}, bf16[512,384]{1,0:T(8,128)(2,1)S(1)}, u32[]{:S(2)}, u32[]{:S(2)}) collective-permute-start(bf16[512,384]{1,0:T(8,128)(2,1)S(1)} %slice.13.w0), channel_id=1, source_target_pairs={{0,64},{8,72},{16,80},{24,88},{32,96},{40,104},{48,112},{56,120},{... | collective-permute-start | bytes 1179656 | tf_op jit(solution)/shard_map/ppermute | solution.py:28
  61.4 0.0 collective-permute-done.3.w1
  61.4 3.6 %collective-permute-start.5 = (bf16[512,384]{1,0:T(8,128)(2,1)S(1)}, bf16[512,384]{1,0:T(8,128)(2,1)S(1)}, u32[]{:S(2)}, u32[]{:S(2)}) collective-permute-start(bf16[512,384]{1,0:T(8,128)(2,1)S(1)} %slice.13.w0), channel_id=1, source_target_pairs={{0,504},{8,448},{16,456},{24,464},{32,472},{40,480},{48,488},{56,4... | collective-permute-start | bytes 1179656 | tf_op jit(solution)/shard_map/ppermute | solution.py:28
  65.0 0.8 slice.11.rim_ref
  65.9 0.1 pad_add_fusion.place
  65.9 0.0 copy-done
  65.9 5.7 %norm.1.x_ref = bf16[4,1024,512]{2,1,0:T(8,128)(2,1)S(1)} custom-call(s32[3]{0:T(128)S(1)} %pad_add_fusion.place, bf16[1024,2048]{1,0:T(8,128)(2,1)} %tok_ref.1, f32[1,2048]{1,0:T(1,128)S(1)} %bitcast.5), custom_call_target="tpu_custom_call" | custom-call | flops 19500000 | bytes 1048576 | tf_op jit(solution)/shard_map/norm/pallas_call | solution.py:78
  71.7 0.0 copy-start.1
  71.7 3.1 %collective-permute-done.4.w2 = bf16[512,384]{1,0:T(8,128)(2,1)S(1)} collective-permute-done((bf16[512,384]{1,0:T(8,128)(2,1)S(1)}, bf16[512,384]{1,0:T(8,128)(2,1)S(1)}, u32[]{:S(2)}, u32[]{:S(2)}) %collective-permute-start.4) | collective-permute-done | bytes 393248 | tf_op jit(solution)/shard_map/ppermute | solution.py:28
  74.7 4.4 %collective-permute-done.5.w3 = bf16[512,384]{1,0:T(8,128)(2,1)S(1)} collective-permute-done((bf16[512,384]{1,0:T(8,128)(2,1)S(1)}, bf16[512,384]{1,0:T(8,128)(2,1)S(1)}, u32[]{:S(2)}, u32[]{:S(2)}) %collective-permute-start.5) | collective-permute-done | bytes 393248 | tf_op jit(solution)/shard_map/ppermute | solution.py:28
  79.1 0.4 tail.1
  79.5 0.0 copy-start.2
  79.5 3.6 %collective-permute-start.6 = (bf16[384,128]{1,0:T(8,128)(2,1)S(1)}, bf16[384,128]{1,0:T(8,128)(2,1)S(1)}, u32[]{:S(2)}, u32[]{:S(2)}) collective-permute-start(bf16[384,128]{1,0:T(8,128)(2,1)S(1)} %tail.1), channel_id=1, source_target_pairs={{0,8},{8,16},{16,24},{24,32},{32,40},{40,48},{48,56},{56,64},{64,7... | collective-permute-start | bytes 294920 | tf_op jit(solution)/shard_map/ppermute | solution.py:33
  83.1 0.0 copy-done.1
  83.1 5.3 %attn.1 = (f32[1024,256]{1,0:T(8,128)S(1)}, f32[4,1024]{1,0:T(4,128)S(1)}, bf16[1024,384]{1,0:T(8,128)(2,1)S(1)}) custom-call(f32[4]{0:T(128)S(1)} %copy-done.1, bf16[4,1024,512]{2,1,0:T(8,128)(2,1)S(1)} %norm.1.x_ref, bf16[512,384]{1,0:T(8,128)(2,1)S(1)} %slice.13.w0, bf16[512,384]{1,0:T(8,128)(2,1)S(1)} %collective-permute-done.3.w1, ...), custom_call_target="tpu_custom_call" | custom-call | flops 31200000 | bytes 1048576 | tf_op jit(solution)/shard_map/attn/pallas_call | solution.py:199
  88.4 0.0 collective-permute-done.6.halo_ref
  88.5 0.0 collective-permute-done.w1
  88.5 0.0 collective-permute-done.1.w2
  88.5 0.0 collective-permute-done.2.w3
  88.5 0.0 copy-done.2
  88.5 5.0 %conv.1 = (bf16[1024,256]{1,0:T(8,128)(2,1)}, f32[4,1024]{1,0:T(4,128)}) custom-call(f32[4]{0:T(128)S(1)} %copy-done.1, s32[3]{0:T(128)S(1)} %pad_add_fusion.place, bf16[4,1024,512]{2,1,0:T(8,128)(2,1)S(1)} %norm.1.x_ref, bf16[512,512]{1,0:T(8,128)(2,1)S(1)} %slice.12.w0, bf16[512,512]{1,0:T(8,128)(2,1)S(1)} %collective-permute-done.w1, ...), custom_call_target="tpu_custom_call" | custom-call | flops 23400000 | bytes 1048576 | tf_op jit(solution)/shard_map/conv/pallas_call | solution.py:260
  (2 shorter events, 0.1 us)
Async XLA Ops:
  0.6 65.3 %copy-start = (f32[2048]{0:T(1024)S(1)}, f32[2048]{0:T(1024)}, u32[]{:S(2)}) copy-start(f32[2048]{0:T(1024)} %param.10) | copy-start | bytes 24580
  42.6 18.8 %collective-permute-start.3 = (bf16[512,384]{1,0:T(8,128)(2,1)S(1)}, bf16[512,384]{1,0:T(8,128)(2,1)S(1)}, u32[]{:S(2)}, u32[]{:S(2)}) collective-permute-start(bf16[512,384]{1,0:T(8,128)(2,1)S(1)} %slice.13.w0), channel_id=1, source_target_pairs={{0,8},{8,16},{16,24},{24,32},{32,40},{40,48},{48,56},{56,0},{64,72... | collective-permute-start | bytes 1179656 | tf_op jit(solution)/shard_map/ppermute | solution.py:28
  48.5 40.0 %collective-permute-start = (bf16[512,512]{1,0:T(8,128)(2,1)S(1)}, bf16[512,512]{1,0:T(8,128)(2,1)S(1)}, u32[]{:S(2)}, u32[]{:S(2)}) collective-permute-start(bf16[512,512]{1,0:T(8,128)(2,1)S(1)} %slice.12.w0), channel_id=1, source_target_pairs={{0,8},{8,16},{16,24},{24,32},{32,40},{40,48},{48,56},{56,0},{64,72... | collective-permute-start | bytes 1572872 | tf_op jit(solution)/shard_map/ppermute | solution.py:28
  50.4 38.1 %collective-permute-start.1 = (bf16[512,512]{1,0:T(8,128)(2,1)S(1)}, bf16[512,512]{1,0:T(8,128)(2,1)S(1)}, u32[]{:S(2)}, u32[]{:S(2)}) collective-permute-start(bf16[512,512]{1,0:T(8,128)(2,1)S(1)} %slice.12.w0), channel_id=1, source_target_pairs={{0,64},{8,72},{16,80},{24,88},{32,96},{40,104},{48,112},{56,120},{... | collective-permute-start | bytes 1572872 | tf_op jit(solution)/shard_map/ppermute | solution.py:28
  54.1 34.4 %collective-permute-start.2 = (bf16[512,512]{1,0:T(8,128)(2,1)S(1)}, bf16[512,512]{1,0:T(8,128)(2,1)}, u32[]{:S(2)}, u32[]{:S(2)}) collective-permute-start(bf16[512,512]{1,0:T(8,128)(2,1)S(1)} %slice.12.w0), channel_id=1, source_target_pairs={{0,504},{8,448},{16,456},{24,464},{32,472},{40,480},{48,488},{56,4... | collective-permute-start | bytes 1572872 | tf_op jit(solution)/shard_map/ppermute | solution.py:28
  58.9 15.8 %collective-permute-start.4 = (bf16[512,384]{1,0:T(8,128)(2,1)S(1)}, bf16[512,384]{1,0:T(8,128)(2,1)S(1)}, u32[]{:S(2)}, u32[]{:S(2)}) collective-permute-start(bf16[512,384]{1,0:T(8,128)(2,1)S(1)} %slice.13.w0), channel_id=1, source_target_pairs={{0,64},{8,72},{16,80},{24,88},{32,96},{40,104},{48,112},{56,120},{... | collective-permute-start | bytes 1179656 | tf_op jit(solution)/shard_map/ppermute | solution.py:28
  61.4 17.7 %collective-permute-start.5 = (bf16[512,384]{1,0:T(8,128)(2,1)S(1)}, bf16[512,384]{1,0:T(8,128)(2,1)S(1)}, u32[]{:S(2)}, u32[]{:S(2)}) collective-permute-start(bf16[512,384]{1,0:T(8,128)(2,1)S(1)} %slice.13.w0), channel_id=1, source_target_pairs={{0,504},{8,448},{16,456},{24,464},{32,472},{40,480},{48,488},{56,4... | collective-permute-start | bytes 1179656 | tf_op jit(solution)/shard_map/ppermute | solution.py:28
  71.7 11.5 %copy-start.1 = (f32[4]{0:T(128)S(1)}, f32[4]{0:T(128)}, u32[]{:S(2)}) copy-start(f32[4]{0:T(128)} %sinks.3) | copy-start | bytes 52
  79.5 9.0 %copy-start.2 = (bf16[3,256]{1,0:T(4,128)(2,1)S(1)}, bf16[3,256]{1,0:T(4,128)(2,1)}, u32[]{:S(2)}) copy-start(bf16[3,256]{1,0:T(4,128)(2,1)} %taps_ref.1) | copy-start | bytes 4612
  79.5 8.9 %collective-permute-start.6 = (bf16[384,128]{1,0:T(8,128)(2,1)S(1)}, bf16[384,128]{1,0:T(8,128)(2,1)S(1)}, u32[]{:S(2)}, u32[]{:S(2)}) collective-permute-start(bf16[384,128]{1,0:T(8,128)(2,1)S(1)} %tail.1), channel_id=1, source_target_pairs={{0,8},{8,16},{16,24},{24,32},{32,40},{40,48},{48,56},{56,64},{64,7... | collective-permute-start | bytes 294920 | tf_op jit(solution)/shard_map/ppermute | solution.py:33

commit v3 on v2

--- a/solution.py
+++ b/solution.py
@@ -1,3 +1,5 @@
+import functools
+
 import jax
 import jax.numpy as jnp
 from jax import lax
@@ -24,8 +26,10 @@
     pairs = []
     for z in range(SIDE):
         for y in range(SIDE):
-            pairs.append((z * SIDE + y, (z + dz) % SIDE * SIDE + (y + dy) % SIDE))
-    return lax.ppermute(value, SP, pairs)
+            for core, sign in enumerate((1, -1)):
+                to = (z + sign * dz) % SIDE * SIDE + (y + sign * dy) % SIDE
+                pairs.append(((z * SIDE + y) * 2 + core, to * 2 + core))
+    return lax.ppermute(value, SP + ("tp",), pairs)
 
 
 def passed_along(value):
@@ -69,24 +73,28 @@
                 ]
 
 
-def norm_kernel(place, tok_ref, gain_ref, out_ref):
-    norm_into(place, tok_ref[...], gain_ref[...], column_sort(), out_ref)
+def norm_kernel(place, tok_hbm, gain_ref, out_hbm, *, block):
+    n, width = tok_hbm.shape
+    swap = column_sort()
+
+    def step(tok_ref, out_ref):
+        norm_into(place, tok_ref[...], gain_ref[...], swap, out_ref)
+
+    pltpu.emit_pipeline(
+        step,
+        grid=(n // block,),
+        in_specs=[pl.BlockSpec((block, width), lambda i: (i, 0))],
+        out_specs=[pl.BlockSpec((4, block, width // 4), lambda i: (0, i, 0))],
+    )(tok_hbm, out_hbm)
 
 
 def norm_classes(place, rows, gain, block):
     n, width = rows.shape
     return pl.pallas_call(
-        norm_kernel,
-        grid_spec=pltpu.PrefetchScalarGridSpec(
-            num_scalar_prefetch=1,
-            grid=(n // block,),
-            in_specs=[
-                pl.BlockSpec((block, width), lambda i, p: (i, 0)),
-                pl.BlockSpec((1, width), lambda i, p: (0, 0)),
-            ],
-            out_specs=pl.BlockSpec((4, block, width // 4), lambda i, p: (0, i, 0)),
-        ),
-        out_shape=jax.ShapeDtypeStruct((4, n, width // 4), jnp.bfloat16),
+        functools.partial(norm_kernel, block=block),
+        in_specs=[SMEM, HBM, VMEM],
+        out_specs=HBM,
+        out_shape=pltpu.HBM((4, n, width // 4), jnp.bfloat16),
         compiler_params=settings(14),
         cost_estimate=cost(5),
         name="norm",
@@ -138,77 +146,71 @@
     return jnp.concatenate(outs, axis=1), jnp.concatenate(logs, axis=0)
 
 
-def tail_kernel(x_ref, w0, w1, w2, w3, rim_ref, out_ref):
-    acc = dot(x_ref[0], w0[...])
-    for c, w in ((1, w1), (2, w2), (3, w3)):
-        acc = acc + dot(x_ref[c], w[...])
-    out_ref[:WINDOW, :] = acc.astype(jnp.bfloat16)
-    for k in range(rim_ref.shape[1] // LANES):
-        out_ref[WINDOW + k * RIM : WINDOW + (k + 1) * RIM, :] = rim_ref[
-            :, k * LANES : (k + 1) * LANES
-        ]
-
-
-def tail_rows(x, parts, rim):
-    n, depth = x.shape[1], x.shape[2]
-    last = n // WINDOW - 1
-    rows = WINDOW + rim.shape[1] // LANES * RIM
-    return pl.pallas_call(
-        tail_kernel,
-        grid=(1,),
-        in_specs=[pl.BlockSpec((4, WINDOW, depth), lambda i: (0, last, 0))]
-        + [pl.BlockSpec((depth, LANES), lambda i: (0, 0))] * 4
-        + [pl.BlockSpec(rim.shape, lambda i: (0, 0))],
-        out_specs=pl.BlockSpec((rows, LANES), lambda i: (0, 0)),
-        out_shape=jax.ShapeDtypeStruct((rows, LANES), jnp.bfloat16),
-        compiler_params=settings(6),
-        cost_estimate=cost(1),
-        name="tail",
-    )(x, *parts, rim)
-
-
-def attn_kernel(sinks, x_ref, w0, w1, w2, w3, att_ref, log_ref, rows_ref):
+def attn_kernel(
+    sinks, x_hbm, w0, w1, w2, w3, rim_ref, att_ref, log_ref, first_ref, last_ref, x_ref, rows_ref, sems
+):
     n = x_ref.shape[1]
     step = 256
     parts = (w0, w1, w2, w3)
-    for at in range(0, n, step):
+    copies = []
+    for k, at in enumerate(range(0, n, step)):
+        copies.append(
+            pltpu.make_async_copy(
+                x_hbm.at[:, at : at + step, :], x_ref.at[:, at : at + step, :], sems.at[k]
+            )
+        )
+        copies[-1].start()
+    heads = [sinks[h] for h in range(4)]
+    att_ref[:WINDOW, :] = jnp.zeros((WINDOW, 2 * LANES), jnp.float32)
+    log_ref[:, :WINDOW] = jnp.zeros((4, WINDOW), jnp.float32)
+    for k in range(rim_ref.shape[1] // LANES):
+        last_ref[WINDOW + k * RIM : WINDOW + (k + 1) * RIM, :] = rim_ref[
+            :, k * LANES : (k + 1) * LANES
+        ]
+    for k, at in enumerate(range(0, n, step)):
+        copies[k].wait()
         acc = dot(x_ref[0, at : at + step, :], w0[...])
         for c in range(1, 4):
             acc = acc + dot(x_ref[c, at : at + step, :], parts[c][...])
         rows_ref[at : at + step, :] = acc.astype(jnp.bfloat16)
-    heads = [sinks[h] for h in range(4)]
-    att_ref[:WINDOW, :] = jnp.zeros((WINDOW, 2 * LANES), jnp.float32)
-    log_ref[:, :WINDOW] = jnp.zeros((4, WINDOW), jnp.float32)
-
-    for b in range(1, n // WINDOW):
-        here, before = b * WINDOW, (b - 1) * WINDOW
-        att, logs = attend_block(
-            rows_ref[here : here + WINDOW, LANES:],
-            rows_ref[before : before + WINDOW, :LANES],
-            rows_ref[here : here + WINDOW, :LANES],
-            heads,
-            None,
-        )
-        att_ref[here : here + WINDOW, :] = att
-        log_ref[:, here : here + WINDOW] = logs
-
-
-def attention(sinks, x, parts):
+        for here in range(max(at, WINDOW), at + step, WINDOW):
+            before = here - WINDOW
+            att, logs = attend_block(
+                rows_ref[here : here + WINDOW, LANES:],
+                rows_ref[before : before + WINDOW, :LANES],
+                rows_ref[here : here + WINDOW, :LANES],
+                heads,
+                None,
+            )
+            att_ref[here : here + WINDOW, :] = att
+            log_ref[:, here : here + WINDOW] = logs
+    first_ref[...] = rows_ref[:WINDOW, :]
+    last_ref[:WINDOW, :] = rows_ref[n - WINDOW : n, :LANES]
+
+
+def attention(sinks, x, parts, rim):
     n = x.shape[1]
     cols = parts[0].shape[1]
+    sent = WINDOW + rim.shape[1] // LANES * RIM
     return pl.pallas_call(
         attn_kernel,
-        in_specs=[SMEM] + [VMEM] * 5,
-        out_specs=[VMEM] * 3,
+        in_specs=[SMEM, HBM] + [VMEM] * 5,
+        out_specs=[VMEM] * 5,
         out_shape=[
             jax.ShapeDtypeStruct((n, 2 * LANES), jnp.float32),
             jax.ShapeDtypeStruct((4, n), jnp.float32),
-            jax.ShapeDtypeStruct((n, cols), jnp.bfloat16),
+            jax.ShapeDtypeStruct((WINDOW, cols), jnp.bfloat16),
+            jax.ShapeDtypeStruct((sent, LANES), jnp.bfloat16),
+            jax.ShapeDtypeStruct(x.shape, x.dtype),
+        ],
+        scratch_shapes=[
+            pltpu.VMEM((n, cols), jnp.bfloat16),
+            pltpu.SemaphoreType.DMA((n // 256,)),
         ],
         compiler_params=settings(20),
         cost_estimate=cost(8),
         name="attn",
-    )(sinks, x, *parts)
+    )(sinks, x, *parts, rim)
 
 
 def conv_kernel(
@@ -297,21 +299,20 @@
     own = own.reshape(16 * mine.shape[0], mine.shape[1])
 
     def classes(block):
-        corner = shift(block, -1, -1)
+        corner = shift(block, 1, 1)
         along_y = shift(block, 0, 1)
         along_z = shift(block, 1, 0)
         return [block, along_y, along_z, corner]
 
     parts_a = classes(own[:, :cut])
     parts_b = classes(own[:, cut:])
+    rim = tokens[n - RIM :]
     x = norm_classes(place, pltpu.with_memory_space_constraint(tokens, pltpu.HBM), gain, 256)
-    last = tail_rows(x, parts_a, tokens[n - RIM :])
+    x = pltpu.with_memory_space_constraint(x, pltpu.HBM)
+    att, logs, first, last, x_near = attention(sink_logits, x, parts_a, rim)
     halo = passed_along(last)
-    att, logs, rows = attention(sink_logits, x, parts_a)
     return tuple(
-        convolution(
-            sink_logits, place, x, parts_b, gain, conv_taps, att, logs, rows, halo
-        )
+        convolution(sink_logits, place, x_near, parts_b, gain, conv_taps, att, logs, first, halo)
     )
 
 

time: 94 us -> 99.3 us (1.056)
  the two profiles are of different devices: /device:TPU:30 before, /device:TPU:68 now
where the time goes in v3:
time: 99.3 us; the launch traced here: 98.8 us
  blocking collectives  43.8 us (44%)
  starting transfers between devices  20.8 us (21%)
  Pallas kernels  19.3 us (19%)
  waiting for transfers between devices  12.1 us (12%)
  local copies, waits for them, and re-layouts  1.88 us (2%)
    all_to_all x1, blocking collectives, layer(): own = lax.all_to_all(sent, ('zh', 'yh'), 0, 0)  43.8 us
    ppermute x6, starting transfers between devices, shift(): return lax.ppermute(value, SP + ('tp',), pairs)  18.9 us
    pallas_call x1, Pallas kernels, attention(): pl.pallas_call(attn_kernel, in_specs=[SMEM, HBM] + [VMEM] * 5, out_specs=...  8.36 us
    ppermute x1, waiting for transfers between devices, passed_along(): return lax.ppermute(value, SP, [(i, i + 1) for i in range(n - 1)])  6.69 us
    pallas_call x1, Pallas kernels, norm_classes(): pl.pallas_call(functools.partial(norm_kernel, block=block), in_specs=[SME...  6.49 us
    ppermute x6, waiting for transfers between devices, shift(): return lax.ppermute(value, SP + ('tp',), pairs)  5.45 us
    pallas_call x1, Pallas kernels, convolution(): pl.pallas_call(conv_kernel, in_specs=[SMEM] * 2 + [VMEM] * 11, out_specs=...  4.48 us
  transfers between devices with their start and end apart: 7, of which 2 were waited for; matrix products, arithmetic and copies ran while one was open for 1% of the time, Pallas kernels for 15%

profile of v3, /device:TPU:68, one launch (start us, length us, event | category | flops | bytes accessed | tf_op | source)
XLA Modules:
  0.0 98.8 jit_solution(13852517541284986149)
XLA Ops:
  0.6 0.0 copy-start
  0.6 0.9 concatenate.3
  1.5 0.1 broadcast_in_dim.2
  1.6 43.8 %all_to_all.5 = bf16[16,32,896]{2,1,0:T(8,128)(2,1)S(1)} all-to-all(bf16[16,32,896]{2,1,0:T(8,128)(2,1)S(1)} %broadcast_in_dim.2), channel_id=1, replica_groups=mesh['zh'=4,'zl'=2,'yh'=4,'yl'=2,'fs'=4,'tp'=2] {'zh','yh'}, dimensions={0} | all-to-all | bytes 1835008 | tf_op jit(solution)/shard_map/all_to_all | solution.py:298
  45.4 1.9 %collective-permute-start = (bf16[512,384]{1,0:T(8,128)(2,1)S(1)}, bf16[512,384]{1,0:T(8,128)(2,1)S(1)}, u32[]{:S(2)}, u32[]{:S(2)}) collective-permute-start(bf16[512,384]{1,0:T(8,128)(2,1)S(1)} %slice.12.w0), channel_id=1, source_target_pairs={{0,8},{1,57},{8,16},{9,1},{16,24},{17,9},{24,32},{25,17},{32,40},{... | collective-permute-start | bytes 1179656 | tf_op jit(solution)/shard_map/ppermute | solution.py:32
  47.4 4.7 %collective-permute-start.3 = (bf16[512,512]{1,0:T(8,128)(2,1)S(1)}, bf16[512,512]{1,0:T(8,128)(2,1)S(1)}, u32[]{:S(2)}, u32[]{:S(2)}) collective-permute-start(bf16[512,512]{1,0:T(8,128)(2,1)S(1)} %slice.13.w0), channel_id=1, source_target_pairs={{0,8},{1,57},{8,16},{9,1},{16,24},{17,9},{24,32},{25,17},{32,40},{... | collective-permute-start | bytes 1572872 | tf_op jit(solution)/shard_map/ppermute | solution.py:32
  52.2 1.9 %collective-permute-start.4 = (bf16[512,512]{1,0:T(8,128)(2,1)S(1)}, bf16[512,512]{1,0:T(8,128)(2,1)S(1)}, u32[]{:S(2)}, u32[]{:S(2)}) collective-permute-start(bf16[512,512]{1,0:T(8,128)(2,1)S(1)} %slice.13.w0), channel_id=1, source_target_pairs={{0,64},{1,449},{8,72},{9,457},{16,80},{17,465},{24,88},{25,473},{3... | collective-permute-start | bytes 1572872 | tf_op jit(solution)/shard_map/ppermute | solution.py:32
  54.1 3.0 %collective-permute-start.5 = (bf16[512,512]{1,0:T(8,128)(2,1)S(1)}, bf16[512,512]{1,0:T(8,128)(2,1)S(1)}, u32[]{:S(2)}, u32[]{:S(2)}) collective-permute-start(bf16[512,512]{1,0:T(8,128)(2,1)S(1)} %slice.13.w0), channel_id=1, source_target_pairs={{0,72},{1,505},{8,80},{9,449},{16,88},{17,457},{24,96},{25,465},{3... | collective-permute-start | bytes 1572872 | tf_op jit(solution)/shard_map/ppermute | solution.py:32
  57.1 2.5 %collective-permute-start.1 = (bf16[512,384]{1,0:T(8,128)(2,1)S(1)}, bf16[512,384]{1,0:T(8,128)(2,1)S(1)}, u32[]{:S(2)}, u32[]{:S(2)}) collective-permute-start(bf16[512,384]{1,0:T(8,128)(2,1)S(1)} %slice.12.w0), channel_id=1, source_target_pairs={{0,64},{1,449},{8,72},{9,457},{16,80},{17,465},{24,88},{25,473},{3... | collective-permute-start | bytes 1179656 | tf_op jit(solution)/shard_map/ppermute | solution.py:32
  59.6 0.0 collective-permute-done.w1
  59.6 4.8 %collective-permute-start.2 = (bf16[512,384]{1,0:T(8,128)(2,1)S(1)}, bf16[512,384]{1,0:T(8,128)(2,1)}, u32[]{:S(2)}, u32[]{:S(2)}) collective-permute-start(bf16[512,384]{1,0:T(8,128)(2,1)S(1)} %slice.12.w0), channel_id=1, source_target_pairs={{0,72},{1,505},{8,80},{9,449},{16,88},{17,457},{24,96},{25,465},{3... | collective-permute-start | bytes 1179656 | tf_op jit(solution)/shard_map/ppermute | solution.py:32
  64.4 0.8 slice.10.rim_ref
  65.3 0.1 pad_add_fusion.place
  65.3 0.0 copy-done
  65.3 0.0 copy-start.2
  65.3 6.5 %norm.1.x_hbm = bf16[4,1024,512]{2,1,0:T(8,128)(2,1)} custom-call(s32[3]{0:T(128)S(1)} %pad_add_fusion.place, bf16[1024,2048]{1,0:T(8,128)(2,1)} %tok_hbm.1, f32[1,2048]{1,0:T(1,128)S(1)} %bitcast.5), custom_call_target="tpu_custom_call" | custom-call | flops 19500000 | bytes 1048576 | tf_op jit(solution)/shard_map/norm/pallas_call | solution.py:93
  71.8 0.0 copy-start.1
  71.8 5.4 %collective-permute-done.1.w2 = bf16[512,384]{1,0:T(8,128)(2,1)S(1)} collective-permute-done((bf16[512,384]{1,0:T(8,128)(2,1)S(1)}, bf16[512,384]{1,0:T(8,128)(2,1)S(1)}, u32[]{:S(2)}, u32[]{:S(2)}) %collective-permute-start.1) | collective-permute-done | bytes 393248 | tf_op jit(solution)/shard_map/ppermute | solution.py:32
  77.3 0.0 collective-permute-done.2.w3
  77.3 0.0 copy-done.2
  77.3 8.4 %attn.1 = (f32[1024,256]{1,0:T(8,128)S(1)}, f32[4,1024]{1,0:T(4,128)S(1)}, bf16[128,384]{1,0:T(8,128)(2,1)S(1)}, bf16[384,128]{1,0:T(8,128)(2,1)S(1)}, bf16[4,1024,512]{2,1,0:T(8,128)(2,1)S(1)}) custom-call(f32[4]{0:T(128)S(1)} %copy-done.2, bf16[4,1024,512]{2,1,0:T(8,128)(2,1)} %norm.1.x_hbm, bf16[512,384]{1,0:T(8,128)(2,1)S(1)} %slice.12.w0, ...), custom_call_target="tpu_custom_call" | custom-call | flops 31200000 | bytes 1048576 | tf_op jit(solution)/shard_map/attn/pallas_call | solution.py:195
  85.7 1.9 %collective-permute-start.6 = (bf16[384,128]{1,0:T(8,128)(2,1)S(1)}, bf16[384,128]{1,0:T(8,128)(2,1)S(1)}, u32[]{:S(2)}, u32[]{:S(2)}) collective-permute-start(bf16[384,128]{1,0:T(8,128)(2,1)S(1)} %get-tuple-element.11), channel_id=1, source_target_pairs={{0,8},{8,16},{16,24},{24,32},{32,40},{40,48},{48,56},{56,64},{64,7... | collective-permute-start | bytes 294920 | tf_op jit(solution)/shard_map/ppermute | solution.py:37
  87.6 6.7 %collective-permute-done.6.halo_ref = bf16[384,128]{1,0:T(8,128)(2,1)S(1)} collective-permute-done((bf16[384,128]{1,0:T(8,128)(2,1)S(1)}, bf16[384,128]{1,0:T(8,128)(2,1)S(1)}, u32[]{:S(2)}, u32[]{:S(2)}) %collective-permute-start.6) | collective-permute-done | bytes 98336 | tf_op jit(solution)/shard_map/ppermute | solution.py:37
  94.3 0.0 collective-permute-done.3.w1
  94.3 0.0 collective-permute-done.4.w2
  94.3 0.0 collective-permute-done.5.w3
  94.3 0.0 copy-done.1
  94.3 4.5 %conv.1 = (bf16[1024,256]{1,0:T(8,128)(2,1)}, f32[4,1024]{1,0:T(4,128)}) custom-call(f32[4]{0:T(128)S(1)} %copy-done.2, s32[3]{0:T(128)S(1)} %pad_add_fusion.place, bf16[4,1024,512]{2,1,0:T(8,128)(2,1)S(1)} %get-tuple-element.7.x_ref, bf16[512,512]{1,0:T(8,128)(2,1)S(1)} %slice.13.w0, bf16[512,512]{1,0:T(8,128)(2,1)S(1)} %collective-permute-done.3.w1, ...), custom_call_target="tpu_custom_call" | custom-call | flops 23400000 | bytes 1048576 | tf_op jit(solution)/shard_map/conv/pallas_call | solution.py:262
  (2 shorter events, 0.1 us)
Async XLA Ops:
  0.6 64.7 %copy-start = (f32[2048]{0:T(1024)S(1)}, f32[2048]{0:T(1024)}, u32[]{:S(2)}) copy-start(f32[2048]{0:T(1024)} %param.10) | copy-start | bytes 24580
  45.4 14.1 %collective-permute-start = (bf16[512,384]{1,0:T(8,128)(2,1)S(1)}, bf16[512,384]{1,0:T(8,128)(2,1)S(1)}, u32[]{:S(2)}, u32[]{:S(2)}) collective-permute-start(bf16[512,384]{1,0:T(8,128)(2,1)S(1)} %slice.12.w0), channel_id=1, source_target_pairs={{0,8},{1,57},{8,16},{9,1},{16,24},{17,9},{24,32},{25,17},{32,40},{... | collective-permute-start | bytes 1179656 | tf_op jit(solution)/shard_map/ppermute | solution.py:32
  47.4 46.9 %collective-permute-start.3 = (bf16[512,512]{1,0:T(8,128)(2,1)S(1)}, bf16[512,512]{1,0:T(8,128)(2,1)S(1)}, u32[]{:S(2)}, u32[]{:S(2)}) collective-permute-start(bf16[512,512]{1,0:T(8,128)(2,1)S(1)} %slice.13.w0), channel_id=1, source_target_pairs={{0,8},{1,57},{8,16},{9,1},{16,24},{17,9},{24,32},{25,17},{32,40},{... | collective-permute-start | bytes 1572872 | tf_op jit(solution)/shard_map/ppermute | solution.py:32
  52.2 42.1 %collective-permute-start.4 = (bf16[512,512]{1,0:T(8,128)(2,1)S(1)}, bf16[512,512]{1,0:T(8,128)(2,1)S(1)}, u32[]{:S(2)}, u32[]{:S(2)}) collective-permute-start(bf16[512,512]{1,0:T(8,128)(2,1)S(1)} %slice.13.w0), channel_id=1, source_target_pairs={{0,64},{1,449},{8,72},{9,457},{16,80},{17,465},{24,88},{25,473},{3... | collective-permute-start | bytes 1572872 | tf_op jit(solution)/shard_map/ppermute | solution.py:32
  54.1 40.2 %collective-permute-start.5 = (bf16[512,512]{1,0:T(8,128)(2,1)S(1)}, bf16[512,512]{1,0:T(8,128)(2,1)S(1)}, u32[]{:S(2)}, u32[]{:S(2)}) collective-permute-start(bf16[512,512]{1,0:T(8,128)(2,1)S(1)} %slice.13.w0), channel_id=1, source_target_pairs={{0,72},{1,505},{8,80},{9,449},{16,88},{17,457},{24,96},{25,465},{3... | collective-permute-start | bytes 1572872 | tf_op jit(solution)/shard_map/ppermute | solution.py:32
  57.1 20.2 %collective-permute-start.1 = (bf16[512,384]{1,0:T(8,128)(2,1)S(1)}, bf16[512,384]{1,0:T(8,128)(2,1)S(1)}, u32[]{:S(2)}, u32[]{:S(2)}) collective-permute-start(bf16[512,384]{1,0:T(8,128)(2,1)S(1)} %slice.12.w0), channel_id=1, source_target_pairs={{0,64},{1,449},{8,72},{9,457},{16,80},{17,465},{24,88},{25,473},{3... | collective-permute-start | bytes 1179656 | tf_op jit(solution)/shard_map/ppermute | solution.py:32
  59.6 17.7 %collective-permute-start.2 = (bf16[512,384]{1,0:T(8,128)(2,1)S(1)}, bf16[512,384]{1,0:T(8,128)(2,1)}, u32[]{:S(2)}, u32[]{:S(2)}) collective-permute-start(bf16[512,384]{1,0:T(8,128)(2,1)S(1)} %slice.12.w0), channel_id=1, source_target_pairs={{0,72},{1,505},{8,80},{9,449},{16,88},{17,457},{24,96},{25,465},{3... | collective-permute-start | bytes 1179656 | tf_op jit(solution)/shard_map/ppermute | solution.py:32
  65.3 11.9 %copy-start.2 = (f32[4]{0:T(128)S(1)}, f32[4]{0:T(128)}, u32[]{:S(2)}) copy-start(f32[4]{0:T(128)} %sinks.3) | copy-start | bytes 52
  71.8 22.5 %copy-start.1 = (bf16[3,256]{1,0:T(4,128)(2,1)S(1)}, bf16[3,256]{1,0:T(4,128)(2,1)}, u32[]{:S(2)}) copy-start(bf16[3,256]{1,0:T(4,128)(2,1)} %taps_ref.1) | copy-start | bytes 4612
  85.7 8.6 %collective-permute-start.6 = (bf16[384,128]{1,0:T(8,128)(2,1)S(1)}, bf16[384,128]{1,0:T(8,128)(2,1)S(1)}, u32[]{:S(2)}, u32[]{:S(2)}) collective-permute-start(bf16[384,128]{1,0:T(8,128)(2,1)S(1)} %get-tuple-element.11), channel_id=1, source_target_pairs={{0,8},{8,16},{16,24},{24,32},{32,40},{40,48},{48,56},{56,64},{64,7... | collective-permute-start | bytes 294920 | tf_op jit(solution)/shard_map/ppermute | solution.py:37

commit v4 on v2

--- a/solution.py
+++ b/solution.py
@@ -69,7 +69,8 @@
                 ]
 
 
-def norm_kernel(place, tok_ref, gain_ref, out_ref):
+def norm_kernel(place, tok_ref, gain_ref, out_ref, rim_ref):
+    rim_ref[...] = tok_ref[tok_ref.shape[0] - RIM :, :]
     norm_into(place, tok_ref[...], gain_ref[...], column_sort(), out_ref)
 
 
@@ -84,9 +85,15 @@
                 pl.BlockSpec((block, width), lambda i, p: (i, 0)),
                 pl.BlockSpec((1, width), lambda i, p: (0, 0)),
             ],
-            out_specs=pl.BlockSpec((4, block, width // 4), lambda i, p: (0, i, 0)),
+            out_specs=[
+                pl.BlockSpec((4, block, width // 4), lambda i, p: (0, i, 0)),
+                pl.BlockSpec((RIM, width), lambda i, p: (0, 0)),
+            ],
         ),
-        out_shape=jax.ShapeDtypeStruct((4, n, width // 4), jnp.bfloat16),
+        out_shape=[
+            jax.ShapeDtypeStruct((4, n, width // 4), jnp.bfloat16),
+            jax.ShapeDtypeStruct((RIM, width), jnp.bfloat16),
+        ],
         compiler_params=settings(14),
         cost_estimate=cost(5),
         name="norm",
@@ -170,11 +177,12 @@
 def attn_kernel(sinks, x_ref, w0, w1, w2, w3, att_ref, log_ref, rows_ref):
     n = x_ref.shape[1]
     step = 256
+    cols = rows_ref.shape[1]
     parts = (w0, w1, w2, w3)
     for at in range(0, n, step):
-        acc = dot(x_ref[0, at : at + step, :], w0[...])
+        acc = dot(x_ref[0, at : at + step, :], w0[:, :cols])
         for c in range(1, 4):
-            acc = acc + dot(x_ref[c, at : at + step, :], parts[c][...])
+            acc = acc + dot(x_ref[c, at : at + step, :], parts[c][:, :cols])
         rows_ref[at : at + step, :] = acc.astype(jnp.bfloat16)
     heads = [sinks[h] for h in range(4)]
     att_ref[:WINDOW, :] = jnp.zeros((WINDOW, 2 * LANES), jnp.float32)
@@ -195,7 +203,7 @@
 
 def attention(sinks, x, parts):
     n = x.shape[1]
-    cols = parts[0].shape[1]
+    cols = parts[1].shape[1]
     return pl.pallas_call(
         attn_kernel,
         in_specs=[SMEM] + [VMEM] * 5,
@@ -218,13 +226,13 @@
     n = x_ref.shape[1]
     width = 2 * LANES
     step = 256
-    parts = (w0, w1, w2, w3)
+    parts = [w[:, w.shape[1] - 2 * width :] for w in (w0, w1, w2, w3)]
     rim = [
         halo_ref[WINDOW + k * RIM : WINDOW + (k + 1) * RIM, :]
         for k in range(gain_ref.shape[1] // LANES)
     ]
     norm_into(place, jnp.concatenate(rim, axis=1), gain_ref[...], column_sort(), prev_x)
-    acc = dot(prev_x[0], w0[:, :width])
+    acc = dot(prev_x[0], parts[0][:, :width])
     for c in range(1, 4):
         acc = acc + dot(prev_x[c], parts[c][:, :width])
     pad_ref[:8, :] = acc[8:16].astype(jnp.bfloat16).astype(jnp.float32)
@@ -239,9 +247,9 @@
     log_out[:, :WINDOW] = log0
     taps = taps_ref[...].astype(jnp.float32)
     for at in range(0, n, step):
-        acc = dot(x_ref[0, at : at + step, :], w0[...])
+        acc = dot(x_ref[0, at : at + step, :], parts[0])
         for c in range(1, 4):
-            acc = acc + dot(x_ref[c, at : at + step, :], parts[c][...])
+            acc = acc + dot(x_ref[c, at : at + step, :], parts[c])
         rounded = acc.astype(jnp.bfloat16).astype(jnp.float32)
         pad_ref[8 + at : 8 + at + step, :] = rounded[:, :width]
         total = taps[0:1] * pad_ref[6 + at : 6 + at + step, :]
@@ -284,7 +292,7 @@
 
 
 def layer(tokens, norm_gain, attn_weights, conv_weights, conv_taps, sink_logits):
-    n, width = tokens.shape
+    _, width = tokens.shape
     gain = norm_gain.reshape(1, width)
     place = jnp.stack(
         [lax.axis_index("zl"), lax.axis_index("yl"), jnp.minimum(lax.axis_index(SP), 1)]
@@ -296,16 +304,17 @@
     own = lax.all_to_all(sent, ("zh", "yh"), 0, 0)
     own = own.reshape(16 * mine.shape[0], mine.shape[1])
 
+    corner = shift(own, -1, -1)
+
     def classes(block):
-        corner = shift(block, -1, -1)
         along_y = shift(block, 0, 1)
         along_z = shift(block, 1, 0)
-        return [block, along_y, along_z, corner]
+        return [own, along_y, along_z, corner]
 
     parts_a = classes(own[:, :cut])
     parts_b = classes(own[:, cut:])
-    x = norm_classes(place, pltpu.with_memory_space_constraint(tokens, pltpu.HBM), gain, 256)
-    last = tail_rows(x, parts_a, tokens[n - RIM :])
+    x, rim = norm_classes(place, pltpu.with_memory_space_constraint(tokens, pltpu.HBM), gain, 256)
+    last = tail_rows(x, parts_a, rim)
     halo = passed_along(last)
     att, logs, rows = attention(sink_logits, x, parts_a)
     return tuple(

time: 94 us -> 92 us (0.979)
  the two profiles are of different devices: /device:TPU:30 before, /device:TPU:42 now
where the time goes in v4:
time: 92 us; the launch traced here: 91.5 us
  blocking collectives  40.3 us (44%)
  starting transfers between devices  24.4 us (27%)
  Pallas kernels  16.4 us (18%)
  waiting for transfers between devices  7.77 us (8%)
  local copies, waits for them, and re-layouts  1.83 us (2%)
    all_to_all x1, blocking collectives, layer(): own = lax.all_to_all(sent, ('zh', 'yh'), 0, 0)  40.3 us
    ppermute x5, starting transfers between devices, shift(): return lax.ppermute(value, SP, pairs)  19.1 us
    ppermute x5, waiting for transfers between devices, shift(): return lax.ppermute(value, SP, pairs)  7.77 us
    pallas_call x1, Pallas kernels, norm_classes(): pl.pallas_call(norm_kernel, grid_spec=pltpu.PrefetchScalarGridSpec(num_sc...  5.71 us
    ppermute x1, starting transfers between devices, passed_along(): return lax.ppermute(value, SP, [(i, i + 1) for i in range(n - 1)])  5.32 us
    pallas_call x1, Pallas kernels, attention(): pl.pallas_call(attn_kernel, in_specs=[SMEM] + [VMEM] * 5, out_specs=[VMEM...  5.31 us
    pallas_call x1, Pallas kernels, convolution(): pl.pallas_call(conv_kernel, in_specs=[SMEM] * 2 + [VMEM] * 11, out_specs=...  5.01 us
  transfers between devices with their start and end apart: 6, of which 2 were waited for; matrix products, arithmetic and copies ran while one was open for 1% of the time, Pallas kernels for 12%

profile of v4, /device:TPU:42, one launch (start us, length us, event | category | flops | bytes accessed | tf_op | source)
XLA Modules:
  0.0 91.5 jit_solution(1356779847885748268)
XLA Ops:
  0.6 0.0 copy-start
  0.6 0.9 concatenate.3
  1.5 0.1 broadcast_in_dim.2
  1.6 40.3 %all_to_all.5 = bf16[16,32,896]{2,1,0:T(8,128)(2,1)S(1)} all-to-all(bf16[16,32,896]{2,1,0:T(8,128)(2,1)S(1)} %broadcast_in_dim.2), channel_id=1, replica_groups=mesh['zh'=4,'zl'=2,'yh'=4,'yl'=2,'fs'=4,'tp'=2] {'zh','yh'}, dimensions={0} | all-to-all | bytes 1835008 | tf_op jit(solution)/shard_map/all_to_all | solution.py:304
  41.9 5.5 %collective-permute-start.2 = (bf16[512,896]{1,0:T(8,128)(2,1)S(1)}, bf16[512,896]{1,0:T(8,128)(2,1)S(1)}, u32[]{:S(2)}, u32[]{:S(2)}) collective-permute-start(bf16[512,896]{1,0:T(8,128)(2,1)S(1)} %bitcast.5), channel_id=1, source_target_pairs={{0,504},{8,448},{16,456},{24,464},{32,472},{40,480},{48,488},{56,4... | collective-permute-start | bytes 2752520 | tf_op jit(solution)/shard_map/ppermute | solution.py:28
  47.4 0.8 slice.8
  48.3 3.4 %collective-permute-start = (bf16[512,512]{1,0:T(8,128)(2,1)}, bf16[512,512]{1,0:T(8,128)(2,1)S(1)}, u32[]{:S(2)}, u32[]{:S(2)}) collective-permute-start(bf16[512,512]{1,0:T(8,128)(2,1)} %slice.8), channel_id=1, source_target_pairs={{0,8},{8,16},{16,24},{24,32},{32,40},{40,48},{48,56},{56,0},{64,72... | collective-permute-start | bytes 1572872 | tf_op jit(solution)/shard_map/ppermute | solution.py:28
  51.7 2.8 %collective-permute-start.1 = (bf16[512,512]{1,0:T(8,128)(2,1)}, bf16[512,512]{1,0:T(8,128)(2,1)}, u32[]{:S(2)}, u32[]{:S(2)}) collective-permute-start(bf16[512,512]{1,0:T(8,128)(2,1)} %slice.8), channel_id=1, source_target_pairs={{0,64},{8,72},{16,80},{24,88},{32,96},{40,104},{48,112},{56,120},{... | collective-permute-start | bytes 1572872 | tf_op jit(solution)/shard_map/ppermute | solution.py:28
  54.6 4.5 %collective-permute-start.3 = (bf16[512,384]{1,0:T(8,128)(2,1)S(1)}, bf16[512,384]{1,0:T(8,128)(2,1)S(1)}, u32[]{:S(2)}, u32[]{:S(2)}) collective-permute-start(bf16[512,384]{1,0:T(8,128)(2,1)S(1)} %slice.9), channel_id=1, source_target_pairs={{0,8},{8,16},{16,24},{24,32},{32,40},{40,48},{48,56},{56,0},{64,72... | collective-permute-start | bytes 1179656 | tf_op jit(solution)/shard_map/ppermute | solution.py:28
  59.1 2.8 %collective-permute-start.4 = (bf16[512,384]{1,0:T(8,128)(2,1)S(1)}, bf16[512,384]{1,0:T(8,128)(2,1)S(1)}, u32[]{:S(2)}, u32[]{:S(2)}) collective-permute-start(bf16[512,384]{1,0:T(8,128)(2,1)S(1)} %slice.9), channel_id=1, source_target_pairs={{0,64},{8,72},{16,80},{24,88},{32,96},{40,104},{48,112},{56,120},{... | collective-permute-start | bytes 1179656 | tf_op jit(solution)/shard_map/ppermute | solution.py:28
  61.9 0.1 pad_add_fusion.place
  62.0 0.0 copy-done
  62.0 5.7 %norm.1 = (bf16[4,1024,512]{2,1,0:T(8,128)(2,1)S(1)}, bf16[16,2048]{1,0:T(8,128)(2,1)S(1)}) custom-call(s32[3]{0:T(128)S(1)} %pad_add_fusion.place, bf16[1024,2048]{1,0:T(8,128)(2,1)} %tok_ref.1, f32[1,2048]{1,0:T(1,128)S(1)} %bitcast.11), custom_call_target="tpu_custom_call" | custom-call | flops 19500000 | bytes 1048576 | tf_op jit(solution)/shard_map/norm/pallas_call | solution.py:79
  67.7 0.0 copy-start.2
  67.7 3.8 %collective-permute-done.3.w1 = bf16[512,384]{1,0:T(8,128)(2,1)S(1)} collective-permute-done((bf16[512,384]{1,0:T(8,128)(2,1)S(1)}, bf16[512,384]{1,0:T(8,128)(2,1)S(1)}, u32[]{:S(2)}, u32[]{:S(2)}) %collective-permute-start.3) | collective-permute-done | bytes 393248 | tf_op jit(solution)/shard_map/ppermute | solution.py:28
  71.5 4.0 %collective-permute-done.4.w2 = bf16[512,384]{1,0:T(8,128)(2,1)S(1)} collective-permute-done((bf16[512,384]{1,0:T(8,128)(2,1)S(1)}, bf16[512,384]{1,0:T(8,128)(2,1)S(1)}, u32[]{:S(2)}, u32[]{:S(2)}) %collective-permute-start.4) | collective-permute-done | bytes 393248 | tf_op jit(solution)/shard_map/ppermute | solution.py:28
  75.5 0.0 collective-permute-done.2.w3
  75.5 0.4 tail.1
  75.8 0.0 copy-start.1
  75.8 5.3 %collective-permute-start.5 = (bf16[384,128]{1,0:T(8,128)(2,1)S(1)}, bf16[384,128]{1,0:T(8,128)(2,1)S(1)}, u32[]{:S(2)}, u32[]{:S(2)}) collective-permute-start(bf16[384,128]{1,0:T(8,128)(2,1)S(1)} %tail.1), channel_id=1, source_target_pairs={{0,8},{8,16},{16,24},{24,32},{32,40},{40,48},{48,56},{56,64},{64,7... | collective-permute-start | bytes 294920 | tf_op jit(solution)/shard_map/ppermute | solution.py:33
  81.2 0.0 copy-done.2
  81.2 5.3 %attn.1 = (f32[1024,256]{1,0:T(8,128)S(1)}, f32[4,1024]{1,0:T(4,128)S(1)}, bf16[1024,384]{1,0:T(8,128)(2,1)S(1)}) custom-call(f32[4]{0:T(128)S(1)} %copy-done.2, bf16[4,1024,512]{2,1,0:T(8,128)(2,1)S(1)} %get-tuple-element.7.x_ref, bf16[512,896]{1,0:T(8,128)(2,1)S(1)} %bitcast.9, bf16[512,384]{1,0:T(8,128)(2,1)S(1)} %collective-permute-done.3.w1, ...), custom_call_target="tpu_custom_call" | custom-call | flops 31200000 | bytes 1048576 | tf_op jit(solution)/shard_map/attn/pallas_call | solution.py:207
  86.5 0.0 collective-permute-done.w1
  86.5 0.0 collective-permute-done.1.w2
  86.5 0.0 collective-permute-done.5.halo_ref
  86.5 0.0 copy-done.1
  86.5 5.0 %conv.1 = (bf16[1024,256]{1,0:T(8,128)(2,1)}, f32[4,1024]{1,0:T(4,128)}) custom-call(f32[4]{0:T(128)S(1)} %copy-done.2, s32[3]{0:T(128)S(1)} %pad_add_fusion.place, bf16[4,1024,512]{2,1,0:T(8,128)(2,1)S(1)} %get-tuple-element.7.x_ref, bf16[512,896]{1,0:T(8,128)(2,1)S(1)} %bitcast.10, bf16[512,512]{1,0:T(8,128)(2,1)S(1)} %collective-permute-done.w1, ...), custom_call_target="tpu_custom_call" | custom-call | flops 23400000 | bytes 1048576 | tf_op jit(solution)/shard_map/conv/pallas_call | solution.py:268
  (1 shorter events, 0.0 us)
Async XLA Ops:
  0.6 61.3 %copy-start = (f32[2048]{0:T(1024)S(1)}, f32[2048]{0:T(1024)}, u32[]{:S(2)}) copy-start(f32[2048]{0:T(1024)} %param.10) | copy-start | bytes 24580
  41.9 33.6 %collective-permute-start.2 = (bf16[512,896]{1,0:T(8,128)(2,1)S(1)}, bf16[512,896]{1,0:T(8,128)(2,1)S(1)}, u32[]{:S(2)}, u32[]{:S(2)}) collective-permute-start(bf16[512,896]{1,0:T(8,128)(2,1)S(1)} %bitcast.5), channel_id=1, source_target_pairs={{0,504},{8,448},{16,456},{24,464},{32,472},{40,480},{48,488},{56,4... | collective-permute-start | bytes 2752520 | tf_op jit(solution)/shard_map/ppermute | solution.py:28
  48.3 38.2 %collective-permute-start = (bf16[512,512]{1,0:T(8,128)(2,1)}, bf16[512,512]{1,0:T(8,128)(2,1)S(1)}, u32[]{:S(2)}, u32[]{:S(2)}) collective-permute-start(bf16[512,512]{1,0:T(8,128)(2,1)} %slice.8), channel_id=1, source_target_pairs={{0,8},{8,16},{16,24},{24,32},{32,40},{40,48},{48,56},{56,0},{64,72... | collective-permute-start | bytes 1572872 | tf_op jit(solution)/shard_map/ppermute | solution.py:28
  51.7 34.8 %collective-permute-start.1 = (bf16[512,512]{1,0:T(8,128)(2,1)}, bf16[512,512]{1,0:T(8,128)(2,1)}, u32[]{:S(2)}, u32[]{:S(2)}) collective-permute-start(bf16[512,512]{1,0:T(8,128)(2,1)} %slice.8), channel_id=1, source_target_pairs={{0,64},{8,72},{16,80},{24,88},{32,96},{40,104},{48,112},{56,120},{... | collective-permute-start | bytes 1572872 | tf_op jit(solution)/shard_map/ppermute | solution.py:28
  54.6 16.9 %collective-permute-start.3 = (bf16[512,384]{1,0:T(8,128)(2,1)S(1)}, bf16[512,384]{1,0:T(8,128)(2,1)S(1)}, u32[]{:S(2)}, u32[]{:S(2)}) collective-permute-start(bf16[512,384]{1,0:T(8,128)(2,1)S(1)} %slice.9), channel_id=1, source_target_pairs={{0,8},{8,16},{16,24},{24,32},{32,40},{40,48},{48,56},{56,0},{64,72... | collective-permute-start | bytes 1179656 | tf_op jit(solution)/shard_map/ppermute | solution.py:28
  59.1 16.4 %collective-permute-start.4 = (bf16[512,384]{1,0:T(8,128)(2,1)S(1)}, bf16[512,384]{1,0:T(8,128)(2,1)S(1)}, u32[]{:S(2)}, u32[]{:S(2)}) collective-permute-start(bf16[512,384]{1,0:T(8,128)(2,1)S(1)} %slice.9), channel_id=1, source_target_pairs={{0,64},{8,72},{16,80},{24,88},{32,96},{40,104},{48,112},{56,120},{... | collective-permute-start | bytes 1179656 | tf_op jit(solution)/shard_map/ppermute | solution.py:28
  67.7 13.5 %copy-start.2 = (f32[4]{0:T(128)S(1)}, f32[4]{0:T(128)}, u32[]{:S(2)}) copy-start(f32[4]{0:T(128)} %sinks.3) | copy-start | bytes 52
  75.8 10.7 %copy-start.1 = (bf16[3,256]{1,0:T(4,128)(2,1)S(1)}, bf16[3,256]{1,0:T(4,128)(2,1)}, u32[]{:S(2)}) copy-start(bf16[3,256]{1,0:T(4,128)(2,1)} %taps_ref.1) | copy-start | bytes 4612
  75.8 10.7 %collective-permute-start.5 = (bf16[384,128]{1,0:T(8,128)(2,1)S(1)}, bf16[384,128]{1,0:T(8,128)(2,1)S(1)}, u32[]{:S(2)}, u32[]{:S(2)}) collective-permute-start(bf16[384,128]{1,0:T(8,128)(2,1)S(1)} %tail.1), channel_id=1, source_target_pairs={{0,8},{8,16},{16,24},{24,32},{32,40},{40,48},{48,56},{56,64},{64,7... | collective-permute-start | bytes 294920 | tf_op jit(solution)/shard_map/ppermute | solution.py:33

commit v5 on v4

--- a/solution.py
+++ b/solution.py
@@ -94,7 +94,7 @@
             jax.ShapeDtypeStruct((4, n, width // 4), jnp.bfloat16),
             jax.ShapeDtypeStruct((RIM, width), jnp.bfloat16),
         ],
-        compiler_params=settings(14),
+        compiler_params=settings(9),
         cost_estimate=cost(5),
         name="norm",
     )(place, rows, gain)
@@ -109,6 +109,7 @@
         zero = jnp.zeros_like(kv)
         return jnp.where(left, kv, zero), jnp.where(left, zero, swapped)
 
+    q = q * jnp.asarray(HEAD_DIM ** (-0.5), q.dtype)
     prev_lo, prev_hi = split(kv_prev)
     cur_lo, cur_hi = split(kv_cur)
     keys = jnp.concatenate([prev_lo, cur_lo, prev_hi, cur_hi], axis=0)
@@ -124,12 +125,12 @@
             cur = both[side * 256 + WINDOW : side * 256 + 2 * WINDOW]
             if has_prev is not None:
                 prev = jnp.where(has_prev, prev, -jnp.inf)
-            scores = jnp.where(from_prev, prev, cur) * HEAD_DIM ** (-0.5)
+            scores = jnp.where(from_prev, prev, cur)
             top = jnp.maximum(jnp.max(scores, axis=0, keepdims=True), sinks[head])
             raised = jnp.exp(scores - top)
             total = jnp.sum(raised, axis=0, keepdims=True) + jnp.exp(sinks[head] - top)
             logs.append(top + jnp.log(total))
-            share = raised / total
+            share = raised * (1.0 / total)
             zero = jnp.zeros_like(share)
             weights.append(
                 jnp.concatenate(
@@ -145,10 +146,59 @@
     return jnp.concatenate(outs, axis=1), jnp.concatenate(logs, axis=0)
 
 
-def tail_kernel(x_ref, w0, w1, w2, w3, rim_ref, out_ref):
-    acc = dot(x_ref[0], w0[...])
-    for c, w in ((1, w1), (2, w2), (3, w3)):
-        acc = acc + dot(x_ref[c], w[...])
+def cut_kernel(own_ref, a_ref, b_ref):
+    cols = a_ref.shape[1]
+    a_ref[...] = own_ref[:, :cols]
+    b_ref[...] = own_ref[:, cols:]
+
+
+def cut_columns(own, cols):
+    n, width = own.shape
+    return pl.pallas_call(
+        cut_kernel,
+        in_specs=[VMEM],
+        out_specs=[VMEM] * 2,
+        out_shape=[
+            jax.ShapeDtypeStruct((n, cols), own.dtype),
+            jax.ShapeDtypeStruct((n, width - cols), own.dtype),
+        ],
+        compiler_params=settings(2),
+        cost_estimate=cost(1),
+        name="cut",
+    )(own)
+
+
+def early_kernel(x_ref, own_ref, y_ref, sum_a, sum_b):
+    n = x_ref.shape[1]
+    cols = sum_a.shape[1]
+    step = 256
+    for at in range(0, n, step):
+        mine = x_ref[0, at : at + step, :]
+        sum_b[at : at + step, :] = dot(mine, own_ref[:, cols:])
+        sum_a[at : at + step, :] = dot(mine, own_ref[:, :cols]) + dot(
+            x_ref[1, at : at + step, :], y_ref[...]
+        )
+
+
+def early_sums(x, own, along_y):
+    n = x.shape[1]
+    cols = along_y.shape[1]
+    return pl.pallas_call(
+        early_kernel,
+        in_specs=[VMEM] * 3,
+        out_specs=[VMEM] * 2,
+        out_shape=[
+            jax.ShapeDtypeStruct((n, cols), jnp.float32),
+            jax.ShapeDtypeStruct((n, own.shape[1] - cols), jnp.float32),
+        ],
+        compiler_params=settings(4),
+        cost_estimate=cost(2),
+        name="early",
+    )(x, own, along_y)
+
+
+def tail_kernel(x_ref, sum_ref, w2, w3, rim_ref, out_ref):
+    acc = sum_ref[...] + dot(x_ref[2], w2[...]) + dot(x_ref[3], w3[...])
     out_ref[:WINDOW, :] = acc.astype(jnp.bfloat16)
     for k in range(rim_ref.shape[1] // LANES):
         out_ref[WINDOW + k * RIM : WINDOW + (k + 1) * RIM, :] = rim_ref[
@@ -156,33 +206,34 @@
         ]
 
 
-def tail_rows(x, parts, rim):
+def tail_rows(x, sums, parts, rim):
     n, depth = x.shape[1], x.shape[2]
     last = n // WINDOW - 1
     rows = WINDOW + rim.shape[1] // LANES * RIM
     return pl.pallas_call(
         tail_kernel,
         grid=(1,),
-        in_specs=[pl.BlockSpec((4, WINDOW, depth), lambda i: (0, last, 0))]
-        + [pl.BlockSpec((depth, LANES), lambda i: (0, 0))] * 4
+        in_specs=[
+            pl.BlockSpec((4, WINDOW, depth), lambda i: (0, last, 0)),
+            pl.BlockSpec((WINDOW, LANES), lambda i: (last, 0)),
+        ]
+        + [pl.BlockSpec((depth, LANES), lambda i: (0, 0))] * 2
         + [pl.BlockSpec(rim.shape, lambda i: (0, 0))],
         out_specs=pl.BlockSpec((rows, LANES), lambda i: (0, 0)),
         out_shape=jax.ShapeDtypeStruct((rows, LANES), jnp.bfloat16),
-        compiler_params=settings(6),
+        compiler_params=settings(3),
         cost_estimate=cost(1),
         name="tail",
-    )(x, *parts, rim)
-
-
-def attn_kernel(sinks, x_ref, w0, w1, w2, w3, att_ref, log_ref, rows_ref):
+    )(x, sums, *parts, rim)
+
+
+def attn_kernel(sinks, x_ref, sum_ref, w2, w3, att_ref, log_ref, rows_ref):
     n = x_ref.shape[1]
     step = 256
     cols = rows_ref.shape[1]
-    parts = (w0, w1, w2, w3)
     for at in range(0, n, step):
-        acc = dot(x_ref[0, at : at + step, :], w0[:, :cols])
-        for c in range(1, 4):
-            acc = acc + dot(x_ref[c, at : at + step, :], parts[c][:, :cols])
+        acc = sum_ref[at : at + step, :] + dot(x_ref[2, at : at + step, :], w2[...])
+        acc = acc + dot(x_ref[3, at : at + step, :], w3[:, :cols])
         rows_ref[at : at + step, :] = acc.astype(jnp.bfloat16)
     heads = [sinks[h] for h in range(4)]
     att_ref[:WINDOW, :] = jnp.zeros((WINDOW, 2 * LANES), jnp.float32)
@@ -201,27 +252,27 @@
         log_ref[:, here : here + WINDOW] = logs
 
 
-def attention(sinks, x, parts):
+def attention(sinks, x, sums, parts):
     n = x.shape[1]
-    cols = parts[1].shape[1]
+    cols = sums.shape[1]
     return pl.pallas_call(
         attn_kernel,
-        in_specs=[SMEM] + [VMEM] * 5,
+        in_specs=[SMEM] + [VMEM] * 4,
         out_specs=[VMEM] * 3,
         out_shape=[
             jax.ShapeDtypeStruct((n, 2 * LANES), jnp.float32),
             jax.ShapeDtypeStruct((4, n), jnp.float32),
             jax.ShapeDtypeStruct((n, cols), jnp.bfloat16),
         ],
-        compiler_params=settings(20),
+        compiler_params=settings(8),
         cost_estimate=cost(8),
         name="attn",
-    )(sinks, x, *parts)
+    )(sinks, x, sums, *parts)
 
 
 def conv_kernel(
-    sinks, place, x_ref, w0, w1, w2, w3, gain_ref, taps_ref, att_ref, log_ref, rows_ref, halo_ref,
-    out_ref, log_out, pad_ref, prev_x,
+    sinks, place, x_ref, sum_ref, w0, w1, w2, w3, gain_ref, taps_ref, att_ref, log_ref, rows_ref, halo_ref,
+    out_hbm, log_out, out_ref, pad_ref, prev_x, sems,
 ):
     n = x_ref.shape[1]
     width = 2 * LANES
@@ -246,9 +297,10 @@
     log_out[...] = log_ref[...]
     log_out[:, :WINDOW] = log0
     taps = taps_ref[...].astype(jnp.float32)
-    for at in range(0, n, step):
-        acc = dot(x_ref[0, at : at + step, :], parts[0])
-        for c in range(1, 4):
+    copies = []
+    for k, at in enumerate(range(0, n, step)):
+        acc = sum_ref[at : at + step, :] + dot(x_ref[1, at : at + step, :], parts[1])
+        for c in range(2, 4):
             acc = acc + dot(x_ref[c, at : at + step, :], parts[c])
         rounded = acc.astype(jnp.bfloat16).astype(jnp.float32)
         pad_ref[8 + at : 8 + at + step, :] = rounded[:, :width]
@@ -261,26 +313,36 @@
         else:
             first = att_ref[at : at + step, :]
         out_ref[at : at + step, :] = (first + gated).astype(jnp.bfloat16)
-
-
-def convolution(sinks, place, x, parts, gain, taps, att, logs, rows, halo):
+        copies.append(
+            pltpu.make_async_copy(
+                out_ref.at[at : at + step, :], out_hbm.at[at : at + step, :], sems.at[k]
+            )
+        )
+        copies[-1].start()
+    for copy in copies:
+        copy.wait()
+
+
+def convolution(sinks, place, x, sums, parts, gain, taps, att, logs, rows, halo):
     n = x.shape[1]
     return pl.pallas_call(
         conv_kernel,
-        in_specs=[SMEM] * 2 + [VMEM] * 11,
-        out_specs=[VMEM] * 2,
+        in_specs=[SMEM] * 2 + [VMEM] * 12,
+        out_specs=[HBM, VMEM],
         out_shape=[
             jax.ShapeDtypeStruct((n, 2 * LANES), jnp.bfloat16),
             jax.ShapeDtypeStruct((4, n), jnp.float32),
         ],
         scratch_shapes=[
+            pltpu.VMEM((n, 2 * LANES), jnp.bfloat16),
             pltpu.VMEM((n + 8, 2 * LANES), jnp.float32),
             pltpu.VMEM((4, RIM, x.shape[2]), jnp.bfloat16),
-        ],
-        compiler_params=settings(20),
+            pltpu.SemaphoreType.DMA((n // 256,)),
+        ],
+        compiler_params=settings(8),
         cost_estimate=cost(6),
         name="conv",
-    )(sinks, place, x, *parts, gain, taps, att, logs, rows, halo)
+    )(sinks, place, x, sums, *parts, gain, taps, att, logs, rows, halo)
 
 
 def body(
@@ -311,16 +373,16 @@
         along_z = shift(block, 1, 0)
         return [own, along_y, along_z, corner]
 
-    parts_a = classes(own[:, :cut])
-    parts_b = classes(own[:, cut:])
+    own_a, own_b = cut_columns(own, cut)
+    parts_a = classes(own_a)
+    parts_b = classes(own_b)
     x, rim = norm_classes(place, pltpu.with_memory_space_constraint(tokens, pltpu.HBM), gain, 256)
-    last = tail_rows(x, parts_a, rim)
+    sum_a, sum_b = early_sums(x, own, parts_a[1])
+    last = tail_rows(x, sum_a, parts_a[2:], rim)
     halo = passed_along(last)
-    att, logs, rows = attention(sink_logits, x, parts_a)
+    att, logs, rows = attention(sink_logits, x, sum_a, parts_a[2:])
     return tuple(
-        convolution(
-            sink_logits, place, x, parts_b, gain, conv_taps, att, logs, rows, halo
-        )
+        convolution(sink_logits, place, x, sum_b, parts_b, gain, conv_taps, att, logs, rows, halo)
     )
 
 

time: 92 us -> 90.9 us (0.988)
  the two profiles are of different devices: /device:TPU:42 before, /device:TPU:70 now
where the time goes in v5:
time: 90.9 us; the launch traced here: 90.4 us
  blocking collectives  43.8 us (48%)
  Pallas kernels  18.5 us (20%)
  starting transfers between devices  15.9 us (17%)
  waiting for transfers between devices  9.59 us (11%)
  local copies, waits for them, and re-layouts  1.65 us (2%)
    all_to_all x1, blocking collectives, layer(): own = lax.all_to_all(sent, ('zh', 'yh'), 0, 0)  43.8 us
    ppermute x5, starting transfers between devices, shift(): return lax.ppermute(value, SP, pairs)  14 us
    ppermute x5, waiting for transfers between devices, shift(): return lax.ppermute(value, SP, pairs)  7.14 us
    pallas_call x1, Pallas kernels, norm_classes(): pl.pallas_call(norm_kernel, grid_spec=pltpu.PrefetchScalarGridSpec(num_sc...  5.72 us
    pallas_call x1, Pallas kernels, convolution(): pl.pallas_call(conv_kernel, in_specs=[SMEM] * 2 + [VMEM] * 12, out_specs=...  4.53 us
    pallas_call x1, Pallas kernels, attention(): pl.pallas_call(attn_kernel, in_specs=[SMEM] + [VMEM] * 4, out_specs=[VMEM...  4.22 us
    pallas_call x1, Pallas kernels, early_sums(): pl.pallas_call(early_kernel, in_specs=[VMEM] * 3, out_specs=[VMEM] * 2, o...  2.83 us
    ppermute x1, waiting for transfers between devices, passed_along(): return lax.ppermute(value, SP, [(i, i + 1) for i in range(n - 1)])  2.44 us
  transfers between devices with their start and end apart: 6, of which 2 were waited for; matrix products, arithmetic and copies ran while one was open for 0% of the time, Pallas kernels for 15%

profile of v5, /device:TPU:70, one launch (start us, length us, event | category | flops | bytes accessed | tf_op | source)
XLA Modules:
  0.0 90.4 jit_solution(632603857184415378)
XLA Ops:
  0.6 0.9 concatenate.3
  1.5 0.1 broadcast_in_dim.2
  1.6 43.8 %all_to_all.5 = bf16[16,32,896]{2,1,0:T(8,128)(2,1)S(1)} all-to-all(bf16[16,32,896]{2,1,0:T(8,128)(2,1)S(1)} %broadcast_in_dim.2), channel_id=1, replica_groups=mesh['zh'=4,'zl'=2,'yh'=4,'yl'=2,'fs'=4,'tp'=2] {'zh','yh'}, dimensions={0} | all-to-all | bytes 1835008 | tf_op jit(solution)/shard_map/all_to_all | solution.py:366
  45.4 1.9 %collective-permute-start.3 = (bf16[512,896]{1,0:T(8,128)(2,1)S(1)}, bf16[512,896]{1,0:T(8,128)(2,1)S(1)}, u32[]{:S(2)}, u32[]{:S(2)}) collective-permute-start(bf16[512,896]{1,0:T(8,128)(2,1)S(1)} %bitcast.5), channel_id=1, source_target_pairs={{0,504},{8,448},{16,456},{24,464},{32,472},{40,480},{48,488},{56,4... | collective-permute-start | bytes 2752520 | tf_op jit(solution)/shard_map/ppermute | solution.py:28
  47.3 1.0 %cut.1 = (bf16[512,384]{1,0:T(8,128)(2,1)}, bf16[512,512]{1,0:T(8,128)(2,1)}) custom-call(bf16[512,896]{1,0:T(8,128)(2,1)S(1)} %bitcast.6), custom_call_target="tpu_custom_call" | custom-call | flops 3900000 | bytes 1048576 | tf_op jit(solution)/shard_map/cut/pallas_call | solution.py:157
  48.3 4.0 %collective-permute-start.1 = (bf16[512,512]{1,0:T(8,128)(2,1)}, bf16[512,512]{1,0:T(8,128)(2,1)S(1)}, u32[]{:S(2)}, u32[]{:S(2)}) collective-permute-start(bf16[512,512]{1,0:T(8,128)(2,1)} %get-tuple-element.14), channel_id=1, source_target_pairs={{0,8},{8,16},{16,24},{24,32},{32,40},{40,48},{48,56},{56,0},{64,72... | collective-permute-start | bytes 1572872 | tf_op jit(solution)/shard_map/ppermute | solution.py:28
  52.3 3.3 %collective-permute-start.2 = (bf16[512,512]{1,0:T(8,128)(2,1)}, bf16[512,512]{1,0:T(8,128)(2,1)S(1)}, u32[]{:S(2)}, u32[]{:S(2)}) collective-permute-start(bf16[512,512]{1,0:T(8,128)(2,1)} %get-tuple-element.14), channel_id=1, source_target_pairs={{0,64},{8,72},{16,80},{24,88},{32,96},{40,104},{48,112},{56,120},{... | collective-permute-start | bytes 1572872 | tf_op jit(solution)/shard_map/ppermute | solution.py:28
  55.6 1.9 %collective-permute-start = (bf16[512,384]{1,0:T(8,128)(2,1)}, bf16[512,384]{1,0:T(8,128)(2,1)}, u32[]{:S(2)}, u32[]{:S(2)}) collective-permute-start(bf16[512,384]{1,0:T(8,128)(2,1)} %get-tuple-element.12), channel_id=1, source_target_pairs={{0,8},{8,16},{16,24},{24,32},{32,40},{40,48},{48,56},{56,0},{64,72... | collective-permute-start | bytes 1179656 | tf_op jit(solution)/shard_map/ppermute | solution.py:28
  57.5 2.9 %collective-permute-start.4 = (bf16[512,384]{1,0:T(8,128)(2,1)}, bf16[512,384]{1,0:T(8,128)(2,1)S(1)}, u32[]{:S(2)}, u32[]{:S(2)}) collective-permute-start(bf16[512,384]{1,0:T(8,128)(2,1)} %get-tuple-element.12), channel_id=1, source_target_pairs={{0,64},{8,72},{16,80},{24,88},{32,96},{40,104},{48,112},{56,120},{... | collective-permute-start | bytes 1179656 | tf_op jit(solution)/shard_map/ppermute | solution.py:28
  60.4 0.1 pad_add_fusion.place
  60.5 0.0 copy-start
  60.5 0.7 copy-done
  61.2 5.7 %norm.1 = (bf16[4,1024,512]{2,1,0:T(8,128)(2,1)S(1)}, bf16[16,2048]{1,0:T(8,128)(2,1)S(1)}) custom-call(s32[3]{0:T(128)S(1)} %pad_add_fusion.place, bf16[1024,2048]{1,0:T(8,128)(2,1)} %tok_ref.1, f32[1,2048]{1,0:T(1,128)S(1)} %bitcast.9), custom_call_target="tpu_custom_call" | custom-call | flops 19500000 | bytes 1048576 | tf_op jit(solution)/shard_map/norm/pallas_call | solution.py:79
  66.9 7.1 %collective-permute-done.y_ref = bf16[512,384]{1,0:T(8,128)(2,1)} collective-permute-done((bf16[512,384]{1,0:T(8,128)(2,1)}, bf16[512,384]{1,0:T(8,128)(2,1)}, u32[]{:S(2)}, u32[]{:S(2)}) %collective-permute-start) | collective-permute-done | bytes 393248 | tf_op jit(solution)/shard_map/ppermute | solution.py:28
  74.1 2.8 %early.1 = (f32[1024,384]{1,0:T(8,128)S(1)}, f32[1024,512]{1,0:T(8,128)S(1)}) custom-call(bf16[4,1024,512]{2,1,0:T(8,128)(2,1)S(1)} %get-tuple-element.11.x_ref, bf16[512,896]{1,0:T(8,128)(2,1)S(1)} %bitcast.7, bf16[512,384]{1,0:T(8,128)(2,1)} %collective-permute-done.y_ref), custom_call_target="tpu_custom_call" | custom-call | flops 7800000 | bytes 1048576 | tf_op jit(solution)/shard_map/early/pallas_call | solution.py:186
  76.9 0.0 copy-start.1
  76.9 0.0 collective-permute-done.4.w2
  76.9 0.0 collective-permute-done.3.w3
  76.9 0.3 tail.1
  77.2 0.0 copy-start.2
  77.2 1.9 %collective-permute-start.5 = (bf16[384,128]{1,0:T(8,128)(2,1)S(1)}, bf16[384,128]{1,0:T(8,128)(2,1)S(1)}, u32[]{:S(2)}, u32[]{:S(2)}) collective-permute-start(bf16[384,128]{1,0:T(8,128)(2,1)S(1)} %tail.1), channel_id=1, source_target_pairs={{0,8},{8,16},{16,24},{24,32},{32,40},{40,48},{48,56},{56,64},{64,7... | collective-permute-start | bytes 294920 | tf_op jit(solution)/shard_map/ppermute | solution.py:33
  79.1 0.0 copy-done.1
  79.2 4.2 %attn.1 = (f32[1024,256]{1,0:T(8,128)S(1)}, f32[4,1024]{1,0:T(4,128)S(1)}, bf16[1024,384]{1,0:T(8,128)(2,1)S(1)}) custom-call(f32[4]{0:T(128)S(1)} %copy-done.1, bf16[4,1024,512]{2,1,0:T(8,128)(2,1)S(1)} %get-tuple-element.11.x_ref, f32[1024,384]{1,0:T(8,128)S(1)} %get-tuple-element.15.sum_ref, bf16[512,384]{1,0:T(8,128)(2,1)S(1)} %collective-permute-done.4.w2, ...), custom_call_target="tpu_custom_call" | custom-call | flops 31200000 | bytes 1048576 | tf_op jit(solution)/shard_map/attn/pallas_call | solution.py:258
  83.4 0.0 collective-permute-done.1.w1
  83.4 0.0 collective-permute-done.2.w2
  83.4 2.4 %collective-permute-done.5.halo_ref = bf16[384,128]{1,0:T(8,128)(2,1)S(1)} collective-permute-done((bf16[384,128]{1,0:T(8,128)(2,1)S(1)}, bf16[384,128]{1,0:T(8,128)(2,1)S(1)}, u32[]{:S(2)}, u32[]{:S(2)}) %collective-permute-start.5) | collective-permute-done | bytes 98336 | tf_op jit(solution)/shard_map/ppermute | solution.py:33
  85.8 0.0 copy-done.2
  85.8 4.5 %conv.1 = (bf16[1024,256]{1,0:T(8,128)(2,1)}, f32[4,1024]{1,0:T(4,128)}) custom-call(f32[4]{0:T(128)S(1)} %copy-done.1, s32[3]{0:T(128)S(1)} %pad_add_fusion.place, bf16[4,1024,512]{2,1,0:T(8,128)(2,1)S(1)} %get-tuple-element.11.x_ref, f32[1024,512]{1,0:T(8,128)S(1)} %get-tuple-element.13.sum_ref, bf16[512,896]{1,0:T(8,128)(2,1)S(1)} %bitcast.8, ...), custom_call_target="tpu_custom_call" | custom-call | flops 23400000 | bytes 1048576 | tf_op jit(solution)/shard_map/conv/pallas_call | solution.py:328
Async XLA Ops:
  45.4 31.6 %collective-permute-start.3 = (bf16[512,896]{1,0:T(8,128)(2,1)S(1)}, bf16[512,896]{1,0:T(8,128)(2,1)S(1)}, u32[]{:S(2)}, u32[]{:S(2)}) collective-permute-start(bf16[512,896]{1,0:T(8,128)(2,1)S(1)} %bitcast.5), channel_id=1, source_target_pairs={{0,504},{8,448},{16,456},{24,464},{32,472},{40,480},{48,488},{56,4... | collective-permute-start | bytes 2752520 | tf_op jit(solution)/shard_map/ppermute | solution.py:28
  48.3 35.1 %collective-permute-start.1 = (bf16[512,512]{1,0:T(8,128)(2,1)}, bf16[512,512]{1,0:T(8,128)(2,1)S(1)}, u32[]{:S(2)}, u32[]{:S(2)}) collective-permute-start(bf16[512,512]{1,0:T(8,128)(2,1)} %get-tuple-element.14), channel_id=1, source_target_pairs={{0,8},{8,16},{16,24},{24,32},{32,40},{40,48},{48,56},{56,0},{64,72... | collective-permute-start | bytes 1572872 | tf_op jit(solution)/shard_map/ppermute | solution.py:28
  52.3 31.1 %collective-permute-start.2 = (bf16[512,512]{1,0:T(8,128)(2,1)}, bf16[512,512]{1,0:T(8,128)(2,1)S(1)}, u32[]{:S(2)}, u32[]{:S(2)}) collective-permute-start(bf16[512,512]{1,0:T(8,128)(2,1)} %get-tuple-element.14), channel_id=1, source_target_pairs={{0,64},{8,72},{16,80},{24,88},{32,96},{40,104},{48,112},{56,120},{... | collective-permute-start | bytes 1572872 | tf_op jit(solution)/shard_map/ppermute | solution.py:28
  55.6 18.5 %collective-permute-start = (bf16[512,384]{1,0:T(8,128)(2,1)}, bf16[512,384]{1,0:T(8,128)(2,1)}, u32[]{:S(2)}, u32[]{:S(2)}) collective-permute-start(bf16[512,384]{1,0:T(8,128)(2,1)} %get-tuple-element.12), channel_id=1, source_target_pairs={{0,8},{8,16},{16,24},{24,32},{32,40},{40,48},{48,56},{56,0},{64,72... | collective-permute-start | bytes 1179656 | tf_op jit(solution)/shard_map/ppermute | solution.py:28
  57.5 19.4 %collective-permute-start.4 = (bf16[512,384]{1,0:T(8,128)(2,1)}, bf16[512,384]{1,0:T(8,128)(2,1)S(1)}, u32[]{:S(2)}, u32[]{:S(2)}) collective-permute-start(bf16[512,384]{1,0:T(8,128)(2,1)} %get-tuple-element.12), channel_id=1, source_target_pairs={{0,64},{8,72},{16,80},{24,88},{32,96},{40,104},{48,112},{56,120},{... | collective-permute-start | bytes 1179656 | tf_op jit(solution)/shard_map/ppermute | solution.py:28
  60.5 0.7 copy-start
  76.9 2.2 %copy-start.1 = (f32[4]{0:T(128)S(1)}, f32[4]{0:T(128)}, u32[]{:S(2)}) copy-start(f32[4]{0:T(128)} %sinks.3) | copy-start | bytes 52
  77.2 8.6 %copy-start.2 = (bf16[3,256]{1,0:T(4,128)(2,1)S(1)}, bf16[3,256]{1,0:T(4,128)(2,1)}, u32[]{:S(2)}) copy-start(bf16[3,256]{1,0:T(4,128)(2,1)} %taps_ref.1) | copy-start | bytes 4612
  77.2 8.6 %collective-permute-start.5 = (bf16[384,128]{1,0:T(8,128)(2,1)S(1)}, bf16[384,128]{1,0:T(8,128)(2,1)S(1)}, u32[]{:S(2)}, u32[]{:S(2)}) collective-permute-start(bf16[384,128]{1,0:T(8,128)(2,1)S(1)} %tail.1), channel_id=1, source_target_pairs={{0,8},{8,16},{16,24},{24,32},{32,40},{40,48},{48,56},{56,64},{64,7... | collective-permute-start | bytes 294920 | tf_op jit(solution)/shard_map/ppermute | solution.py:33

commit v6 on v5

--- a/solution.py
+++ b/solution.py
@@ -168,77 +168,51 @@
     )(own)
 
 
-def early_kernel(x_ref, own_ref, y_ref, sum_a, sum_b):
+def early_kernel(x_ref, own_ref, y_ref, z_ref, sum_ref):
     n = x_ref.shape[1]
-    cols = sum_a.shape[1]
-    step = 256
+    cols = sum_ref.shape[1]
+    step = 512
     for at in range(0, n, step):
-        mine = x_ref[0, at : at + step, :]
-        sum_b[at : at + step, :] = dot(mine, own_ref[:, cols:])
-        sum_a[at : at + step, :] = dot(mine, own_ref[:, :cols]) + dot(
-            x_ref[1, at : at + step, :], y_ref[...]
-        )
-
-
-def early_sums(x, own, along_y):
+        acc = dot(x_ref[0, at : at + step, :], own_ref[:, :cols])
+        acc = acc + dot(x_ref[1, at : at + step, :], y_ref[...])
+        sum_ref[at : at + step, :] = acc + dot(x_ref[2, at : at + step, :], z_ref[...])
+
+
+def early_sums(x, own, along_y, along_z):
     n = x.shape[1]
     cols = along_y.shape[1]
     return pl.pallas_call(
         early_kernel,
-        in_specs=[VMEM] * 3,
-        out_specs=[VMEM] * 2,
-        out_shape=[
-            jax.ShapeDtypeStruct((n, cols), jnp.float32),
-            jax.ShapeDtypeStruct((n, own.shape[1] - cols), jnp.float32),
-        ],
+        in_specs=[VMEM] * 4,
+        out_specs=VMEM,
+        out_shape=jax.ShapeDtypeStruct((n, cols), jnp.float32),
         compiler_params=settings(4),
         cost_estimate=cost(2),
         name="early",
-    )(x, own, along_y)
-
-
-def tail_kernel(x_ref, sum_ref, w2, w3, rim_ref, out_ref):
-    acc = sum_ref[...] + dot(x_ref[2], w2[...]) + dot(x_ref[3], w3[...])
-    out_ref[:WINDOW, :] = acc.astype(jnp.bfloat16)
-    for k in range(rim_ref.shape[1] // LANES):
-        out_ref[WINDOW + k * RIM : WINDOW + (k + 1) * RIM, :] = rim_ref[
-            :, k * LANES : (k + 1) * LANES
-        ]
-
-
-def tail_rows(x, sums, parts, rim):
-    n, depth = x.shape[1], x.shape[2]
-    last = n // WINDOW - 1
-    rows = WINDOW + rim.shape[1] // LANES * RIM
-    return pl.pallas_call(
-        tail_kernel,
-        grid=(1,),
-        in_specs=[
-            pl.BlockSpec((4, WINDOW, depth), lambda i: (0, last, 0)),
-            pl.BlockSpec((WINDOW, LANES), lambda i: (last, 0)),
-        ]
-        + [pl.BlockSpec((depth, LANES), lambda i: (0, 0))] * 2
-        + [pl.BlockSpec(rim.shape, lambda i: (0, 0))],
-        out_specs=pl.BlockSpec((rows, LANES), lambda i: (0, 0)),
-        out_shape=jax.ShapeDtypeStruct((rows, LANES), jnp.bfloat16),
-        compiler_params=settings(3),
-        cost_estimate=cost(1),
-        name="tail",
-    )(x, sums, *parts, rim)
-
-
-def attn_kernel(sinks, x_ref, sum_ref, w2, w3, att_ref, log_ref, rows_ref):
+    )(x, own, along_y, along_z)
+
+
+def attn_kernel(
+    sinks, x_ref, sum_ref, own_ref, corner_ref, rim_ref, att_ref, log_ref, first_ref, last_ref, sum_b, rows_ref
+):
     n = x_ref.shape[1]
     step = 256
     cols = rows_ref.shape[1]
+    heads = [sinks[h] for h in range(4)]
+    log_ref[:, :WINDOW] = jnp.zeros((4, WINDOW), jnp.float32)
+    for k in range(rim_ref.shape[1] // LANES):
+        last_ref[WINDOW + k * RIM : WINDOW + (k + 1) * RIM, :] = rim_ref[
+            :, k * LANES : (k + 1) * LANES
+        ]
     for at in range(0, n, step):
-        acc = sum_ref[at : at + step, :] + dot(x_ref[2, at : at + step, :], w2[...])
-        acc = acc + dot(x_ref[3, at : at + step, :], w3[:, :cols])
+        far = x_ref[3, at : at + step, :]
+        acc = sum_ref[at : at + step, :] + dot(far, corner_ref[:, :cols])
         rows_ref[at : at + step, :] = acc.astype(jnp.bfloat16)
-    heads = [sinks[h] for h in range(4)]
-    att_ref[:WINDOW, :] = jnp.zeros((WINDOW, 2 * LANES), jnp.float32)
-    log_ref[:, :WINDOW] = jnp.zeros((4, WINDOW), jnp.float32)
-
+        sum_b[at : at + step, :] = dot(far, corner_ref[:, cols:]) + dot(
+            x_ref[0, at : at + step, :], own_ref[:, cols:]
+        )
+    first_ref[...] = rows_ref[:WINDOW, :]
+    last_ref[:WINDOW, :] = rows_ref[n - WINDOW : n, :LANES]
     for b in range(1, n // WINDOW):
         here, before = b * WINDOW, (b - 1) * WINDOW
         att, logs = attend_block(
@@ -248,101 +222,152 @@
             heads,
             None,
         )
-        att_ref[here : here + WINDOW, :] = att
+        att_ref[before : before + WINDOW, :] = att
         log_ref[:, here : here + WINDOW] = logs
 
 
-def attention(sinks, x, sums, parts):
+def attention(sinks, x, sums, own, corner, rim):
     n = x.shape[1]
     cols = sums.shape[1]
     return pl.pallas_call(
         attn_kernel,
-        in_specs=[SMEM] + [VMEM] * 4,
-        out_specs=[VMEM] * 3,
+        in_specs=[SMEM] + [VMEM] * 5,
+        out_specs=[VMEM] * 5,
         out_shape=[
-            jax.ShapeDtypeStruct((n, 2 * LANES), jnp.float32),
+            jax.ShapeDtypeStruct((n - WINDOW, 2 * LANES), jnp.float32),
             jax.ShapeDtypeStruct((4, n), jnp.float32),
-            jax.ShapeDtypeStruct((n, cols), jnp.bfloat16),
-        ],
+            jax.ShapeDtypeStruct((WINDOW, cols), jnp.bfloat16),
+            jax.ShapeDtypeStruct((WINDOW + rim.shape[1] // LANES * RIM, LANES), jnp.bfloat16),
+            jax.ShapeDtypeStruct((n, own.shape[1] - cols), jnp.float32),
+        ],
+        scratch_shapes=[pltpu.VMEM((n, cols), jnp.bfloat16)],
         compiler_params=settings(8),
-        cost_estimate=cost(8),
+        cost_estimate=cost(6),
         name="attn",
-    )(sinks, x, sums, *parts)
+    )(sinks, x, sums, own, corner, rim)
 
 
 def conv_kernel(
-    sinks, place, x_ref, sum_ref, w0, w1, w2, w3, gain_ref, taps_ref, att_ref, log_ref, rows_ref, halo_ref,
-    out_hbm, log_out, out_ref, pad_ref, prev_x, sems,
+    x_ref, sum_ref, y_ref, z_ref, taps_ref, att_ref, log_ref,
+    out_hbm, log_hbm, first_ref, out_ref, pad_ref, sems, log_sem,
 ):
     n = x_ref.shape[1]
     width = 2 * LANES
     step = 256
-    parts = [w[:, w.shape[1] - 2 * width :] for w in (w0, w1, w2, w3)]
+    log_copy = pltpu.make_async_copy(log_ref, log_hbm, log_sem)
+    log_copy.start()
+    taps = taps_ref[...].astype(jnp.float32)
+    copies = []
+    for k, at in enumerate(range(0, n, step)):
+        acc = sum_ref[at : at + step, :] + dot(x_ref[1, at : at + step, :], y_ref[...])
+        acc = acc + dot(x_ref[2, at : at + step, :], z_ref[...])
+        rounded = acc.astype(jnp.bfloat16)
+        low = 0
+        if at == 0:
+            first_ref[...] = rounded[:WINDOW, :]
+            low = WINDOW
+        rounded = rounded.astype(jnp.float32)
+        pad_ref[at : at + step, :] = rounded[:, :width]
+        total = taps[0:1] * pad_ref[at + low - 2 : at + step - 2, :]
+        total = total + taps[1:2] * pad_ref[at + low - 1 : at + step - 1, :]
+        total = total + taps[2:3] * rounded[low:, :width]
+        gated = rounded[low:, width:] * total
+        summed = att_ref[at + low - WINDOW : at + step - WINDOW, :] + gated
+        out_ref[at + low : at + step, :] = summed.astype(jnp.bfloat16)
+        copies.append(
+            pltpu.make_async_copy(
+                out_ref.at[at + low : at + step, :], out_hbm.at[at + low : at + step, :], sems.at[k]
+            )
+        )
+        copies[-1].start()
+    for copy in copies:
+        copy.wait()
+    log_copy.wait()
+
+
+def convolution(x, sums, along_y, along_z, taps, att, logs):
+    n = x.shape[1]
+    return pl.pallas_call(
+        conv_kernel,
+        in_specs=[VMEM] * 7,
+        out_specs=[HBM, HBM, VMEM],
+        out_shape=[
+            jax.ShapeDtypeStruct((n, 2 * LANES), jnp.bfloat16),
+            jax.ShapeDtypeStruct((4, n), jnp.float32),
+            jax.ShapeDtypeStruct((WINDOW, 4 * LANES), jnp.bfloat16),
+        ],
+        scratch_shapes=[
+            pltpu.VMEM((n, 2 * LANES), jnp.bfloat16),
+            pltpu.VMEM((n, 2 * LANES), jnp.float32),
+            pltpu.SemaphoreType.DMA((n // 256,)),
+            pltpu.SemaphoreType.DMA(()),
+        ],
+        compiler_params=settings(8),
+        cost_estimate=cost(4),
+        name="conv",
+    )(x, sums, along_y, along_z, taps, att, logs)
+
+
+def head_kernel(
+    sinks, place, w0, w1, w2, w3, gain_ref, taps_ref, rows_ref, conv_ref, halo_ref, out_in, log_in,
+    out_hbm, log_hbm, out_ref, log_ref, pad_ref, prev_x, sem, log_sem,
+):
+    width = 2 * LANES
+    att, logs = attend_block(
+        rows_ref[:, LANES:],
+        halo_ref[:WINDOW, :],
+        rows_ref[:, :LANES],
+        [sinks[h] for h in range(4)],
+        place[2] > 0,
+    )
+    log_ref[...] = logs
+    log_copy = pltpu.make_async_copy(log_ref, log_hbm.at[:, :WINDOW], log_sem)
+    log_copy.start()
     rim = [
         halo_ref[WINDOW + k * RIM : WINDOW + (k + 1) * RIM, :]
         for k in range(gain_ref.shape[1] // LANES)
     ]
     norm_into(place, jnp.concatenate(rim, axis=1), gain_ref[...], column_sort(), prev_x)
-    acc = dot(prev_x[0], parts[0][:, :width])
+    parts = [w[:, w.shape[1] - 2 * width : w.shape[1] - width] for w in (w0, w1, w2, w3)]
+    acc = dot(prev_x[0], parts[0])
     for c in range(1, 4):
-        acc = acc + dot(prev_x[c], parts[c][:, :width])
+        acc = acc + dot(prev_x[c], parts[c])
     pad_ref[:8, :] = acc[8:16].astype(jnp.bfloat16).astype(jnp.float32)
-    att0, log0 = attend_block(
-        rows_ref[:WINDOW, LANES:],
-        halo_ref[:WINDOW, :],
-        rows_ref[:WINDOW, :LANES],
-        [sinks[h] for h in range(4)],
-        place[2] > 0,
-    )
-    log_out[...] = log_ref[...]
-    log_out[:, :WINDOW] = log0
     taps = taps_ref[...].astype(jnp.float32)
-    copies = []
-    for k, at in enumerate(range(0, n, step)):
-        acc = sum_ref[at : at + step, :] + dot(x_ref[1, at : at + step, :], parts[1])
-        for c in range(2, 4):
-            acc = acc + dot(x_ref[c, at : at + step, :], parts[c])
-        rounded = acc.astype(jnp.bfloat16).astype(jnp.float32)
-        pad_ref[8 + at : 8 + at + step, :] = rounded[:, :width]
-        total = taps[0:1] * pad_ref[6 + at : 6 + at + step, :]
-        total = total + taps[1:2] * pad_ref[7 + at : 7 + at + step, :]
-        total = total + taps[2:3] * rounded[:, :width]
-        gated = rounded[:, width:] * total
-        if at == 0:
-            first = jnp.concatenate([att0, att_ref[WINDOW:step, :]], axis=0)
-        else:
-            first = att_ref[at : at + step, :]
-        out_ref[at : at + step, :] = (first + gated).astype(jnp.bfloat16)
-        copies.append(
-            pltpu.make_async_copy(
-                out_ref.at[at : at + step, :], out_hbm.at[at : at + step, :], sems.at[k]
-            )
-        )
-        copies[-1].start()
-    for copy in copies:
-        copy.wait()
-
-
-def convolution(sinks, place, x, sums, parts, gain, taps, att, logs, rows, halo):
-    n = x.shape[1]
-    return pl.pallas_call(
-        conv_kernel,
-        in_specs=[SMEM] * 2 + [VMEM] * 12,
-        out_specs=[HBM, VMEM],
+    rounded = conv_ref[...].astype(jnp.float32)
+    pad_ref[8:, :] = rounded[:, :width]
+    total = taps[0:1] * pad_ref[6 : 6 + WINDOW, :]
+    total = total + taps[1:2] * pad_ref[7 : 7 + WINDOW, :]
+    total = total + taps[2:3] * rounded[:, :width]
+    out_ref[...] = (att + rounded[:, width:] * total).astype(jnp.bfloat16)
+    copy = pltpu.make_async_copy(out_ref, out_hbm.at[:WINDOW, :], sem)
+    copy.start()
+    copy.wait()
+    log_copy.wait()
+
+
+def head(sinks, place, parts, gain, taps, rows, conv_rows, halo, mixed, logs):
+    return pl.pallas_call(
+        head_kernel,
+        in_specs=[SMEM] * 2 + [VMEM] * 9 + [HBM] * 2,
+        out_specs=[HBM, HBM],
         out_shape=[
-            jax.ShapeDtypeStruct((n, 2 * LANES), jnp.bfloat16),
-            jax.ShapeDtypeStruct((4, n), jnp.float32),
-        ],
+            jax.ShapeDtypeStruct(mixed.shape, mixed.dtype),
+            jax.ShapeDtypeStruct(logs.shape, logs.dtype),
+        ],
+        input_output_aliases={11: 0, 12: 1},
         scratch_shapes=[
-            pltpu.VMEM((n, 2 * LANES), jnp.bfloat16),
-            pltpu.VMEM((n + 8, 2 * LANES), jnp.float32),
-            pltpu.VMEM((4, RIM, x.shape[2]), jnp.bfloat16),
-            pltpu.SemaphoreType.DMA((n // 256,)),
-        ],
-        compiler_params=settings(8),
-        cost_estimate=cost(6),
-        name="conv",
-    )(sinks, place, x, sums, *parts, gain, taps, att, logs, rows, halo)
+            pltpu.VMEM((WINDOW, 2 * LANES), jnp.bfloat16),
+            pltpu.VMEM((4, WINDOW), jnp.float32),
+            pltpu.VMEM((WINDOW + 8, 2 * LANES), jnp.float32),
+            pltpu.VMEM((4, RIM, parts[0].shape[0]), jnp.bfloat16),
+            pltpu.SemaphoreType.DMA(()),
+            pltpu.SemaphoreType.DMA(()),
+        ],
+        compiler_params=settings(6),
+        cost_estimate=cost(2),
+        name="head",
+    )(sinks, place, *parts, gain, taps, rows, conv_rows, halo, mixed, logs)
 
 
 def body(
@@ -376,13 +401,18 @@
     own_a, own_b = cut_columns(own, cut)
     parts_a = classes(own_a)
     parts_b = classes(own_b)
-    x, rim = norm_classes(place, pltpu.with_memory_space_constraint(tokens, pltpu.HBM), gain, 256)
-    sum_a, sum_b = early_sums(x, own, parts_a[1])
-    last = tail_rows(x, sum_a, parts_a[2:], rim)
+    near = pltpu.with_memory_space_constraint
+    x, rim = norm_classes(place, near(tokens, pltpu.HBM), near(gain, pltpu.HBM), 256)
+    sum_a = early_sums(x, own, parts_a[1], parts_a[2])
+    att, logs, rows, last, sum_b = attention(sink_logits, x, sum_a, own, corner, rim)
     halo = passed_along(last)
-    att, logs, rows = attention(sink_logits, x, sum_a, parts_a[2:])
+    mixed, logs, conv_rows = convolution(
+        x, sum_b, parts_b[1], parts_b[2], conv_taps, att, logs
+    )
     return tuple(
-        convolution(sink_logits, place, x, sum_b, parts_b, gain, conv_taps, att, logs, rows, halo)
+        head(
+            sink_logits, place, parts_b, gain, conv_taps, rows, conv_rows, halo, mixed, logs
+        )
     )
 
 

time: 90.9 us -> 95.5 us (1.051)
  the two profiles are of different devices: /device:TPU:70 before, /device:TPU:68 now
where the time goes in v6:
time: 95.5 us; the launch traced here: 95 us
  blocking collectives  43.8 us (46%)
  Pallas kernels  18.8 us (20%)
  starting transfers between devices  17.2 us (18%)
  waiting for transfers between devices  13.4 us (14%)
  local copies, waits for them, and re-layouts  0.96 us (1%)
    all_to_all x1, blocking collectives, layer(): own = lax.all_to_all(sent, ('zh', 'yh'), 0, 0)  43.8 us
    ppermute x5, starting transfers between devices, shift(): return lax.ppermute(value, SP, pairs)  14 us
    ppermute x5, waiting for transfers between devices, shift(): return lax.ppermute(value, SP, pairs)  8.83 us
    pallas_call x1, Pallas kernels, norm_classes(): pl.pallas_call(norm_kernel, grid_spec=pltpu.PrefetchScalarGridSpec(num_sc...  5.73 us
    pallas_call x1, Pallas kernels, attention(): pl.pallas_call(attn_kernel, in_specs=[SMEM] + [VMEM] * 5, out_specs=[VMEM...  4.78 us
    ppermute x1, waiting for transfers between devices, passed_along(): return lax.ppermute(value, SP, [(i, i + 1) for i in range(n - 1)])  4.6 us
    ppermute x1, starting transfers between devices, passed_along(): return lax.ppermute(value, SP, [(i, i + 1) for i in range(n - 1)])  3.16 us
    pallas_call x1, Pallas kernels, early_sums(): pl.pallas_call(early_kernel, in_specs=[VMEM] * 4, out_specs=VMEM, out_sha...  2.79 us
  transfers between devices with their start and end apart: 6, of which 3 were waited for; matrix products, arithmetic and copies ran while one was open for 0% of the time, Pallas kernels for 17%

profile of v6, /device:TPU:68, one launch (start us, length us, event | category | flops | bytes accessed | tf_op | source)
XLA Modules:
  0.0 95.0 jit_solution(7877408498312435779)
XLA Ops:
  0.6 0.9 concatenate.3
  1.5 0.1 broadcast_in_dim.2
  1.6 43.8 %all_to_all.5 = bf16[16,32,896]{2,1,0:T(8,128)(2,1)S(1)} all-to-all(bf16[16,32,896]{2,1,0:T(8,128)(2,1)S(1)} %broadcast_in_dim.2), channel_id=1, replica_groups=mesh['zh'=4,'zl'=2,'yh'=4,'yl'=2,'fs'=4,'tp'=2] {'zh','yh'}, dimensions={0} | all-to-all | bytes 1835008 | tf_op jit(solution)/shard_map/all_to_all | solution.py:391
  45.4 1.9 %collective-permute-start.2 = (bf16[512,896]{1,0:T(8,128)(2,1)S(1)}, bf16[512,896]{1,0:T(8,128)(2,1)S(1)}, u32[]{:S(2)}, u32[]{:S(2)}) collective-permute-start(bf16[512,896]{1,0:T(8,128)(2,1)S(1)} %bitcast.5), channel_id=1, source_target_pairs={{0,504},{8,448},{16,456},{24,464},{32,472},{40,480},{48,488},{56,4... | collective-permute-start | bytes 2752520 | tf_op jit(solution)/shard_map/ppermute | solution.py:28
  47.3 1.0 %cut.1 = (bf16[512,384]{1,0:T(8,128)(2,1)}, bf16[512,512]{1,0:T(8,128)(2,1)}) custom-call(bf16[512,896]{1,0:T(8,128)(2,1)S(1)} %bitcast.6), custom_call_target="tpu_custom_call" | custom-call | flops 3900000 | bytes 1048576 | tf_op jit(solution)/shard_map/cut/pallas_call | solution.py:157
  48.3 4.0 %collective-permute-start = (bf16[512,512]{1,0:T(8,128)(2,1)}, bf16[512,512]{1,0:T(8,128)(2,1)S(1)}, u32[]{:S(2)}, u32[]{:S(2)}) collective-permute-start(bf16[512,512]{1,0:T(8,128)(2,1)} %get-tuple-element.14), channel_id=1, source_target_pairs={{0,8},{8,16},{16,24},{24,32},{32,40},{40,48},{48,56},{56,0},{64,72... | collective-permute-start | bytes 1572872 | tf_op jit(solution)/shard_map/ppermute | solution.py:28
  52.3 3.3 %collective-permute-start.1 = (bf16[512,512]{1,0:T(8,128)(2,1)}, bf16[512,512]{1,0:T(8,128)(2,1)S(1)}, u32[]{:S(2)}, u32[]{:S(2)}) collective-permute-start(bf16[512,512]{1,0:T(8,128)(2,1)} %get-tuple-element.14), channel_id=1, source_target_pairs={{0,64},{8,72},{16,80},{24,88},{32,96},{40,104},{48,112},{56,120},{... | collective-permute-start | bytes 1572872 | tf_op jit(solution)/shard_map/ppermute | solution.py:28
  55.6 1.9 %collective-permute-start.3 = (bf16[512,384]{1,0:T(8,128)(2,1)}, bf16[512,384]{1,0:T(8,128)(2,1)S(1)}, u32[]{:S(2)}, u32[]{:S(2)}) collective-permute-start(bf16[512,384]{1,0:T(8,128)(2,1)} %get-tuple-element.16), channel_id=1, source_target_pairs={{0,8},{8,16},{16,24},{24,32},{32,40},{40,48},{48,56},{56,0},{64,72... | collective-permute-start | bytes 1179656 | tf_op jit(solution)/shard_map/ppermute | solution.py:28
  57.5 2.9 %collective-permute-start.4 = (bf16[512,384]{1,0:T(8,128)(2,1)}, bf16[512,384]{1,0:T(8,128)(2,1)}, u32[]{:S(2)}, u32[]{:S(2)}) collective-permute-start(bf16[512,384]{1,0:T(8,128)(2,1)} %get-tuple-element.16), channel_id=1, source_target_pairs={{0,64},{8,72},{16,80},{24,88},{32,96},{40,104},{48,112},{56,120},{... | collective-permute-start | bytes 1179656 | tf_op jit(solution)/shard_map/ppermute | solution.py:28
  60.4 0.1 pad_add_fusion.place
  60.5 5.7 %norm.1 = (bf16[4,1024,512]{2,1,0:T(8,128)(2,1)S(1)}, bf16[16,2048]{1,0:T(8,128)(2,1)S(1)}) custom-call(s32[3]{0:T(128)S(1)} %pad_add_fusion.place, bf16[1024,2048]{1,0:T(8,128)(2,1)} %tok_ref.1, f32[1,2048]{1,0:T(1,128)} %bitcast.10), custom_call_target="tpu_custom_call" | custom-call | flops 19500000 | bytes 1048576 | tf_op jit(solution)/shard_map/norm/pallas_call | solution.py:79
  66.3 0.0 copy-start.2
  66.3 7.7 %collective-permute-done.3.y_ref = bf16[512,384]{1,0:T(8,128)(2,1)S(1)} collective-permute-done((bf16[512,384]{1,0:T(8,128)(2,1)}, bf16[512,384]{1,0:T(8,128)(2,1)S(1)}, u32[]{:S(2)}, u32[]{:S(2)}) %collective-permute-start.3) | collective-permute-done | bytes 393248 | tf_op jit(solution)/shard_map/ppermute | solution.py:28
  74.0 1.1 %collective-permute-done.4.z_ref = bf16[512,384]{1,0:T(8,128)(2,1)} collective-permute-done((bf16[512,384]{1,0:T(8,128)(2,1)}, bf16[512,384]{1,0:T(8,128)(2,1)}, u32[]{:S(2)}, u32[]{:S(2)}) %collective-permute-start.4) | collective-permute-done | bytes 393248 | tf_op jit(solution)/shard_map/ppermute | solution.py:28
  75.1 2.8 %early.1.sum_ref = f32[1024,384]{1,0:T(8,128)S(1)} custom-call(bf16[4,1024,512]{2,1,0:T(8,128)(2,1)S(1)} %get-tuple-element.15.x_ref, bf16[512,896]{1,0:T(8,128)(2,1)S(1)} %bitcast.7, bf16[512,384]{1,0:T(8,128)(2,1)S(1)} %collective-permute-done.3.y_ref, bf16[512,384]{1,0:T(8,128)(2,1)} %collective-permute-done.4.z_ref), custom_call_target="tpu_custom_call" | custom-call | flops 7800000 | bytes 1048576 | tf_op jit(solution)/shard_map/early/pallas_call | solution.py:184
  77.9 0.0 copy-start.1
  77.9 0.0 collective-permute-done.2.corner_ref.w3
  77.9 0.0 copy-done.2
  77.9 4.8 %attn.1 = (f32[896,256]{1,0:T(8,128)S(1)}, f32[4,1024]{1,0:T(4,128)S(1)}, bf16[128,384]{1,0:T(8,128)(2,1)S(1)}, bf16[384,128]{1,0:T(8,128)(2,1)S(1)}, f32[1024,512]{1,0:T(8,128)S(1)}) custom-call(f32[4]{0:T(128)S(1)} %copy-done.2, bf16[4,1024,512]{2,1,0:T(8,128)(2,1)S(1)} %get-tuple-element.15.x_ref, f32[1024,384]{1,0:T(8,128)S(1)} %early.1.sum_ref, ...), custom_call_target="tpu_custom_call" | custom-call | flops 23400000 | bytes 1048576 | tf_op jit(solution)/shard_map/attn/pallas_call | solution.py:232
  82.7 0.0 copy-start
  82.7 3.2 %collective-permute-start.5 = (bf16[384,128]{1,0:T(8,128)(2,1)S(1)}, bf16[384,128]{1,0:T(8,128)(2,1)S(1)}, u32[]{:S(2)}, u32[]{:S(2)}) collective-permute-start(bf16[384,128]{1,0:T(8,128)(2,1)S(1)} %get-tuple-element.23), channel_id=1, source_target_pairs={{0,8},{8,16},{16,24},{24,32},{32,40},{40,48},{48,56},{56,64},{64,7... | collective-permute-start | bytes 294920 | tf_op jit(solution)/shard_map/ppermute | solution.py:33
  85.9 0.0 collective-permute-done.y_ref.w1
  85.9 0.0 collective-permute-done.1.z_ref.w2
  85.9 0.0 copy-done.1
  85.9 2.2 %conv.1 = (bf16[1024,256]{1,0:T(8,128)(2,1)}, f32[4,1024]{1,0:T(4,128)}, bf16[128,512]{1,0:T(8,128)(2,1)S(1)}) custom-call(bf16[4,1024,512]{2,1,0:T(8,128)(2,1)S(1)} %get-tuple-element.15.x_ref, f32[1024,512]{1,0:T(8,128)S(1)} %get-tuple-element.19.sum_ref, bf16[512,512]{1,0:T(8,128)(2,1)S(1)} %collective-permute-done.y_ref.w1, ...), custom_call_target="tpu_custom_call" | custom-call | flops 15600000 | bytes 1048576 | tf_op jit(solution)/shard_map/conv/pallas_call | solution.py:290
  88.1 4.6 %collective-permute-done.5.halo_ref = bf16[384,128]{1,0:T(8,128)(2,1)S(1)} collective-permute-done((bf16[384,128]{1,0:T(8,128)(2,1)S(1)}, bf16[384,128]{1,0:T(8,128)(2,1)S(1)}, u32[]{:S(2)}, u32[]{:S(2)}) %collective-permute-start.5) | collective-permute-done | bytes 98336 | tf_op jit(solution)/shard_map/ppermute | solution.py:33
  92.7 0.0 copy-done
  92.7 2.3 %head.1 = (bf16[1024,256]{1,0:T(8,128)(2,1)}, f32[4,1024]{1,0:T(4,128)}) custom-call(f32[4]{0:T(128)S(1)} %copy-done.2, s32[3]{0:T(128)S(1)} %pad_add_fusion.place, bf16[512,896]{1,0:T(8,128)(2,1)S(1)} %bitcast.9, bf16[512,512]{1,0:T(8,128)(2,1)S(1)} %collective-permute-done.y_ref.w1, ...), custom_call_target="tpu_custom_call", output_to_operand_aliasing={{0}: (11, {}), {1}: (12, {})} | custom-call | flops 7800000 | bytes 1048576 | tf_op jit(solution)/shard_map/head/pallas_call | solution.py:350
Async XLA Ops:
  45.4 32.5 %collective-permute-start.2 = (bf16[512,896]{1,0:T(8,128)(2,1)S(1)}, bf16[512,896]{1,0:T(8,128)(2,1)S(1)}, u32[]{:S(2)}, u32[]{:S(2)}) collective-permute-start(bf16[512,896]{1,0:T(8,128)(2,1)S(1)} %bitcast.5), channel_id=1, source_target_pairs={{0,504},{8,448},{16,456},{24,464},{32,472},{40,480},{48,488},{56,4... | collective-permute-start | bytes 2752520 | tf_op jit(solution)/shard_map/ppermute | solution.py:28
  48.3 37.6 %collective-permute-start = (bf16[512,512]{1,0:T(8,128)(2,1)}, bf16[512,512]{1,0:T(8,128)(2,1)S(1)}, u32[]{:S(2)}, u32[]{:S(2)}) collective-permute-start(bf16[512,512]{1,0:T(8,128)(2,1)} %get-tuple-element.14), channel_id=1, source_target_pairs={{0,8},{8,16},{16,24},{24,32},{32,40},{40,48},{48,56},{56,0},{64,72... | collective-permute-start | bytes 1572872 | tf_op jit(solution)/shard_map/ppermute | solution.py:28
  52.3 33.6 %collective-permute-start.1 = (bf16[512,512]{1,0:T(8,128)(2,1)}, bf16[512,512]{1,0:T(8,128)(2,1)S(1)}, u32[]{:S(2)}, u32[]{:S(2)}) collective-permute-start(bf16[512,512]{1,0:T(8,128)(2,1)} %get-tuple-element.14), channel_id=1, source_target_pairs={{0,64},{8,72},{16,80},{24,88},{32,96},{40,104},{48,112},{56,120},{... | collective-permute-start | bytes 1572872 | tf_op jit(solution)/shard_map/ppermute | solution.py:28
  55.6 18.4 %collective-permute-start.3 = (bf16[512,384]{1,0:T(8,128)(2,1)}, bf16[512,384]{1,0:T(8,128)(2,1)S(1)}, u32[]{:S(2)}, u32[]{:S(2)}) collective-permute-start(bf16[512,384]{1,0:T(8,128)(2,1)} %get-tuple-element.16), channel_id=1, source_target_pairs={{0,8},{8,16},{16,24},{24,32},{32,40},{40,48},{48,56},{56,0},{64,72... | collective-permute-start | bytes 1179656 | tf_op jit(solution)/shard_map/ppermute | solution.py:28
  57.5 17.6 %collective-permute-start.4 = (bf16[512,384]{1,0:T(8,128)(2,1)}, bf16[512,384]{1,0:T(8,128)(2,1)}, u32[]{:S(2)}, u32[]{:S(2)}) collective-permute-start(bf16[512,384]{1,0:T(8,128)(2,1)} %get-tuple-element.16), channel_id=1, source_target_pairs={{0,64},{8,72},{16,80},{24,88},{32,96},{40,104},{48,112},{56,120},{... | collective-permute-start | bytes 1179656 | tf_op jit(solution)/shard_map/ppermute | solution.py:28
  66.3 11.6 %copy-start.2 = (f32[4]{0:T(128)S(1)}, f32[4]{0:T(128)}, u32[]{:S(2)}) copy-start(f32[4]{0:T(128)} %sinks.3) | copy-start | bytes 52
  77.9 8.0 %copy-start.1 = (bf16[3,256]{1,0:T(4,128)(2,1)S(1)}, bf16[3,256]{1,0:T(4,128)(2,1)}, u32[]{:S(2)}) copy-start(bf16[3,256]{1,0:T(4,128)(2,1)} %taps_ref.3) | copy-start | bytes 4612
  82.7 10.0 %copy-start = (f32[2048]{0:T(1024)S(1)}, f32[2048]{0:T(1024)}, u32[]{:S(2)}) copy-start(f32[2048]{0:T(1024)} %param.10) | copy-start | bytes 24580
  82.7 10.0 %collective-permute-start.5 = (bf16[384,128]{1,0:T(8,128)(2,1)S(1)}, bf16[384,128]{1,0:T(8,128)(2,1)S(1)}, u32[]{:S(2)}, u32[]{:S(2)}) collective-permute-start(bf16[384,128]{1,0:T(8,128)(2,1)S(1)} %get-tuple-element.23), channel_id=1, source_target_pairs={{0,8},{8,16},{16,24},{24,32},{32,40},{40,48},{48,56},{56,64},{64,7... | collective-permute-start | bytes 294920 | tf_op jit(solution)/shard_map/ppermute | solution.py:33

commit v7 on v5

--- a/solution.py
+++ b/solution.py
@@ -100,19 +100,16 @@
     )(place, rows, gain)
 
 
-def attend_block(q, kv_prev, kv_cur, sinks, has_prev):
-    lane = lax.broadcasted_iota(jnp.int32, (WINDOW, LANES), 1)
-    left = lane < HEAD_DIM
-
-    def split(kv):
-        swapped = pltpu.roll(kv.astype(jnp.float32), HEAD_DIM, 1).astype(jnp.bfloat16)
-        zero = jnp.zeros_like(kv)
-        return jnp.where(left, kv, zero), jnp.where(left, zero, swapped)
-
+def key_copies(kv):
+    left = lax.broadcasted_iota(jnp.int32, kv.shape, 1) < HEAD_DIM
+    swapped = pltpu.roll(kv.astype(jnp.float32), HEAD_DIM, 1).astype(kv.dtype)
+    zero = jnp.zeros_like(kv)
+    return jnp.where(left, kv, zero), jnp.where(left, zero, swapped)
+
+
+def attend_block(q, keys_lo, keys_hi, values, sinks, has_prev):
     q = q * jnp.asarray(HEAD_DIM ** (-0.5), q.dtype)
-    prev_lo, prev_hi = split(kv_prev)
-    cur_lo, cur_hi = split(kv_cur)
-    keys = jnp.concatenate([prev_lo, cur_lo, prev_hi, cur_hi], axis=0)
+    keys = jnp.concatenate([keys_lo, keys_hi], axis=0)
     key_idx = lax.broadcasted_iota(jnp.int32, (WINDOW, WINDOW), 0)
     query_idx = lax.broadcasted_iota(jnp.int32, (WINDOW, WINDOW), 1)
     from_prev = key_idx > query_idx
@@ -137,7 +134,6 @@
                     [jnp.where(from_prev, share, zero), jnp.where(from_prev, zero, share)], axis=0
                 ).astype(jnp.bfloat16)
             )
-    values = jnp.concatenate([kv_prev, kv_cur], axis=0)
     outs = []
     for pair in range(2):
         got = dot(values, jnp.concatenate(weights[pair * 2 : pair * 2 + 2], axis=1), ((0,), (0,)))
@@ -168,14 +164,12 @@
     )(own)
 
 
-def early_kernel(x_ref, own_ref, y_ref, sum_a, sum_b):
+def early_kernel(x_ref, own_ref, y_ref, sum_ref):
     n = x_ref.shape[1]
-    cols = sum_a.shape[1]
+    cols = sum_ref.shape[1]
     step = 256
     for at in range(0, n, step):
-        mine = x_ref[0, at : at + step, :]
-        sum_b[at : at + step, :] = dot(mine, own_ref[:, cols:])
-        sum_a[at : at + step, :] = dot(mine, own_ref[:, :cols]) + dot(
+        sum_ref[at : at + step, :] = dot(x_ref[0, at : at + step, :], own_ref[:, :cols]) + dot(
             x_ref[1, at : at + step, :], y_ref[...]
         )
 
@@ -186,11 +180,8 @@
     return pl.pallas_call(
         early_kernel,
         in_specs=[VMEM] * 3,
-        out_specs=[VMEM] * 2,
-        out_shape=[
-            jax.ShapeDtypeStruct((n, cols), jnp.float32),
-            jax.ShapeDtypeStruct((n, own.shape[1] - cols), jnp.float32),
-        ],
+        out_specs=VMEM,
+        out_shape=jax.ShapeDtypeStruct((n, cols), jnp.float32),
         compiler_params=settings(4),
         cost_estimate=cost(2),
         name="early",
@@ -227,14 +218,16 @@
     )(x, sums, *parts, rim)
 
 
-def attn_kernel(sinks, x_ref, sum_ref, w2, w3, att_ref, log_ref, rows_ref):
+def attn_kernel(sinks, x_ref, sum_ref, w2, w3, att_ref, log_ref, rows_ref, lo_ref, hi_ref):
     n = x_ref.shape[1]
     step = 256
     cols = rows_ref.shape[1]
     for at in range(0, n, step):
         acc = sum_ref[at : at + step, :] + dot(x_ref[2, at : at + step, :], w2[...])
         acc = acc + dot(x_ref[3, at : at + step, :], w3[:, :cols])
-        rows_ref[at : at + step, :] = acc.astype(jnp.bfloat16)
+        rows = acc.astype(jnp.bfloat16)
+        rows_ref[at : at + step, :] = rows
+        lo_ref[at : at + step, :], hi_ref[at : at + step, :] = key_copies(rows[:, :LANES])
     heads = [sinks[h] for h in range(4)]
     att_ref[:WINDOW, :] = jnp.zeros((WINDOW, 2 * LANES), jnp.float32)
     log_ref[:, :WINDOW] = jnp.zeros((4, WINDOW), jnp.float32)
@@ -243,8 +236,9 @@
         here, before = b * WINDOW, (b - 1) * WINDOW
         att, logs = attend_block(
             rows_ref[here : here + WINDOW, LANES:],
-            rows_ref[before : before + WINDOW, :LANES],
-            rows_ref[here : here + WINDOW, :LANES],
+            lo_ref[before : here + WINDOW, :],
+            hi_ref[before : here + WINDOW, :],
+            rows_ref[before : here + WINDOW, :LANES],
             heads,
             None,
         )
@@ -264,6 +258,7 @@
             jax.ShapeDtypeStruct((4, n), jnp.float32),
             jax.ShapeDtypeStruct((n, cols), jnp.bfloat16),
         ],
+        scratch_shapes=[pltpu.VMEM((n, LANES), jnp.bfloat16)] * 2,
         compiler_params=settings(8),
         cost_estimate=cost(8),
         name="attn",
@@ -271,7 +266,7 @@
 
 
 def conv_kernel(
-    sinks, place, x_ref, sum_ref, w0, w1, w2, w3, gain_ref, taps_ref, att_ref, log_ref, rows_ref, halo_ref,
+    sinks, place, x_ref, w0, w1, w2, w3, gain_ref, taps_ref, att_ref, log_ref, rows_ref, halo_ref,
     out_hbm, log_out, out_ref, pad_ref, prev_x, sems,
 ):
     n = x_ref.shape[1]
@@ -287,10 +282,11 @@
     for c in range(1, 4):
         acc = acc + dot(prev_x[c], parts[c][:, :width])
     pad_ref[:8, :] = acc[8:16].astype(jnp.bfloat16).astype(jnp.float32)
+    span = jnp.concatenate([halo_ref[:WINDOW, :], rows_ref[:WINDOW, :LANES]], axis=0)
     att0, log0 = attend_block(
         rows_ref[:WINDOW, LANES:],
-        halo_ref[:WINDOW, :],
-        rows_ref[:WINDOW, :LANES],
+        *key_copies(span),
+        span,
         [sinks[h] for h in range(4)],
         place[2] > 0,
     )
@@ -299,8 +295,8 @@
     taps = taps_ref[...].astype(jnp.float32)
     copies = []
     for k, at in enumerate(range(0, n, step)):
-        acc = sum_ref[at : at + step, :] + dot(x_ref[1, at : at + step, :], parts[1])
-        for c in range(2, 4):
+        acc = dot(x_ref[0, at : at + step, :], parts[0])
+        for c in range(1, 4):
             acc = acc + dot(x_ref[c, at : at + step, :], parts[c])
         rounded = acc.astype(jnp.bfloat16).astype(jnp.float32)
         pad_ref[8 + at : 8 + at + step, :] = rounded[:, :width]
@@ -323,11 +319,11 @@
         copy.wait()
 
 
-def convolution(sinks, place, x, sums, parts, gain, taps, att, logs, rows, halo):
+def convolution(sinks, place, x, parts, gain, taps, att, logs, rows, halo):
     n = x.shape[1]
     return pl.pallas_call(
         conv_kernel,
-        in_specs=[SMEM] * 2 + [VMEM] * 12,
+        in_specs=[SMEM] * 2 + [VMEM] * 11,
         out_specs=[HBM, VMEM],
         out_shape=[
             jax.ShapeDtypeStruct((n, 2 * LANES), jnp.bfloat16),
@@ -342,7 +338,7 @@
         compiler_params=settings(8),
         cost_estimate=cost(6),
         name="conv",
-    )(sinks, place, x, sums, *parts, gain, taps, att, logs, rows, halo)
+    )(sinks, place, x, *parts, gain, taps, att, logs, rows, halo)
 
 
 def body(
@@ -376,13 +372,16 @@
     own_a, own_b = cut_columns(own, cut)
     parts_a = classes(own_a)
     parts_b = classes(own_b)
-    x, rim = norm_classes(place, pltpu.with_memory_space_constraint(tokens, pltpu.HBM), gain, 256)
-    sum_a, sum_b = early_sums(x, own, parts_a[1])
+    near = pltpu.with_memory_space_constraint
+    x, rim = norm_classes(place, near(tokens, pltpu.HBM), near(gain, pltpu.HBM), 256)
+    sum_a = early_sums(x, own, parts_a[1])
     last = tail_rows(x, sum_a, parts_a[2:], rim)
     halo = passed_along(last)
     att, logs, rows = attention(sink_logits, x, sum_a, parts_a[2:])
     return tuple(
-        convolution(sink_logits, place, x, sum_b, parts_b, gain, conv_taps, att, logs, rows, halo)
+        convolution(
+            sink_logits, place, x, parts_b, gain, conv_taps, att, logs, rows, halo
+        )
     )
 
 

time: 90.9 us -> 90.9 us (level)
  the two profiles are of different devices: /device:TPU:70 before, /device:TPU:40 now
where the time goes in v7:
time: 90.9 us; the launch traced here: 90.4 us
  blocking collectives  40.3 us (44%)
  starting transfers between devices  24.4 us (27%)
  Pallas kernels  18.3 us (20%)
  waiting for transfers between devices  5.53 us (6%)
  local copies, waits for them, and re-layouts  0.96 us (1%)
    all_to_all x1, blocking collectives, layer(): own = lax.all_to_all(sent, ('zh', 'yh'), 0, 0)  40.3 us
    ppermute x5, starting transfers between devices, shift(): return lax.ppermute(value, SP, pairs)  19.1 us
    pallas_call x1, Pallas kernels, norm_classes(): pl.pallas_call(norm_kernel, grid_spec=pltpu.PrefetchScalarGridSpec(num_sc...  5.73 us
    ppermute x5, waiting for transfers between devices, shift(): return lax.ppermute(value, SP, pairs)  5.53 us
    ppermute x1, starting transfers between devices, passed_along(): return lax.ppermute(value, SP, [(i, i + 1) for i in range(n - 1)])  5.32 us
    pallas_call x1, Pallas kernels, convolution(): pl.pallas_call(conv_kernel, in_specs=[SMEM] * 2 + [VMEM] * 11, out_specs=...  4.98 us
    pallas_call x1, Pallas kernels, attention(): pl.pallas_call(attn_kernel, in_specs=[SMEM] + [VMEM] * 4, out_specs=[VMEM...  4.12 us
    pallas_call x1, Pallas kernels, early_sums(): pl.pallas_call(early_kernel, in_specs=[VMEM] * 3, out_specs=VMEM, out_sha...  2.27 us
  transfers between devices with their start and end apart: 6, of which 2 were waited for; matrix products, arithmetic and copies ran while one was open for 0% of the time, Pallas kernels for 15%

profile of v7, /device:TPU:40, one launch (start us, length us, event | category | flops | bytes accessed | tf_op | source)
XLA Modules:
  0.0 90.4 jit_solution(15745020501342900124)
XLA Ops:
  0.6 0.9 concatenate.3
  1.5 0.1 broadcast_in_dim.2
  1.6 40.3 %all_to_all.5 = bf16[16,32,896]{2,1,0:T(8,128)(2,1)S(1)} all-to-all(bf16[16,32,896]{2,1,0:T(8,128)(2,1)S(1)} %broadcast_in_dim.2), channel_id=1, replica_groups=mesh['zh'=4,'zl'=2,'yh'=4,'yl'=2,'fs'=4,'tp'=2] {'zh','yh'}, dimensions={0} | all-to-all | bytes 1835008 | tf_op jit(solution)/shard_map/all_to_all | solution.py:362
  41.9 5.5 %collective-permute-start.2 = (bf16[512,896]{1,0:T(8,128)(2,1)S(1)}, bf16[512,896]{1,0:T(8,128)(2,1)S(1)}, u32[]{:S(2)}, u32[]{:S(2)}) collective-permute-start(bf16[512,896]{1,0:T(8,128)(2,1)S(1)} %bitcast.5), channel_id=1, source_target_pairs={{0,504},{8,448},{16,456},{24,464},{32,472},{40,480},{48,488},{56,4... | collective-permute-start | bytes 2752520 | tf_op jit(solution)/shard_map/ppermute | solution.py:28
  47.4 1.0 %cut.1 = (bf16[512,384]{1,0:T(8,128)(2,1)}, bf16[512,512]{1,0:T(8,128)(2,1)}) custom-call(bf16[512,896]{1,0:T(8,128)(2,1)S(1)} %bitcast.6), custom_call_target="tpu_custom_call" | custom-call | flops 3900000 | bytes 1048576 | tf_op jit(solution)/shard_map/cut/pallas_call | solution.py:153
  48.4 3.4 %collective-permute-start = (bf16[512,512]{1,0:T(8,128)(2,1)}, bf16[512,512]{1,0:T(8,128)(2,1)S(1)}, u32[]{:S(2)}, u32[]{:S(2)}) collective-permute-start(bf16[512,512]{1,0:T(8,128)(2,1)} %get-tuple-element.10), channel_id=1, source_target_pairs={{0,8},{8,16},{16,24},{24,32},{32,40},{40,48},{48,56},{56,0},{64,72... | collective-permute-start | bytes 1572872 | tf_op jit(solution)/shard_map/ppermute | solution.py:28
  51.9 2.8 %collective-permute-start.1 = (bf16[512,512]{1,0:T(8,128)(2,1)}, bf16[512,512]{1,0:T(8,128)(2,1)S(1)}, u32[]{:S(2)}, u32[]{:S(2)}) collective-permute-start(bf16[512,512]{1,0:T(8,128)(2,1)} %get-tuple-element.10), channel_id=1, source_target_pairs={{0,64},{8,72},{16,80},{24,88},{32,96},{40,104},{48,112},{56,120},{... | collective-permute-start | bytes 1572872 | tf_op jit(solution)/shard_map/ppermute | solution.py:28
  54.7 4.5 %collective-permute-start.3 = (bf16[512,384]{1,0:T(8,128)(2,1)}, bf16[512,384]{1,0:T(8,128)(2,1)}, u32[]{:S(2)}, u32[]{:S(2)}) collective-permute-start(bf16[512,384]{1,0:T(8,128)(2,1)} %get-tuple-element.11), channel_id=1, source_target_pairs={{0,8},{8,16},{16,24},{24,32},{32,40},{40,48},{48,56},{56,0},{64,72... | collective-permute-start | bytes 1179656 | tf_op jit(solution)/shard_map/ppermute | solution.py:28
  59.2 2.8 %collective-permute-start.4 = (bf16[512,384]{1,0:T(8,128)(2,1)}, bf16[512,384]{1,0:T(8,128)(2,1)S(1)}, u32[]{:S(2)}, u32[]{:S(2)}) collective-permute-start(bf16[512,384]{1,0:T(8,128)(2,1)} %get-tuple-element.11), channel_id=1, source_target_pairs={{0,64},{8,72},{16,80},{24,88},{32,96},{40,104},{48,112},{56,120},{... | collective-permute-start | bytes 1179656 | tf_op jit(solution)/shard_map/ppermute | solution.py:28
  62.0 0.1 pad_add_fusion.place
  62.1 5.7 %norm.1 = (bf16[4,1024,512]{2,1,0:T(8,128)(2,1)S(1)}, bf16[16,2048]{1,0:T(8,128)(2,1)S(1)}) custom-call(s32[3]{0:T(128)S(1)} %pad_add_fusion.place, bf16[1024,2048]{1,0:T(8,128)(2,1)} %tok_ref.1, f32[1,2048]{1,0:T(1,128)} %bitcast.9), custom_call_target="tpu_custom_call" | custom-call | flops 19500000 | bytes 1048576 | tf_op jit(solution)/shard_map/norm/pallas_call | solution.py:79
  67.8 3.9 %collective-permute-done.3.y_ref = bf16[512,384]{1,0:T(8,128)(2,1)} collective-permute-done((bf16[512,384]{1,0:T(8,128)(2,1)}, bf16[512,384]{1,0:T(8,128)(2,1)}, u32[]{:S(2)}, u32[]{:S(2)}) %collective-permute-start.3) | collective-permute-done | bytes 393248 | tf_op jit(solution)/shard_map/ppermute | solution.py:28
  71.7 2.3 %early.1.sum_ref = f32[1024,384]{1,0:T(8,128)S(1)} custom-call(bf16[4,1024,512]{2,1,0:T(8,128)(2,1)S(1)} %get-tuple-element.9.x_ref, bf16[512,896]{1,0:T(8,128)(2,1)S(1)} %bitcast.7, bf16[512,384]{1,0:T(8,128)(2,1)} %collective-permute-done.3.y_ref), custom_call_target="tpu_custom_call" | custom-call | flops 7800000 | bytes 1048576 | tf_op jit(solution)/shard_map/early/pallas_call | solution.py:180
  74.0 0.0 copy-start.2
  74.0 1.6 %collective-permute-done.4.w2 = bf16[512,384]{1,0:T(8,128)(2,1)S(1)} collective-permute-done((bf16[512,384]{1,0:T(8,128)(2,1)}, bf16[512,384]{1,0:T(8,128)(2,1)S(1)}, u32[]{:S(2)}, u32[]{:S(2)}) %collective-permute-start.4) | collective-permute-done | bytes 393248 | tf_op jit(solution)/shard_map/ppermute | solution.py:28
  75.6 0.0 collective-permute-done.2.w3
  75.6 0.2 tail.1
  75.9 0.0 copy-start
  75.9 0.0 copy-start.1
  75.9 5.3 %collective-permute-start.5 = (bf16[384,128]{1,0:T(8,128)(2,1)S(1)}, bf16[384,128]{1,0:T(8,128)(2,1)S(1)}, u32[]{:S(2)}, u32[]{:S(2)}) collective-permute-start(bf16[384,128]{1,0:T(8,128)(2,1)S(1)} %tail.1), channel_id=1, source_target_pairs={{0,8},{8,16},{16,24},{24,32},{32,40},{40,48},{48,56},{56,64},{64,7... | collective-permute-start | bytes 294920 | tf_op jit(solution)/shard_map/ppermute | solution.py:33
  81.2 0.0 copy-done.2
  81.2 4.1 %attn.1 = (f32[1024,256]{1,0:T(8,128)S(1)}, f32[4,1024]{1,0:T(4,128)S(1)}, bf16[1024,384]{1,0:T(8,128)(2,1)S(1)}) custom-call(f32[4]{0:T(128)S(1)} %copy-done.2, bf16[4,1024,512]{2,1,0:T(8,128)(2,1)S(1)} %get-tuple-element.9.x_ref, f32[1024,384]{1,0:T(8,128)S(1)} %early.1.sum_ref, bf16[512,384]{1,0:T(8,128)(2,1)S(1)} %collective-permute-done.4.w2, ...), custom_call_target="tpu_custom_call" | custom-call | flops 31200000 | bytes 1048576 | tf_op jit(solution)/shard_map/attn/pallas_call | solution.py:252
  85.4 0.0 collective-permute-done.w1
  85.4 0.0 collective-permute-done.1.w2
  85.4 0.0 collective-permute-done.5.halo_ref
  85.4 0.0 copy-done
  85.4 0.0 copy-done.1
  85.4 5.0 %conv.1 = (bf16[1024,256]{1,0:T(8,128)(2,1)}, f32[4,1024]{1,0:T(4,128)}) custom-call(f32[4]{0:T(128)S(1)} %copy-done.2, s32[3]{0:T(128)S(1)} %pad_add_fusion.place, bf16[4,1024,512]{2,1,0:T(8,128)(2,1)S(1)} %get-tuple-element.9.x_ref, bf16[512,896]{1,0:T(8,128)(2,1)S(1)} %bitcast.8, bf16[512,512]{1,0:T(8,128)(2,1)S(1)} %collective-permute-done.w1, ...), custom_call_target="tpu_custom_call" | custom-call | flops 23400000 | bytes 1048576 | tf_op jit(solution)/shard_map/conv/pallas_call | solution.py:324
Async XLA Ops:
  41.9 33.7 %collective-permute-start.2 = (bf16[512,896]{1,0:T(8,128)(2,1)S(1)}, bf16[512,896]{1,0:T(8,128)(2,1)S(1)}, u32[]{:S(2)}, u32[]{:S(2)}) collective-permute-start(bf16[512,896]{1,0:T(8,128)(2,1)S(1)} %bitcast.5), channel_id=1, source_target_pairs={{0,504},{8,448},{16,456},{24,464},{32,472},{40,480},{48,488},{56,4... | collective-permute-start | bytes 2752520 | tf_op jit(solution)/shard_map/ppermute | solution.py:28
  48.4 37.0 %collective-permute-start = (bf16[512,512]{1,0:T(8,128)(2,1)}, bf16[512,512]{1,0:T(8,128)(2,1)S(1)}, u32[]{:S(2)}, u32[]{:S(2)}) collective-permute-start(bf16[512,512]{1,0:T(8,128)(2,1)} %get-tuple-element.10), channel_id=1, source_target_pairs={{0,8},{8,16},{16,24},{24,32},{32,40},{40,48},{48,56},{56,0},{64,72... | collective-permute-start | bytes 1572872 | tf_op jit(solution)/shard_map/ppermute | solution.py:28
  51.9 33.5 %collective-permute-start.1 = (bf16[512,512]{1,0:T(8,128)(2,1)}, bf16[512,512]{1,0:T(8,128)(2,1)S(1)}, u32[]{:S(2)}, u32[]{:S(2)}) collective-permute-start(bf16[512,512]{1,0:T(8,128)(2,1)} %get-tuple-element.10), channel_id=1, source_target_pairs={{0,64},{8,72},{16,80},{24,88},{32,96},{40,104},{48,112},{56,120},{... | collective-permute-start | bytes 1572872 | tf_op jit(solution)/shard_map/ppermute | solution.py:28
  54.7 17.0 %collective-permute-start.3 = (bf16[512,384]{1,0:T(8,128)(2,1)}, bf16[512,384]{1,0:T(8,128)(2,1)}, u32[]{:S(2)}, u32[]{:S(2)}) collective-permute-start(bf16[512,384]{1,0:T(8,128)(2,1)} %get-tuple-element.11), channel_id=1, source_target_pairs={{0,8},{8,16},{16,24},{24,32},{32,40},{40,48},{48,56},{56,0},{64,72... | collective-permute-start | bytes 1179656 | tf_op jit(solution)/shard_map/ppermute | solution.py:28
  59.2 16.5 %collective-permute-start.4 = (bf16[512,384]{1,0:T(8,128)(2,1)}, bf16[512,384]{1,0:T(8,128)(2,1)S(1)}, u32[]{:S(2)}, u32[]{:S(2)}) collective-permute-start(bf16[512,384]{1,0:T(8,128)(2,1)} %get-tuple-element.11), channel_id=1, source_target_pairs={{0,64},{8,72},{16,80},{24,88},{32,96},{40,104},{48,112},{56,120},{... | collective-permute-start | bytes 1179656 | tf_op jit(solution)/shard_map/ppermute | solution.py:28
  74.0 7.2 %copy-start.2 = (f32[4]{0:T(128)S(1)}, f32[4]{0:T(128)}, u32[]{:S(2)}) copy-start(f32[4]{0:T(128)} %sinks.3) | copy-start | bytes 52
  75.9 9.5 %copy-start = (f32[2048]{0:T(1024)S(1)}, f32[2048]{0:T(1024)}, u32[]{:S(2)}) copy-start(f32[2048]{0:T(1024)} %param.10) | copy-start | bytes 24580
  75.9 9.5 %copy-start.1 = (bf16[3,256]{1,0:T(4,128)(2,1)S(1)}, bf16[3,256]{1,0:T(4,128)(2,1)}, u32[]{:S(2)}) copy-start(bf16[3,256]{1,0:T(4,128)(2,1)} %taps_ref.1) | copy-start | bytes 4612
  75.9 9.5 %collective-permute-start.5 = (bf16[384,128]{1,0:T(8,128)(2,1)S(1)}, bf16[384,128]{1,0:T(8,128)(2,1)S(1)}, u32[]{:S(2)}, u32[]{:S(2)}) collective-permute-start(bf16[384,128]{1,0:T(8,128)(2,1)S(1)} %tail.1), channel_id=1, source_target_pairs={{0,8},{8,16},{16,24},{24,32},{32,40},{40,48},{48,56},{56,64},{64,7... | collective-permute-start | bytes 294920 | tf_op jit(solution)/shard_map/ppermute | solution.py:33

commit v8 on v7

--- a/solution.py
+++ b/solution.py
@@ -1,3 +1,5 @@
+import functools
+
 import jax
 import jax.numpy as jnp
 from jax import lax
@@ -24,8 +26,10 @@
     pairs = []
     for z in range(SIDE):
         for y in range(SIDE):
-            pairs.append((z * SIDE + y, (z + dz) % SIDE * SIDE + (y + dy) % SIDE))
-    return lax.ppermute(value, SP, pairs)
+            for core, sign in enumerate((1, -1)):
+                to = (z + sign * dz) % SIDE * SIDE + (y + sign * dy) % SIDE
+                pairs.append(((z * SIDE + y) * 2 + core, to * 2 + core))
+    return lax.ppermute(value, SP + ("tp",), pairs)
 
 
 def passed_along(value):
@@ -69,31 +73,35 @@
                 ]
 
 
-def norm_kernel(place, tok_ref, gain_ref, out_ref, rim_ref):
-    rim_ref[...] = tok_ref[tok_ref.shape[0] - RIM :, :]
-    norm_into(place, tok_ref[...], gain_ref[...], column_sort(), out_ref)
+def norm_kernel(place, tok_hbm, gain_ref, out_hbm, rim_ref, sem, *, block):
+    n, width = tok_hbm.shape
+    swap = column_sort()
+    rim = pltpu.make_async_copy(tok_hbm.at[n - RIM : n, :], rim_ref, sem)
+    rim.start()
+
+    def step(tok_ref, out_ref):
+        norm_into(place, tok_ref[...], gain_ref[...], swap, out_ref)
+
+    pltpu.emit_pipeline(
+        step,
+        grid=(n // block,),
+        in_specs=[pl.BlockSpec((block, width), lambda i: (i, 0))],
+        out_specs=[pl.BlockSpec((4, block, width // 4), lambda i: (0, i, 0))],
+    )(tok_hbm, out_hbm)
+    rim.wait()
 
 
 def norm_classes(place, rows, gain, block):
     n, width = rows.shape
     return pl.pallas_call(
-        norm_kernel,
-        grid_spec=pltpu.PrefetchScalarGridSpec(
-            num_scalar_prefetch=1,
-            grid=(n // block,),
-            in_specs=[
-                pl.BlockSpec((block, width), lambda i, p: (i, 0)),
-                pl.BlockSpec((1, width), lambda i, p: (0, 0)),
-            ],
-            out_specs=[
-                pl.BlockSpec((4, block, width // 4), lambda i, p: (0, i, 0)),
-                pl.BlockSpec((RIM, width), lambda i, p: (0, 0)),
-            ],
-        ),
+        functools.partial(norm_kernel, block=block),
+        in_specs=[SMEM, HBM, VMEM],
+        out_specs=[HBM, VMEM],
         out_shape=[
-            jax.ShapeDtypeStruct((4, n, width // 4), jnp.bfloat16),
+            pltpu.HBM((4, n, width // 4), jnp.bfloat16),
             jax.ShapeDtypeStruct((RIM, width), jnp.bfloat16),
         ],
+        scratch_shapes=[pltpu.SemaphoreType.DMA(())],
         compiler_params=settings(9),
         cost_estimate=cost(5),
         name="norm",
@@ -164,14 +172,25 @@
     )(own)
 
 
-def early_kernel(x_ref, own_ref, y_ref, sum_ref):
+def early_kernel(x_hbm, own_ref, y_ref, sum_a, sum_b, x_ref, sems):
     n = x_ref.shape[1]
-    cols = sum_ref.shape[1]
+    cols = sum_a.shape[1]
     step = 256
-    for at in range(0, n, step):
-        sum_ref[at : at + step, :] = dot(x_ref[0, at : at + step, :], own_ref[:, :cols]) + dot(
+    copies = []
+    for k, at in enumerate(range(0, n, step)):
+        copies.append(
+            pltpu.make_async_copy(
+                x_hbm.at[:, at : at + step, :], x_ref.at[:, at : at + step, :], sems.at[k]
+            )
+        )
+        copies[-1].start()
+    for k, at in enumerate(range(0, n, step)):
+        copies[k].wait()
+        mine = x_ref[0, at : at + step, :]
+        sum_a[at : at + step, :] = dot(mine, own_ref[:, :cols]) + dot(
             x_ref[1, at : at + step, :], y_ref[...]
         )
+        sum_b[at : at + step, :] = dot(mine, own_ref[:, cols:])
 
 
 def early_sums(x, own, along_y):
@@ -179,11 +198,16 @@
     cols = along_y.shape[1]
     return pl.pallas_call(
         early_kernel,
-        in_specs=[VMEM] * 3,
-        out_specs=VMEM,
-        out_shape=jax.ShapeDtypeStruct((n, cols), jnp.float32),
+        in_specs=[HBM] + [VMEM] * 2,
+        out_specs=[VMEM] * 3,
+        out_shape=[
+            jax.ShapeDtypeStruct((n, cols), jnp.float32),
+            jax.ShapeDtypeStruct((n, own.shape[1] - cols), jnp.float32),
+            jax.ShapeDtypeStruct(x.shape, x.dtype),
+        ],
+        scratch_shapes=[pltpu.SemaphoreType.DMA((n // 256,))],
         compiler_params=settings(4),
-        cost_estimate=cost(2),
+        cost_estimate=cost(3),
         name="early",
     )(x, own, along_y)
 
@@ -266,8 +290,8 @@
 
 
 def conv_kernel(
-    sinks, place, x_ref, w0, w1, w2, w3, gain_ref, taps_ref, att_ref, log_ref, rows_ref, halo_ref,
-    out_hbm, log_out, out_ref, pad_ref, prev_x, sems,
+    sinks, place, x_ref, sum_ref, w0, w1, w2, w3, gain_ref, taps_ref, att_ref, log_ref, rows_ref, halo_ref,
+    out_hbm, log_hbm, out_ref, log_out, pad_ref, prev_x, sems, log_sem,
 ):
     n = x_ref.shape[1]
     width = 2 * LANES
@@ -292,11 +316,13 @@
     )
     log_out[...] = log_ref[...]
     log_out[:, :WINDOW] = log0
+    log_copy = pltpu.make_async_copy(log_out, log_hbm, log_sem)
+    log_copy.start()
     taps = taps_ref[...].astype(jnp.float32)
     copies = []
     for k, at in enumerate(range(0, n, step)):
-        acc = dot(x_ref[0, at : at + step, :], parts[0])
-        for c in range(1, 4):
+        acc = sum_ref[at : at + step, :] + dot(x_ref[1, at : at + step, :], parts[1])
+        for c in range(2, 4):
             acc = acc + dot(x_ref[c, at : at + step, :], parts[c])
         rounded = acc.astype(jnp.bfloat16).astype(jnp.float32)
         pad_ref[8 + at : 8 + at + step, :] = rounded[:, :width]
@@ -317,28 +343,31 @@
         copies[-1].start()
     for copy in copies:
         copy.wait()
-
-
-def convolution(sinks, place, x, parts, gain, taps, att, logs, rows, halo):
+    log_copy.wait()
+
+
+def convolution(sinks, place, x, sums, parts, gain, taps, att, logs, rows, halo):
     n = x.shape[1]
     return pl.pallas_call(
         conv_kernel,
-        in_specs=[SMEM] * 2 + [VMEM] * 11,
-        out_specs=[HBM, VMEM],
+        in_specs=[SMEM] * 2 + [VMEM] * 12,
+        out_specs=[HBM, HBM],
         out_shape=[
             jax.ShapeDtypeStruct((n, 2 * LANES), jnp.bfloat16),
             jax.ShapeDtypeStruct((4, n), jnp.float32),
         ],
         scratch_shapes=[
             pltpu.VMEM((n, 2 * LANES), jnp.bfloat16),
+            pltpu.VMEM((4, n), jnp.float32),
             pltpu.VMEM((n + 8, 2 * LANES), jnp.float32),
             pltpu.VMEM((4, RIM, x.shape[2]), jnp.bfloat16),
             pltpu.SemaphoreType.DMA((n // 256,)),
+            pltpu.SemaphoreType.DMA(()),
         ],
         compiler_params=settings(8),
         cost_estimate=cost(6),
         name="conv",
-    )(sinks, place, x, *parts, gain, taps, att, logs, rows, halo)
+    )(sinks, place, x, sums, *parts, gain, taps, att, logs, rows, halo)
 
 
 def body(
@@ -373,15 +402,14 @@
     parts_a = classes(own_a)
     parts_b = classes(own_b)
     near = pltpu.with_memory_space_constraint
-    x, rim = norm_classes(place, near(tokens, pltpu.HBM), near(gain, pltpu.HBM), 256)
-    sum_a = early_sums(x, own, parts_a[1])
+    x_far, rim = norm_classes(place, near(tokens, pltpu.HBM), gain, 256)
+    x_far = near(x_far, pltpu.HBM)
+    sum_a, sum_b, x = early_sums(x_far, own, parts_a[1])
     last = tail_rows(x, sum_a, parts_a[2:], rim)
     halo = passed_along(last)
     att, logs, rows = attention(sink_logits, x, sum_a, parts_a[2:])
     return tuple(
-        convolution(
-            sink_logits, place, x, parts_b, gain, conv_taps, att, logs, rows, halo
-        )
+        convolution(sink_logits, place, x, sum_b, parts_b, gain, conv_taps, att, logs, rows, halo)
     )
 
 

time: 90.9 us -> 88.5 us (0.974)
  the two profiles are of different devices: /device:TPU:40 before, /device:TPU:1 now
where the time goes in v8:
time: 88.5 us; the launch traced here: 88 us
  blocking collectives  44 us (50%)
  Pallas kernels  20.4 us (23%)
  starting transfers between devices  17.3 us (20%)
  waiting for transfers between devices  3.7 us (4%)
  local copies, waits for them, and re-layouts  1.65 us (2%)
    all_to_all x1, blocking collectives, layer(): own = lax.all_to_all(sent, ('zh', 'yh'), 0, 0)  44 us
    ppermute x5, starting transfers between devices, shift(): return lax.ppermute(value, SP + ('tp',), pairs)  16 us
    pallas_call x1, Pallas kernels, norm_classes(): pl.pallas_call(functools.partial(norm_kernel, block=block), in_specs=[SME...  6.52 us
    pallas_call x1, Pallas kernels, early_sums(): pl.pallas_call(early_kernel, in_specs=[HBM] + [VMEM] * 2, out_specs=[VMEM...  4.61 us
    pallas_call x1, Pallas kernels, attention(): pl.pallas_call(attn_kernel, in_specs=[SMEM] + [VMEM] * 4, out_specs=[VMEM...  4.14 us
    pallas_call x1, Pallas kernels, convolution(): pl.pallas_call(conv_kernel, in_specs=[SMEM] * 2 + [VMEM] * 12, out_specs=...  3.93 us
    ppermute x5, waiting for transfers between devices, shift(): return lax.ppermute(value, SP + ('tp',), pairs)  3.7 us
  transfers between devices with their start and end apart: 6, of which 1 were waited for; matrix products, arithmetic and copies ran while one was open for 0% of the time, Pallas kernels for 19%

profile of v8, /device:TPU:1, one launch (start us, length us, event | category | flops | bytes accessed | tf_op | source)
XLA Modules:
  0.0 88.0 jit_solution(9597842476554293544)
XLA Ops:
  0.6 0.9 concatenate.3
  1.5 0.1 broadcast_in_dim.2
  1.6 44.0 %all_to_all.5 = bf16[16,32,896]{2,1,0:T(8,128)(2,1)S(1)} all-to-all(bf16[16,32,896]{2,1,0:T(8,128)(2,1)S(1)} %broadcast_in_dim.2), channel_id=1, replica_groups=mesh['zh'=4,'zl'=2,'yh'=4,'yl'=2,'fs'=4,'tp'=2] {'zh','yh'}, dimensions={0} | all-to-all | bytes 1835008 | tf_op jit(solution)/shard_map/all_to_all | solution.py:391
  45.6 1.9 %collective-permute-start.3 = (bf16[512,896]{1,0:T(8,128)(2,1)S(1)}, bf16[512,896]{1,0:T(8,128)(2,1)S(1)}, u32[]{:S(2)}, u32[]{:S(2)}) collective-permute-start(bf16[512,896]{1,0:T(8,128)(2,1)S(1)} %bitcast.5), channel_id=1, source_target_pairs={{0,504},{1,73},{8,448},{9,81},{16,456},{17,89},{24,464},{25,97},{3... | collective-permute-start | bytes 2752520 | tf_op jit(solution)/shard_map/ppermute | solution.py:32
  47.5 1.0 %cut.1 = (bf16[512,384]{1,0:T(8,128)(2,1)}, bf16[512,512]{1,0:T(8,128)(2,1)}) custom-call(bf16[512,896]{1,0:T(8,128)(2,1)S(1)} %bitcast.6), custom_call_target="tpu_custom_call" | custom-call | flops 3900000 | bytes 1048576 | tf_op jit(solution)/shard_map/cut/pallas_call | solution.py:161
  48.5 5.1 %collective-permute-start.1 = (bf16[512,512]{1,0:T(8,128)(2,1)}, bf16[512,512]{1,0:T(8,128)(2,1)S(1)}, u32[]{:S(2)}, u32[]{:S(2)}) collective-permute-start(bf16[512,512]{1,0:T(8,128)(2,1)} %get-tuple-element.16), channel_id=1, source_target_pairs={{0,8},{1,57},{8,16},{9,1},{16,24},{17,9},{24,32},{25,17},{32,40},{... | collective-permute-start | bytes 1572872 | tf_op jit(solution)/shard_map/ppermute | solution.py:32
  53.6 3.7 %collective-permute-start.2 = (bf16[512,512]{1,0:T(8,128)(2,1)}, bf16[512,512]{1,0:T(8,128)(2,1)S(1)}, u32[]{:S(2)}, u32[]{:S(2)}) collective-permute-start(bf16[512,512]{1,0:T(8,128)(2,1)} %get-tuple-element.16), channel_id=1, source_target_pairs={{0,64},{1,449},{8,72},{9,457},{16,80},{17,465},{24,88},{25,473},{3... | collective-permute-start | bytes 1572872 | tf_op jit(solution)/shard_map/ppermute | solution.py:32
  57.4 3.3 %collective-permute-start = (bf16[512,384]{1,0:T(8,128)(2,1)}, bf16[512,384]{1,0:T(8,128)(2,1)}, u32[]{:S(2)}, u32[]{:S(2)}) collective-permute-start(bf16[512,384]{1,0:T(8,128)(2,1)} %get-tuple-element.13), channel_id=1, source_target_pairs={{0,8},{1,57},{8,16},{9,1},{16,24},{17,9},{24,32},{25,17},{32,40},{... | collective-permute-start | bytes 1179656 | tf_op jit(solution)/shard_map/ppermute | solution.py:32
  60.7 1.9 %collective-permute-start.4 = (bf16[512,384]{1,0:T(8,128)(2,1)}, bf16[512,384]{1,0:T(8,128)(2,1)S(1)}, u32[]{:S(2)}, u32[]{:S(2)}) collective-permute-start(bf16[512,384]{1,0:T(8,128)(2,1)} %get-tuple-element.13), channel_id=1, source_target_pairs={{0,64},{1,449},{8,72},{9,457},{16,80},{17,465},{24,88},{25,473},{3... | collective-permute-start | bytes 1179656 | tf_op jit(solution)/shard_map/ppermute | solution.py:32
  62.6 0.1 pad_add_fusion.place
  62.7 0.0 copy-start
  62.7 0.7 copy-done
  63.4 6.5 %norm.1 = (bf16[4,1024,512]{2,1,0:T(8,128)(2,1)}, bf16[16,2048]{1,0:T(8,128)(2,1)S(1)}) custom-call(s32[3]{0:T(128)S(1)} %pad_add_fusion.place, bf16[1024,2048]{1,0:T(8,128)(2,1)} %tok_hbm.1, f32[1,2048]{1,0:T(1,128)S(1)} %bitcast.9), custom_call_target="tpu_custom_call" | custom-call | flops 19500000 | bytes 1048576 | tf_op jit(solution)/shard_map/norm/pallas_call | solution.py:96
  69.9 3.7 %collective-permute-done.y_ref = bf16[512,384]{1,0:T(8,128)(2,1)} collective-permute-done((bf16[512,384]{1,0:T(8,128)(2,1)}, bf16[512,384]{1,0:T(8,128)(2,1)}, u32[]{:S(2)}, u32[]{:S(2)}) %collective-permute-start) | collective-permute-done | bytes 393248 | tf_op jit(solution)/shard_map/ppermute | solution.py:32
  73.6 4.6 %early.1 = (f32[1024,384]{1,0:T(8,128)S(1)}, f32[1024,512]{1,0:T(8,128)S(1)}, bf16[4,1024,512]{2,1,0:T(8,128)(2,1)S(1)}) custom-call(bf16[4,1024,512]{2,1,0:T(8,128)(2,1)} %get-tuple-element.12.x_hbm, bf16[512,896]{1,0:T(8,128)(2,1)S(1)} %bitcast.7, bf16[512,384]{1,0:T(8,128)(2,1)} %collective-permute-done.y_ref), custom_call_target="tpu_custom_call" | custom-call | flops 11700000 | bytes 1048576 | tf_op jit(solution)/shard_map/early/pallas_call | solution.py:199
  78.2 0.0 copy-start.1
  78.2 0.0 collective-permute-done.4.w2
  78.3 0.0 collective-permute-done.3.w3
  78.3 0.3 tail.1
  78.5 0.0 copy-start.2
  78.5 1.3 %collective-permute-start.5 = (bf16[384,128]{1,0:T(8,128)(2,1)S(1)}, bf16[384,128]{1,0:T(8,128)(2,1)S(1)}, u32[]{:S(2)}, u32[]{:S(2)}) collective-permute-start(bf16[384,128]{1,0:T(8,128)(2,1)S(1)} %tail.1), channel_id=1, source_target_pairs={{0,8},{8,16},{16,24},{24,32},{32,40},{40,48},{48,56},{56,64},{64,7... | collective-permute-start | bytes 294920 | tf_op jit(solution)/shard_map/ppermute | solution.py:37
  79.8 0.0 copy-done.1
  79.8 4.1 %attn.1 = (f32[1024,256]{1,0:T(8,128)S(1)}, f32[4,1024]{1,0:T(4,128)S(1)}, bf16[1024,384]{1,0:T(8,128)(2,1)S(1)}) custom-call(f32[4]{0:T(128)S(1)} %copy-done.1, bf16[4,1024,512]{2,1,0:T(8,128)(2,1)S(1)} %get-tuple-element.14.x_ref, f32[1024,384]{1,0:T(8,128)S(1)} %get-tuple-element.17.sum_ref, bf16[512,384]{1,0:T(8,128)(2,1)S(1)} %collective-permute-done.4.w2, ...), custom_call_target="tpu_custom_call" | custom-call | flops 31200000 | bytes 1048576 | tf_op jit(solution)/shard_map/attn/pallas_call | solution.py:276
  84.0 0.0 collective-permute-done.1.w1
  84.0 0.0 collective-permute-done.2.w2
  84.0 0.0 collective-permute-done.5.halo_ref
  84.0 0.0 copy-done.2
  84.0 3.9 %conv.1 = (bf16[1024,256]{1,0:T(8,128)(2,1)}, f32[4,1024]{1,0:T(4,128)}) custom-call(f32[4]{0:T(128)S(1)} %copy-done.1, s32[3]{0:T(128)S(1)} %pad_add_fusion.place, bf16[4,1024,512]{2,1,0:T(8,128)(2,1)S(1)} %get-tuple-element.14.x_ref, f32[1024,512]{1,0:T(8,128)S(1)} %get-tuple-element.15.sum_ref, bf16[512,896]{1,0:T(8,128)(2,1)S(1)} %bitcast.8, ...), custom_call_target="tpu_custom_call" | custom-call | flops 23400000 | bytes 1048576 | tf_op jit(solution)/shard_map/conv/pallas_call | solution.py:351
Async XLA Ops:
  45.6 32.7 %collective-permute-start.3 = (bf16[512,896]{1,0:T(8,128)(2,1)S(1)}, bf16[512,896]{1,0:T(8,128)(2,1)S(1)}, u32[]{:S(2)}, u32[]{:S(2)}) collective-permute-start(bf16[512,896]{1,0:T(8,128)(2,1)S(1)} %bitcast.5), channel_id=1, source_target_pairs={{0,504},{1,73},{8,448},{9,81},{16,456},{17,89},{24,464},{25,97},{3... | collective-permute-start | bytes 2752520 | tf_op jit(solution)/shard_map/ppermute | solution.py:32
  48.5 35.5 %collective-permute-start.1 = (bf16[512,512]{1,0:T(8,128)(2,1)}, bf16[512,512]{1,0:T(8,128)(2,1)S(1)}, u32[]{:S(2)}, u32[]{:S(2)}) collective-permute-start(bf16[512,512]{1,0:T(8,128)(2,1)} %get-tuple-element.16), channel_id=1, source_target_pairs={{0,8},{1,57},{8,16},{9,1},{16,24},{17,9},{24,32},{25,17},{32,40},{... | collective-permute-start | bytes 1572872 | tf_op jit(solution)/shard_map/ppermute | solution.py:32
  53.6 30.4 %collective-permute-start.2 = (bf16[512,512]{1,0:T(8,128)(2,1)}, bf16[512,512]{1,0:T(8,128)(2,1)S(1)}, u32[]{:S(2)}, u32[]{:S(2)}) collective-permute-start(bf16[512,512]{1,0:T(8,128)(2,1)} %get-tuple-element.16), channel_id=1, source_target_pairs={{0,64},{1,449},{8,72},{9,457},{16,80},{17,465},{24,88},{25,473},{3... | collective-permute-start | bytes 1572872 | tf_op jit(solution)/shard_map/ppermute | solution.py:32
  57.4 16.2 %collective-permute-start = (bf16[512,384]{1,0:T(8,128)(2,1)}, bf16[512,384]{1,0:T(8,128)(2,1)}, u32[]{:S(2)}, u32[]{:S(2)}) collective-permute-start(bf16[512,384]{1,0:T(8,128)(2,1)} %get-tuple-element.13), channel_id=1, source_target_pairs={{0,8},{1,57},{8,16},{9,1},{16,24},{17,9},{24,32},{25,17},{32,40},{... | collective-permute-start | bytes 1179656 | tf_op jit(solution)/shard_map/ppermute | solution.py:32
  60.7 17.6 %collective-permute-start.4 = (bf16[512,384]{1,0:T(8,128)(2,1)}, bf16[512,384]{1,0:T(8,128)(2,1)S(1)}, u32[]{:S(2)}, u32[]{:S(2)}) collective-permute-start(bf16[512,384]{1,0:T(8,128)(2,1)} %get-tuple-element.13), channel_id=1, source_target_pairs={{0,64},{1,449},{8,72},{9,457},{16,80},{17,465},{24,88},{25,473},{3... | collective-permute-start | bytes 1179656 | tf_op jit(solution)/shard_map/ppermute | solution.py:32
  62.7 0.7 copy-start
  78.2 1.6 %copy-start.1 = (f32[4]{0:T(128)S(1)}, f32[4]{0:T(128)}, u32[]{:S(2)}) copy-start(f32[4]{0:T(128)} %sinks.3) | copy-start | bytes 52
  78.5 5.5 %copy-start.2 = (bf16[3,256]{1,0:T(4,128)(2,1)S(1)}, bf16[3,256]{1,0:T(4,128)(2,1)}, u32[]{:S(2)}) copy-start(bf16[3,256]{1,0:T(4,128)(2,1)} %taps_ref.1) | copy-start | bytes 4612
  78.5 5.5 %collective-permute-start.5 = (bf16[384,128]{1,0:T(8,128)(2,1)S(1)}, bf16[384,128]{1,0:T(8,128)(2,1)S(1)}, u32[]{:S(2)}, u32[]{:S(2)}) collective-permute-start(bf16[384,128]{1,0:T(8,128)(2,1)S(1)} %tail.1), channel_id=1, source_target_pairs={{0,8},{8,16},{16,24},{24,32},{32,40},{40,48},{48,56},{56,64},{64,7... | collective-permute-start | bytes 294920 | tf_op jit(solution)/shard_map/ppermute | solution.py:37

commit v9 on v7

--- a/solution.py
+++ b/solution.py
@@ -113,7 +113,7 @@
     key_idx = lax.broadcasted_iota(jnp.int32, (WINDOW, WINDOW), 0)
     query_idx = lax.broadcasted_iota(jnp.int32, (WINDOW, WINDOW), 1)
     from_prev = key_idx > query_idx
-    weights, logs = [], []
+    weights, scales, logs = [], [], []
     for pair in range(2):
         both = dot(keys, q[:, pair * LANES : (pair + 1) * LANES], ((1,), (1,)))
         for side in range(2):
@@ -127,17 +127,23 @@
             raised = jnp.exp(scores - top)
             total = jnp.sum(raised, axis=0, keepdims=True) + jnp.exp(sinks[head] - top)
             logs.append(top + jnp.log(total))
-            share = raised * (1.0 / total)
-            zero = jnp.zeros_like(share)
+            scales.append(1.0 / total)
+            zero = jnp.zeros_like(raised)
             weights.append(
                 jnp.concatenate(
-                    [jnp.where(from_prev, share, zero), jnp.where(from_prev, zero, share)], axis=0
+                    [jnp.where(from_prev, raised, zero), jnp.where(from_prev, zero, raised)], axis=0
                 ).astype(jnp.bfloat16)
             )
     outs = []
     for pair in range(2):
         got = dot(values, jnp.concatenate(weights[pair * 2 : pair * 2 + 2], axis=1), ((0,), (0,)))
-        stacked = jnp.concatenate([got[HEAD_DIM:, :WINDOW], got[HEAD_DIM:, WINDOW:]], axis=0)
+        stacked = jnp.concatenate(
+            [
+                got[HEAD_DIM:, :WINDOW] * scales[pair * 2],
+                got[HEAD_DIM:, WINDOW:] * scales[pair * 2 + 1],
+            ],
+            axis=0,
+        )
         outs.append(stacked.T)
     return jnp.concatenate(outs, axis=1), jnp.concatenate(logs, axis=0)
 
@@ -164,14 +170,16 @@
     )(own)
 
 
-def early_kernel(x_ref, own_ref, y_ref, sum_ref):
+def early_kernel(x_ref, own_ref, y_ref, sum_a, sum_b):
     n = x_ref.shape[1]
-    cols = sum_ref.shape[1]
+    cols = sum_a.shape[1]
     step = 256
     for at in range(0, n, step):
-        sum_ref[at : at + step, :] = dot(x_ref[0, at : at + step, :], own_ref[:, :cols]) + dot(
+        mine = x_ref[0, at : at + step, :]
+        sum_a[at : at + step, :] = dot(mine, own_ref[:, :cols]) + dot(
             x_ref[1, at : at + step, :], y_ref[...]
         )
+        sum_b[at : at + step, :] = dot(mine, own_ref[:, cols:])
 
 
 def early_sums(x, own, along_y):
@@ -180,8 +188,11 @@
     return pl.pallas_call(
         early_kernel,
         in_specs=[VMEM] * 3,
-        out_specs=VMEM,
-        out_shape=jax.ShapeDtypeStruct((n, cols), jnp.float32),
+        out_specs=[VMEM] * 2,
+        out_shape=[
+            jax.ShapeDtypeStruct((n, cols), jnp.float32),
+            jax.ShapeDtypeStruct((n, own.shape[1] - cols), jnp.float32),
+        ],
         compiler_params=settings(4),
         cost_estimate=cost(2),
         name="early",
@@ -266,8 +277,8 @@
 
 
 def conv_kernel(
-    sinks, place, x_ref, w0, w1, w2, w3, gain_ref, taps_ref, att_ref, log_ref, rows_ref, halo_ref,
-    out_hbm, log_out, out_ref, pad_ref, prev_x, sems,
+    sinks, place, x_ref, sum_ref, w0, w1, w2, w3, gain_ref, taps_ref, att_ref, log_ref, rows_ref, halo_ref,
+    out_hbm, log_hbm, out_ref, log_out, pad_ref, prev_x, sems, log_sem,
 ):
     n = x_ref.shape[1]
     width = 2 * LANES
@@ -292,11 +303,13 @@
     )
     log_out[...] = log_ref[...]
     log_out[:, :WINDOW] = log0
+    log_copy = pltpu.make_async_copy(log_out, log_hbm, log_sem)
+    log_copy.start()
     taps = taps_ref[...].astype(jnp.float32)
     copies = []
     for k, at in enumerate(range(0, n, step)):
-        acc = dot(x_ref[0, at : at + step, :], parts[0])
-        for c in range(1, 4):
+        acc = sum_ref[at : at + step, :] + dot(x_ref[1, at : at + step, :], parts[1])
+        for c in range(2, 4):
             acc = acc + dot(x_ref[c, at : at + step, :], parts[c])
         rounded = acc.astype(jnp.bfloat16).astype(jnp.float32)
         pad_ref[8 + at : 8 + at + step, :] = rounded[:, :width]
@@ -317,28 +330,31 @@
         copies[-1].start()
     for copy in copies:
         copy.wait()
-
-
-def convolution(sinks, place, x, parts, gain, taps, att, logs, rows, halo):
+    log_copy.wait()
+
+
+def convolution(sinks, place, x, sums, parts, gain, taps, att, logs, rows, halo):
     n = x.shape[1]
     return pl.pallas_call(
         conv_kernel,
-        in_specs=[SMEM] * 2 + [VMEM] * 11,
-        out_specs=[HBM, VMEM],
+        in_specs=[SMEM] * 2 + [VMEM] * 12,
+        out_specs=[HBM, HBM],
         out_shape=[
             jax.ShapeDtypeStruct((n, 2 * LANES), jnp.bfloat16),
             jax.ShapeDtypeStruct((4, n), jnp.float32),
         ],
         scratch_shapes=[
             pltpu.VMEM((n, 2 * LANES), jnp.bfloat16),
+            pltpu.VMEM((4, n), jnp.float32),
             pltpu.VMEM((n + 8, 2 * LANES), jnp.float32),
             pltpu.VMEM((4, RIM, x.shape[2]), jnp.bfloat16),
             pltpu.SemaphoreType.DMA((n // 256,)),
+            pltpu.SemaphoreType.DMA(()),
         ],
         compiler_params=settings(8),
         cost_estimate=cost(6),
         name="conv",
-    )(sinks, place, x, *parts, gain, taps, att, logs, rows, halo)
+    )(sinks, place, x, sums, *parts, gain, taps, att, logs, rows, halo)
 
 
 def body(
@@ -374,14 +390,12 @@
     parts_b = classes(own_b)
     near = pltpu.with_memory_space_constraint
     x, rim = norm_classes(place, near(tokens, pltpu.HBM), near(gain, pltpu.HBM), 256)
-    sum_a = early_sums(x, own, parts_a[1])
+    sum_a, sum_b = early_sums(x, own, parts_a[1])
     last = tail_rows(x, sum_a, parts_a[2:], rim)
     halo = passed_along(last)
     att, logs, rows = attention(sink_logits, x, sum_a, parts_a[2:])
     return tuple(
-        convolution(
-            sink_logits, place, x, parts_b, gain, conv_taps, att, logs, rows, halo
-        )
+        convolution(sink_logits, place, x, sum_b, parts_b, gain, conv_taps, att, logs, rows, halo)
     )
 
 

time: 90.9 us -> 90.3 us (level)
  the two profiles are of different devices: /device:TPU:40 before, /device:TPU:66 now
where the time goes in v9:
time: 90.3 us; the launch traced here: 89.8 us
  blocking collectives  43.8 us (49%)
  Pallas kernels  17.7 us (20%)
  starting transfers between devices  15.9 us (18%)
  waiting for transfers between devices  10.6 us (12%)
  local copies, waits for them, and re-layouts  0.96 us (1%)
    all_to_all x1, blocking collectives, layer(): own = lax.all_to_all(sent, ('zh', 'yh'), 0, 0)  43.8 us
    ppermute x5, starting transfers between devices, shift(): return lax.ppermute(value, SP, pairs)  14 us
    ppermute x5, waiting for transfers between devices, shift(): return lax.ppermute(value, SP, pairs)  7.82 us
    pallas_call x1, Pallas kernels, norm_classes(): pl.pallas_call(norm_kernel, grid_spec=pltpu.PrefetchScalarGridSpec(num_sc...  5.73 us
    pallas_call x1, Pallas kernels, attention(): pl.pallas_call(attn_kernel, in_specs=[SMEM] + [VMEM] * 4, out_specs=[VMEM...  3.93 us
    pallas_call x1, Pallas kernels, convolution(): pl.pallas_call(conv_kernel, in_specs=[SMEM] * 2 + [VMEM] * 12, out_specs=...  3.92 us
    pallas_call x1, Pallas kernels, early_sums(): pl.pallas_call(early_kernel, in_specs=[VMEM] * 3, out_specs=[VMEM] * 2, o...  2.83 us
    ppermute x1, waiting for transfers between devices, passed_along(): return lax.ppermute(value, SP, [(i, i + 1) for i in range(n - 1)])  2.73 us
  transfers between devices with their start and end apart: 6, of which 2 were waited for; matrix products, arithmetic and copies ran while one was open for 0% of the time, Pallas kernels for 15%

profile of v9, /device:TPU:66, one launch (start us, length us, event | category | flops | bytes accessed | tf_op | source)
XLA Modules:
  0.0 89.8 jit_solution(9539048188701071277)
XLA Ops:
  0.6 0.9 concatenate.3
  1.5 0.1 broadcast_in_dim.2
  1.6 43.8 %all_to_all.5 = bf16[16,32,896]{2,1,0:T(8,128)(2,1)S(1)} all-to-all(bf16[16,32,896]{2,1,0:T(8,128)(2,1)S(1)} %broadcast_in_dim.2), channel_id=1, replica_groups=mesh['zh'=4,'zl'=2,'yh'=4,'yl'=2,'fs'=4,'tp'=2] {'zh','yh'}, dimensions={0} | all-to-all | bytes 1835008 | tf_op jit(solution)/shard_map/all_to_all | solution.py:378
  45.4 1.9 %collective-permute-start.3 = (bf16[512,896]{1,0:T(8,128)(2,1)S(1)}, bf16[512,896]{1,0:T(8,128)(2,1)S(1)}, u32[]{:S(2)}, u32[]{:S(2)}) collective-permute-start(bf16[512,896]{1,0:T(8,128)(2,1)S(1)} %bitcast.5), channel_id=1, source_target_pairs={{0,504},{8,448},{16,456},{24,464},{32,472},{40,480},{48,488},{56,4... | collective-permute-start | bytes 2752520 | tf_op jit(solution)/shard_map/ppermute | solution.py:28
  47.3 1.0 %cut.1 = (bf16[512,384]{1,0:T(8,128)(2,1)}, bf16[512,512]{1,0:T(8,128)(2,1)}) custom-call(bf16[512,896]{1,0:T(8,128)(2,1)S(1)} %bitcast.6), custom_call_target="tpu_custom_call" | custom-call | flops 3900000 | bytes 1048576 | tf_op jit(solution)/shard_map/cut/pallas_call | solution.py:159
  48.3 4.0 %collective-permute-start.1 = (bf16[512,512]{1,0:T(8,128)(2,1)}, bf16[512,512]{1,0:T(8,128)(2,1)S(1)}, u32[]{:S(2)}, u32[]{:S(2)}) collective-permute-start(bf16[512,512]{1,0:T(8,128)(2,1)} %get-tuple-element.14), channel_id=1, source_target_pairs={{0,8},{8,16},{16,24},{24,32},{32,40},{40,48},{48,56},{56,0},{64,72... | collective-permute-start | bytes 1572872 | tf_op jit(solution)/shard_map/ppermute | solution.py:28
  52.3 3.3 %collective-permute-start.2 = (bf16[512,512]{1,0:T(8,128)(2,1)}, bf16[512,512]{1,0:T(8,128)(2,1)S(1)}, u32[]{:S(2)}, u32[]{:S(2)}) collective-permute-start(bf16[512,512]{1,0:T(8,128)(2,1)} %get-tuple-element.14), channel_id=1, source_target_pairs={{0,64},{8,72},{16,80},{24,88},{32,96},{40,104},{48,112},{56,120},{... | collective-permute-start | bytes 1572872 | tf_op jit(solution)/shard_map/ppermute | solution.py:28
  55.6 1.9 %collective-permute-start = (bf16[512,384]{1,0:T(8,128)(2,1)}, bf16[512,384]{1,0:T(8,128)(2,1)}, u32[]{:S(2)}, u32[]{:S(2)}) collective-permute-start(bf16[512,384]{1,0:T(8,128)(2,1)} %get-tuple-element.12), channel_id=1, source_target_pairs={{0,8},{8,16},{16,24},{24,32},{32,40},{40,48},{48,56},{56,0},{64,72... | collective-permute-start | bytes 1179656 | tf_op jit(solution)/shard_map/ppermute | solution.py:28
  57.5 2.9 %collective-permute-start.4 = (bf16[512,384]{1,0:T(8,128)(2,1)}, bf16[512,384]{1,0:T(8,128)(2,1)S(1)}, u32[]{:S(2)}, u32[]{:S(2)}) collective-permute-start(bf16[512,384]{1,0:T(8,128)(2,1)} %get-tuple-element.12), channel_id=1, source_target_pairs={{0,64},{8,72},{16,80},{24,88},{32,96},{40,104},{48,112},{56,120},{... | collective-permute-start | bytes 1179656 | tf_op jit(solution)/shard_map/ppermute | solution.py:28
  60.4 0.1 pad_add_fusion.place
  60.5 5.7 %norm.1 = (bf16[4,1024,512]{2,1,0:T(8,128)(2,1)S(1)}, bf16[16,2048]{1,0:T(8,128)(2,1)S(1)}) custom-call(s32[3]{0:T(128)S(1)} %pad_add_fusion.place, bf16[1024,2048]{1,0:T(8,128)(2,1)} %tok_ref.1, f32[1,2048]{1,0:T(1,128)} %bitcast.9), custom_call_target="tpu_custom_call" | custom-call | flops 19500000 | bytes 1048576 | tf_op jit(solution)/shard_map/norm/pallas_call | solution.py:79
  66.3 7.8 %collective-permute-done.y_ref = bf16[512,384]{1,0:T(8,128)(2,1)} collective-permute-done((bf16[512,384]{1,0:T(8,128)(2,1)}, bf16[512,384]{1,0:T(8,128)(2,1)}, u32[]{:S(2)}, u32[]{:S(2)}) %collective-permute-start) | collective-permute-done | bytes 393248 | tf_op jit(solution)/shard_map/ppermute | solution.py:28
  74.1 2.8 %early.1 = (f32[1024,384]{1,0:T(8,128)S(1)}, f32[1024,512]{1,0:T(8,128)S(1)}) custom-call(bf16[4,1024,512]{2,1,0:T(8,128)(2,1)S(1)} %get-tuple-element.11.x_ref, bf16[512,896]{1,0:T(8,128)(2,1)S(1)} %bitcast.7, bf16[512,384]{1,0:T(8,128)(2,1)} %collective-permute-done.y_ref), custom_call_target="tpu_custom_call" | custom-call | flops 7800000 | bytes 1048576 | tf_op jit(solution)/shard_map/early/pallas_call | solution.py:188
  76.9 0.0 copy-start.1
  76.9 0.0 collective-permute-done.4.w2
  76.9 0.0 collective-permute-done.3.w3
  76.9 0.3 tail.1
  77.2 0.0 copy-start
  77.2 0.0 copy-start.2
  77.2 1.9 %collective-permute-start.5 = (bf16[384,128]{1,0:T(8,128)(2,1)S(1)}, bf16[384,128]{1,0:T(8,128)(2,1)S(1)}, u32[]{:S(2)}, u32[]{:S(2)}) collective-permute-start(bf16[384,128]{1,0:T(8,128)(2,1)S(1)} %tail.1), channel_id=1, source_target_pairs={{0,8},{8,16},{16,24},{24,32},{32,40},{40,48},{48,56},{56,64},{64,7... | collective-permute-start | bytes 294920 | tf_op jit(solution)/shard_map/ppermute | solution.py:33
  79.2 0.0 copy-done.1
  79.2 3.9 %attn.1 = (f32[1024,256]{1,0:T(8,128)S(1)}, f32[4,1024]{1,0:T(4,128)S(1)}, bf16[1024,384]{1,0:T(8,128)(2,1)S(1)}) custom-call(f32[4]{0:T(128)S(1)} %copy-done.1, bf16[4,1024,512]{2,1,0:T(8,128)(2,1)S(1)} %get-tuple-element.11.x_ref, f32[1024,384]{1,0:T(8,128)S(1)} %get-tuple-element.15.sum_ref, bf16[512,384]{1,0:T(8,128)(2,1)S(1)} %collective-permute-done.4.w2, ...), custom_call_target="tpu_custom_call" | custom-call | flops 31200000 | bytes 1048576 | tf_op jit(solution)/shard_map/attn/pallas_call | solution.py:263
  83.1 0.0 collective-permute-done.1.w1
  83.1 0.0 collective-permute-done.2.w2
  83.1 2.7 %collective-permute-done.5.halo_ref = bf16[384,128]{1,0:T(8,128)(2,1)S(1)} collective-permute-done((bf16[384,128]{1,0:T(8,128)(2,1)S(1)}, bf16[384,128]{1,0:T(8,128)(2,1)S(1)}, u32[]{:S(2)}, u32[]{:S(2)}) %collective-permute-start.5) | collective-permute-done | bytes 98336 | tf_op jit(solution)/shard_map/ppermute | solution.py:33
  85.9 0.0 copy-done
  85.9 0.0 copy-done.2
  85.9 3.9 %conv.1 = (bf16[1024,256]{1,0:T(8,128)(2,1)}, f32[4,1024]{1,0:T(4,128)}) custom-call(f32[4]{0:T(128)S(1)} %copy-done.1, s32[3]{0:T(128)S(1)} %pad_add_fusion.place, bf16[4,1024,512]{2,1,0:T(8,128)(2,1)S(1)} %get-tuple-element.11.x_ref, f32[1024,512]{1,0:T(8,128)S(1)} %get-tuple-element.13.sum_ref, bf16[512,896]{1,0:T(8,128)(2,1)S(1)} %bitcast.8, ...), custom_call_target="tpu_custom_call" | custom-call | flops 23400000 | bytes 1048576 | tf_op jit(solution)/shard_map/conv/pallas_call | solution.py:338
Async XLA Ops:
  45.4 31.6 %collective-permute-start.3 = (bf16[512,896]{1,0:T(8,128)(2,1)S(1)}, bf16[512,896]{1,0:T(8,128)(2,1)S(1)}, u32[]{:S(2)}, u32[]{:S(2)}) collective-permute-start(bf16[512,896]{1,0:T(8,128)(2,1)S(1)} %bitcast.5), channel_id=1, source_target_pairs={{0,504},{8,448},{16,456},{24,464},{32,472},{40,480},{48,488},{56,4... | collective-permute-start | bytes 2752520 | tf_op jit(solution)/shard_map/ppermute | solution.py:28
  48.3 34.8 %collective-permute-start.1 = (bf16[512,512]{1,0:T(8,128)(2,1)}, bf16[512,512]{1,0:T(8,128)(2,1)S(1)}, u32[]{:S(2)}, u32[]{:S(2)}) collective-permute-start(bf16[512,512]{1,0:T(8,128)(2,1)} %get-tuple-element.14), channel_id=1, source_target_pairs={{0,8},{8,16},{16,24},{24,32},{32,40},{40,48},{48,56},{56,0},{64,72... | collective-permute-start | bytes 1572872 | tf_op jit(solution)/shard_map/ppermute | solution.py:28
  52.3 30.8 %collective-permute-start.2 = (bf16[512,512]{1,0:T(8,128)(2,1)}, bf16[512,512]{1,0:T(8,128)(2,1)S(1)}, u32[]{:S(2)}, u32[]{:S(2)}) collective-permute-start(bf16[512,512]{1,0:T(8,128)(2,1)} %get-tuple-element.14), channel_id=1, source_target_pairs={{0,64},{8,72},{16,80},{24,88},{32,96},{40,104},{48,112},{56,120},{... | collective-permute-start | bytes 1572872 | tf_op jit(solution)/shard_map/ppermute | solution.py:28
  55.6 18.5 %collective-permute-start = (bf16[512,384]{1,0:T(8,128)(2,1)}, bf16[512,384]{1,0:T(8,128)(2,1)}, u32[]{:S(2)}, u32[]{:S(2)}) collective-permute-start(bf16[512,384]{1,0:T(8,128)(2,1)} %get-tuple-element.12), channel_id=1, source_target_pairs={{0,8},{8,16},{16,24},{24,32},{32,40},{40,48},{48,56},{56,0},{64,72... | collective-permute-start | bytes 1179656 | tf_op jit(solution)/shard_map/ppermute | solution.py:28
  57.5 19.4 %collective-permute-start.4 = (bf16[512,384]{1,0:T(8,128)(2,1)}, bf16[512,384]{1,0:T(8,128)(2,1)S(1)}, u32[]{:S(2)}, u32[]{:S(2)}) collective-permute-start(bf16[512,384]{1,0:T(8,128)(2,1)} %get-tuple-element.12), channel_id=1, source_target_pairs={{0,64},{8,72},{16,80},{24,88},{32,96},{40,104},{48,112},{56,120},{... | collective-permute-start | bytes 1179656 | tf_op jit(solution)/shard_map/ppermute | solution.py:28
  76.9 2.2 %copy-start.1 = (f32[4]{0:T(128)S(1)}, f32[4]{0:T(128)}, u32[]{:S(2)}) copy-start(f32[4]{0:T(128)} %sinks.3) | copy-start | bytes 52
  77.2 8.6 %copy-start = (f32[2048]{0:T(1024)S(1)}, f32[2048]{0:T(1024)}, u32[]{:S(2)}) copy-start(f32[2048]{0:T(1024)} %param.10) | copy-start | bytes 24580
  77.2 8.6 %copy-start.2 = (bf16[3,256]{1,0:T(4,128)(2,1)S(1)}, bf16[3,256]{1,0:T(4,128)(2,1)}, u32[]{:S(2)}) copy-start(bf16[3,256]{1,0:T(4,128)(2,1)} %taps_ref.1) | copy-start | bytes 4612
  77.2 8.6 %collective-permute-start.5 = (bf16[384,128]{1,0:T(8,128)(2,1)S(1)}, bf16[384,128]{1,0:T(8,128)(2,1)S(1)}, u32[]{:S(2)}, u32[]{:S(2)}) collective-permute-start(bf16[384,128]{1,0:T(8,128)(2,1)S(1)} %tail.1), channel_id=1, source_target_pairs={{0,8},{8,16},{16,24},{24,32},{32,40},{40,48},{48,56},{56,64},{64,7... | collective-permute-start | bytes 294920 | tf_op jit(solution)/shard_map/ppermute | solution.py:33

commit v10 on v9

--- a/solution.py
+++ b/solution.py
@@ -14,7 +14,7 @@
 COLS = ("fs", "tp")
 SIDE = 8
 LANES = 128
-RIM = 16
+RIM = 8
 VMEM = pl.BlockSpec(memory_space=pltpu.VMEM)
 SMEM = pl.BlockSpec(memory_space=pltpu.SMEM)
 HBM = pl.BlockSpec(memory_space=pltpu.HBM)
@@ -113,7 +113,7 @@
     key_idx = lax.broadcasted_iota(jnp.int32, (WINDOW, WINDOW), 0)
     query_idx = lax.broadcasted_iota(jnp.int32, (WINDOW, WINDOW), 1)
     from_prev = key_idx > query_idx
-    weights, scales, logs = [], [], []
+    weights, logs = [], []
     for pair in range(2):
         both = dot(keys, q[:, pair * LANES : (pair + 1) * LANES], ((1,), (1,)))
         for side in range(2):
@@ -127,23 +127,17 @@
             raised = jnp.exp(scores - top)
             total = jnp.sum(raised, axis=0, keepdims=True) + jnp.exp(sinks[head] - top)
             logs.append(top + jnp.log(total))
-            scales.append(1.0 / total)
-            zero = jnp.zeros_like(raised)
+            share = raised * (1.0 / total)
+            zero = jnp.zeros_like(share)
             weights.append(
                 jnp.concatenate(
-                    [jnp.where(from_prev, raised, zero), jnp.where(from_prev, zero, raised)], axis=0
+                    [jnp.where(from_prev, share, zero), jnp.where(from_prev, zero, share)], axis=0
                 ).astype(jnp.bfloat16)
             )
     outs = []
     for pair in range(2):
         got = dot(values, jnp.concatenate(weights[pair * 2 : pair * 2 + 2], axis=1), ((0,), (0,)))
-        stacked = jnp.concatenate(
-            [
-                got[HEAD_DIM:, :WINDOW] * scales[pair * 2],
-                got[HEAD_DIM:, WINDOW:] * scales[pair * 2 + 1],
-            ],
-            axis=0,
-        )
+        stacked = jnp.concatenate([got[HEAD_DIM:, :WINDOW], got[HEAD_DIM:, WINDOW:]], axis=0)
         outs.append(stacked.T)
     return jnp.concatenate(outs, axis=1), jnp.concatenate(logs, axis=0)
 
@@ -292,7 +286,7 @@
     acc = dot(prev_x[0], parts[0][:, :width])
     for c in range(1, 4):
         acc = acc + dot(prev_x[c], parts[c][:, :width])
-    pad_ref[:8, :] = acc[8:16].astype(jnp.bfloat16).astype(jnp.float32)
+    pad_ref[:8, :] = acc[RIM - 8 : RIM].astype(jnp.bfloat16).astype(jnp.float32)
     span = jnp.concatenate([halo_ref[:WINDOW, :], rows_ref[:WINDOW, :LANES]], axis=0)
     att0, log0 = attend_block(
         rows_ref[:WINDOW, LANES:],

time: 90.3 us -> 89.9 us (level)
  transfers between devices with their start and end apart: 6 -> 6, of which waited for: 2 -> 2; matrix products, arithmetic and copies ran while one was open for 0% -> 0% of each run, Pallas kernels for 15% -> 16%
where the time goes in v10:
time: 89.9 us; the launch traced here: 89.5 us
  blocking collectives  43.8 us (49%)
  Pallas kernels  17.9 us (20%)
  starting transfers between devices  15.9 us (18%)
  waiting for transfers between devices  10 us (11%)
  local copies, waits for them, and re-layouts  0.96 us (1%)
    all_to_all x1, blocking collectives, layer(): own = lax.all_to_all(sent, ('zh', 'yh'), 0, 0)  43.8 us
    ppermute x5, starting transfers between devices, shift(): return lax.ppermute(value, SP, pairs)  14 us
    ppermute x5, waiting for transfers between devices, shift(): return lax.ppermute(value, SP, pairs)  7.83 us
    pallas_call x1, Pallas kernels, norm_classes(): pl.pallas_call(norm_kernel, grid_spec=pltpu.PrefetchScalarGridSpec(num_sc...  5.73 us
    pallas_call x1, Pallas kernels, attention(): pl.pallas_call(attn_kernel, in_specs=[SMEM] + [VMEM] * 4, out_specs=[VMEM...  4.13 us
    pallas_call x1, Pallas kernels, convolution(): pl.pallas_call(conv_kernel, in_specs=[SMEM] * 2 + [VMEM] * 12, out_specs=...  3.95 us
    pallas_call x1, Pallas kernels, early_sums(): pl.pallas_call(early_kernel, in_specs=[VMEM] * 3, out_specs=[VMEM] * 2, o...  2.83 us
    ppermute x1, waiting for transfers between devices, passed_along(): return lax.ppermute(value, SP, [(i, i + 1) for i in range(n - 1)])  2.18 us
  transfers between devices with their start and end apart: 6, of which 2 were waited for; matrix products, arithmetic and copies ran while one was open for 0% of the time, Pallas kernels for 16%

profile of v10, /device:TPU:66, one launch (start us, length us, event | category | flops | bytes accessed | tf_op | source)
XLA Modules:
  0.0 89.5 jit_solution(1805820989169727285)
XLA Ops:
  0.6 0.9 concatenate.3
  1.5 0.1 broadcast_in_dim.2
  1.6 43.8 %all_to_all.5 = bf16[16,32,896]{2,1,0:T(8,128)(2,1)S(1)} all-to-all(bf16[16,32,896]{2,1,0:T(8,128)(2,1)S(1)} %broadcast_in_dim.2), channel_id=1, replica_groups=mesh['zh'=4,'zl'=2,'yh'=4,'yl'=2,'fs'=4,'tp'=2] {'zh','yh'}, dimensions={0} | all-to-all | bytes 1835008 | tf_op jit(solution)/shard_map/all_to_all | solution.py:372
  45.4 1.9 %collective-permute-start.3 = (bf16[512,896]{1,0:T(8,128)(2,1)S(1)}, bf16[512,896]{1,0:T(8,128)(2,1)S(1)}, u32[]{:S(2)}, u32[]{:S(2)}) collective-permute-start(bf16[512,896]{1,0:T(8,128)(2,1)S(1)} %bitcast.5), channel_id=1, source_target_pairs={{0,504},{8,448},{16,456},{24,464},{32,472},{40,480},{48,488},{56,4... | collective-permute-start | bytes 2752520 | tf_op jit(solution)/shard_map/ppermute | solution.py:28
  47.3 1.0 %cut.1 = (bf16[512,384]{1,0:T(8,128)(2,1)}, bf16[512,512]{1,0:T(8,128)(2,1)}) custom-call(bf16[512,896]{1,0:T(8,128)(2,1)S(1)} %bitcast.6), custom_call_target="tpu_custom_call" | custom-call | flops 3900000 | bytes 1048576 | tf_op jit(solution)/shard_map/cut/pallas_call | solution.py:153
  48.3 4.0 %collective-permute-start.1 = (bf16[512,512]{1,0:T(8,128)(2,1)}, bf16[512,512]{1,0:T(8,128)(2,1)S(1)}, u32[]{:S(2)}, u32[]{:S(2)}) collective-permute-start(bf16[512,512]{1,0:T(8,128)(2,1)} %get-tuple-element.14), channel_id=1, source_target_pairs={{0,8},{8,16},{16,24},{24,32},{32,40},{40,48},{48,56},{56,0},{64,72... | collective-permute-start | bytes 1572872 | tf_op jit(solution)/shard_map/ppermute | solution.py:28
  52.3 3.3 %collective-permute-start.2 = (bf16[512,512]{1,0:T(8,128)(2,1)}, bf16[512,512]{1,0:T(8,128)(2,1)S(1)}, u32[]{:S(2)}, u32[]{:S(2)}) collective-permute-start(bf16[512,512]{1,0:T(8,128)(2,1)} %get-tuple-element.14), channel_id=1, source_target_pairs={{0,64},{8,72},{16,80},{24,88},{32,96},{40,104},{48,112},{56,120},{... | collective-permute-start | bytes 1572872 | tf_op jit(solution)/shard_map/ppermute | solution.py:28
  55.6 1.9 %collective-permute-start = (bf16[512,384]{1,0:T(8,128)(2,1)}, bf16[512,384]{1,0:T(8,128)(2,1)}, u32[]{:S(2)}, u32[]{:S(2)}) collective-permute-start(bf16[512,384]{1,0:T(8,128)(2,1)} %get-tuple-element.12), channel_id=1, source_target_pairs={{0,8},{8,16},{16,24},{24,32},{32,40},{40,48},{48,56},{56,0},{64,72... | collective-permute-start | bytes 1179656 | tf_op jit(solution)/shard_map/ppermute | solution.py:28
  57.5 2.9 %collective-permute-start.4 = (bf16[512,384]{1,0:T(8,128)(2,1)}, bf16[512,384]{1,0:T(8,128)(2,1)S(1)}, u32[]{:S(2)}, u32[]{:S(2)}) collective-permute-start(bf16[512,384]{1,0:T(8,128)(2,1)} %get-tuple-element.12), channel_id=1, source_target_pairs={{0,64},{8,72},{16,80},{24,88},{32,96},{40,104},{48,112},{56,120},{... | collective-permute-start | bytes 1179656 | tf_op jit(solution)/shard_map/ppermute | solution.py:28
  60.4 0.1 pad_add_fusion.place
  60.5 5.7 %norm.1 = (bf16[4,1024,512]{2,1,0:T(8,128)(2,1)S(1)}, bf16[8,2048]{1,0:T(8,128)(2,1)S(1)}) custom-call(s32[3]{0:T(128)S(1)} %pad_add_fusion.place, bf16[1024,2048]{1,0:T(8,128)(2,1)} %tok_ref.1, f32[1,2048]{1,0:T(1,128)} %bitcast.9), custom_call_target="tpu_custom_call" | custom-call | flops 19500000 | bytes 1048576 | tf_op jit(solution)/shard_map/norm/pallas_call | solution.py:79
  66.3 7.8 %collective-permute-done.y_ref = bf16[512,384]{1,0:T(8,128)(2,1)} collective-permute-done((bf16[512,384]{1,0:T(8,128)(2,1)}, bf16[512,384]{1,0:T(8,128)(2,1)}, u32[]{:S(2)}, u32[]{:S(2)}) %collective-permute-start) | collective-permute-done | bytes 393248 | tf_op jit(solution)/shard_map/ppermute | solution.py:28
  74.1 2.8 %early.1 = (f32[1024,384]{1,0:T(8,128)S(1)}, f32[1024,512]{1,0:T(8,128)S(1)}) custom-call(bf16[4,1024,512]{2,1,0:T(8,128)(2,1)S(1)} %get-tuple-element.11.x_ref, bf16[512,896]{1,0:T(8,128)(2,1)S(1)} %bitcast.7, bf16[512,384]{1,0:T(8,128)(2,1)} %collective-permute-done.y_ref), custom_call_target="tpu_custom_call" | custom-call | flops 7800000 | bytes 1048576 | tf_op jit(solution)/shard_map/early/pallas_call | solution.py:182
  76.9 0.0 copy-start.1
  76.9 0.0 collective-permute-done.4.w2
  76.9 0.0 collective-permute-done.3.w3
  76.9 0.3 tail.1
  77.2 0.0 copy-start
  77.2 0.0 copy-start.2
  77.2 1.9 %collective-permute-start.5 = (bf16[256,128]{1,0:T(8,128)(2,1)S(1)}, bf16[256,128]{1,0:T(8,128)(2,1)S(1)}, u32[]{:S(2)}, u32[]{:S(2)}) collective-permute-start(bf16[256,128]{1,0:T(8,128)(2,1)S(1)} %tail.1), channel_id=1, source_target_pairs={{0,8},{8,16},{16,24},{24,32},{32,40},{40,48},{48,56},{56,64},{64,7... | collective-permute-start | bytes 196616 | tf_op jit(solution)/shard_map/ppermute | solution.py:33
  79.2 0.0 copy-done.1
  79.2 4.1 %attn.1 = (f32[1024,256]{1,0:T(8,128)S(1)}, f32[4,1024]{1,0:T(4,128)S(1)}, bf16[1024,384]{1,0:T(8,128)(2,1)S(1)}) custom-call(f32[4]{0:T(128)S(1)} %copy-done.1, bf16[4,1024,512]{2,1,0:T(8,128)(2,1)S(1)} %get-tuple-element.11.x_ref, f32[1024,384]{1,0:T(8,128)S(1)} %get-tuple-element.15.sum_ref, bf16[512,384]{1,0:T(8,128)(2,1)S(1)} %collective-permute-done.4.w2, ...), custom_call_target="tpu_custom_call" | custom-call | flops 31200000 | bytes 1048576 | tf_op jit(solution)/shard_map/attn/pallas_call | solution.py:257
  83.3 0.0 collective-permute-done.1.w1
  83.3 0.0 collective-permute-done.2.w2
  83.3 2.2 %collective-permute-done.5.halo_ref = bf16[256,128]{1,0:T(8,128)(2,1)S(1)} collective-permute-done((bf16[256,128]{1,0:T(8,128)(2,1)S(1)}, bf16[256,128]{1,0:T(8,128)(2,1)S(1)}, u32[]{:S(2)}, u32[]{:S(2)}) %collective-permute-start.5) | collective-permute-done | bytes 65568 | tf_op jit(solution)/shard_map/ppermute | solution.py:33
  85.5 0.0 copy-done
  85.5 0.0 copy-done.2
  85.5 4.0 %conv.1 = (bf16[1024,256]{1,0:T(8,128)(2,1)}, f32[4,1024]{1,0:T(4,128)}) custom-call(f32[4]{0:T(128)S(1)} %copy-done.1, s32[3]{0:T(128)S(1)} %pad_add_fusion.place, bf16[4,1024,512]{2,1,0:T(8,128)(2,1)S(1)} %get-tuple-element.11.x_ref, f32[1024,512]{1,0:T(8,128)S(1)} %get-tuple-element.13.sum_ref, bf16[512,896]{1,0:T(8,128)(2,1)S(1)} %bitcast.8, ...), custom_call_target="tpu_custom_call" | custom-call | flops 23400000 | bytes 1048576 | tf_op jit(solution)/shard_map/conv/pallas_call | solution.py:332
Async XLA Ops:
  45.4 31.6 %collective-permute-start.3 = (bf16[512,896]{1,0:T(8,128)(2,1)S(1)}, bf16[512,896]{1,0:T(8,128)(2,1)S(1)}, u32[]{:S(2)}, u32[]{:S(2)}) collective-permute-start(bf16[512,896]{1,0:T(8,128)(2,1)S(1)} %bitcast.5), channel_id=1, source_target_pairs={{0,504},{8,448},{16,456},{24,464},{32,472},{40,480},{48,488},{56,4... | collective-permute-start | bytes 2752520 | tf_op jit(solution)/shard_map/ppermute | solution.py:28
  48.3 35.0 %collective-permute-start.1 = (bf16[512,512]{1,0:T(8,128)(2,1)}, bf16[512,512]{1,0:T(8,128)(2,1)S(1)}, u32[]{:S(2)}, u32[]{:S(2)}) collective-permute-start(bf16[512,512]{1,0:T(8,128)(2,1)} %get-tuple-element.14), channel_id=1, source_target_pairs={{0,8},{8,16},{16,24},{24,32},{32,40},{40,48},{48,56},{56,0},{64,72... | collective-permute-start | bytes 1572872 | tf_op jit(solution)/shard_map/ppermute | solution.py:28
  52.3 31.0 %collective-permute-start.2 = (bf16[512,512]{1,0:T(8,128)(2,1)}, bf16[512,512]{1,0:T(8,128)(2,1)S(1)}, u32[]{:S(2)}, u32[]{:S(2)}) collective-permute-start(bf16[512,512]{1,0:T(8,128)(2,1)} %get-tuple-element.14), channel_id=1, source_target_pairs={{0,64},{8,72},{16,80},{24,88},{32,96},{40,104},{48,112},{56,120},{... | collective-permute-start | bytes 1572872 | tf_op jit(solution)/shard_map/ppermute | solution.py:28
  55.6 18.5 %collective-permute-start = (bf16[512,384]{1,0:T(8,128)(2,1)}, bf16[512,384]{1,0:T(8,128)(2,1)}, u32[]{:S(2)}, u32[]{:S(2)}) collective-permute-start(bf16[512,384]{1,0:T(8,128)(2,1)} %get-tuple-element.12), channel_id=1, source_target_pairs={{0,8},{8,16},{16,24},{24,32},{32,40},{40,48},{48,56},{56,0},{64,72... | collective-permute-start | bytes 1179656 | tf_op jit(solution)/shard_map/ppermute | solution.py:28
  57.5 19.4 %collective-permute-start.4 = (bf16[512,384]{1,0:T(8,128)(2,1)}, bf16[512,384]{1,0:T(8,128)(2,1)S(1)}, u32[]{:S(2)}, u32[]{:S(2)}) collective-permute-start(bf16[512,384]{1,0:T(8,128)(2,1)} %get-tuple-element.12), channel_id=1, source_target_pairs={{0,64},{8,72},{16,80},{24,88},{32,96},{40,104},{48,112},{56,120},{... | collective-permute-start | bytes 1179656 | tf_op jit(solution)/shard_map/ppermute | solution.py:28
  76.9 2.2 %copy-start.1 = (f32[4]{0:T(128)S(1)}, f32[4]{0:T(128)}, u32[]{:S(2)}) copy-start(f32[4]{0:T(128)} %sinks.3) | copy-start | bytes 52
  77.2 8.3 %copy-start = (f32[2048]{0:T(1024)S(1)}, f32[2048]{0:T(1024)}, u32[]{:S(2)}) copy-start(f32[2048]{0:T(1024)} %param.10) | copy-start | bytes 24580
  77.2 8.3 %copy-start.2 = (bf16[3,256]{1,0:T(4,128)(2,1)S(1)}, bf16[3,256]{1,0:T(4,128)(2,1)}, u32[]{:S(2)}) copy-start(bf16[3,256]{1,0:T(4,128)(2,1)} %taps_ref.1) | copy-start | bytes 4612
  77.2 8.3 %collective-permute-start.5 = (bf16[256,128]{1,0:T(8,128)(2,1)S(1)}, bf16[256,128]{1,0:T(8,128)(2,1)S(1)}, u32[]{:S(2)}, u32[]{:S(2)}) collective-permute-start(bf16[256,128]{1,0:T(8,128)(2,1)S(1)} %tail.1), channel_id=1, source_target_pairs={{0,8},{8,16},{16,24},{24,32},{32,40},{40,48},{48,56},{56,64},{64,7... | collective-permute-start | bytes 196616 | tf_op jit(solution)/shard_map/ppermute | solution.py:33
